TPU v7x, 512 devices: a whole 4x4x16 slice. The times are simulated.
512 devices in a mesh: sp: 64 (over z, y), tp: 8 (over x, core).
Axes of the slice: x: 4, y: 4, z: 16, core: 2. Of those that a mesh axis runs over, the one named last changes fastest.
Arguments:
- query_logits: bfloat16 [8192, 1024], P('sp', 'tp'), may hold values from -6 to 6
- value_rows: bfloat16 [8192, 1024], P('sp', 'tp'), may hold values from -6 to 6
- onward_forget_logits: bfloat16 [8192, 1024], P('sp', 'tp'), may hold values from -5.5 to 5.5
- reverse_forget_logits: bfloat16 [8192, 1024], P('sp', 'tp'), may hold values from -5.5 to 5.5
- output_gate_logits: bfloat16 [8192, 1024], P('sp', 'tp'), may hold values from -6 to 6
- onward_floor_gap: float32 [1024], P('tp'), may hold values from 0 to 0.12, as said below
- reverse_floor_gap: float32 [1024], P('tp'), may hold values from 0 to 0.12, as said below
- extra_log_decay: float32 [8192, 8], P('sp', 'tp'), may hold values from -2.1 to 0
- per_head_gain: float32 [128], replicated, may hold values from 0.1 to 1.9
- residual: bfloat16 [8192, 2048], P('sp', 'tp'), may hold values from -8 to 8
- output_matrix: bfloat16 [1024, 2048], P(None, 'tp'), may hold values from -0.375 to 0.375
- inner_norm_gain: float32 [2048], P('tp'), may hold values from 0.1 to 1.9
- inner_norm_bias: float32 [2048], P('tp'), may hold values from -1.5 to 1.5
- gate_matrix: bfloat16 [2048, 5632], P('sp', 'tp'), may hold values from -0.125 to 0.125
- up_matrix: bfloat16 [2048, 5632], P('sp', 'tp'), may hold values from -0.125 to 0.125
- down_matrix: bfloat16 [5632, 2048], P('tp', 'sp'), may hold values from -0.15625 to 0.15625
- closing_norm_gain: float32 [2048], P('tp'), may hold values from 0.1 to 1.9
- closing_norm_bias: float32 [2048], P('tp'), may hold values from -1.5 to 1.5
Outputs:
- layer_output: bfloat16 [8192, 2048], P('sp', 'tp')
Inputs may be any that keep to these rules, and one draw needn't show every extreme that they name: `onward_floor_gap`: positive. `reverse_floor_gap`: positive.
All inputs are finite; a program needn't handle non-finite values.
Results may differ from a plain program's by a relative error of at most 0.014.
Values may be sent and summed in bfloat16 or wider, within the bound.
No kernel may reach another device: no remote copies, remote signals or barrier semaphores. Data moves between devices by JAX's collectives and lax.ppermute only.
A program may use at most 64 MiB of HBM per device.

v0:
```python
import math

import jax
import jax.numpy as jnp
from jax import lax
from jax.sharding import Mesh
from jax.sharding import PartitionSpec as P

D = 2048
SP = ("sp_0", "sp_1")


highest_precision = lax.Precision.HIGHEST
alpha_mix = 2.0**0.25
norm_eps = 1e-05
head_eps = 1e-06


def turned_gather(arrays, axis, dims):
    turned = [jnp.moveaxis(a, dim, 0) for a, dim in zip(arrays, dims)]
    widths = [t[0].size for t in turned]
    both = jnp.concatenate([t.reshape(-1, w) for t, w in zip(turned, widths)], axis=1)
    out = lax.all_gather(both, axis, axis=0, tiled=True)
    blocks = jnp.split(out, [sum(widths[:k]) for k in range(1, len(widths))], axis=1)
    return tuple(
        (
            jnp.moveaxis(b.reshape(-1, *t.shape[1:]), 0, dim)
            for b, t, dim in zip(blocks, turned, dims)
        )
    )


def neutral_like(x, identity):
    return jax.tree.map(
        lambda a, e: jnp.broadcast_to(jnp.asarray(e, a.dtype), a.shape), x, identity
    )


def collected_together(x, axis):
    leaves = jax.tree.leaves(x)
    order = sorted(range(len(leaves)), key=lambda k: -leaves[k].size)
    width = (1, *leaves[order[0]].shape)[-1]
    lines = [
        jnp.pad(leaves[k].reshape(-1), (0, -leaves[k].size % width)).reshape(-1, width)
        for k in order
    ]
    both, at, found = (lax.all_gather(jnp.concatenate(lines), axis), 0, {})
    for k, line in zip(order, lines):
        share = both[:, at : at + len(line)].reshape(len(both), -1)
        found[k] = share[:, : leaves[k].size].reshape(-1, *leaves[k].shape)
        at += len(line)
    numbers = iter(range(len(leaves)))
    return jax.tree.map(lambda _: found[next(numbers)], x)


def prefix_by_axis(x, axes, combine, identity, reverse):
    before = start = neutral_like(x, identity)
    total = x
    for axis in reversed(axes):
        devices, mine = (lax.axis_size(axis), lax.axis_index(axis))
        pieces = collected_together(
            jax.tree.map(lambda part, kind: part.astype(kind), total, (jnp.bfloat16, jnp.bfloat16)),
            axis,
        )
        inside, total = (start, start)
        for k in reversed(range(devices)) if reverse else range(devices):
            passed = k > mine if reverse else k < mine
            total = combine(
                total, jax.tree.map(lambda part, own: part[k].astype(own.dtype), pieces, x)
            )
            inside = jax.tree.map(lambda new, old: jnp.where(passed, new, old), total, inside)
        before = combine(inside, before)
    return before


def sent_to_all(x, axis):
    devices = lax.axis_size(axis)
    return lax.all_to_all(jnp.broadcast_to(x[None], (devices, *x.shape)), axis, 0, 0, tiled=True)


def joined_along(blocks, dim):
    shape = list(blocks.shape[1:])
    shape[dim] *= blocks.shape[0]
    return jnp.moveaxis(blocks, 0, dim).reshape(shape)


def gather_directly(x, axis, dim):
    blocks = sent_to_all(x, axis)
    return joined_along(blocks, dim)


def of_everyone(x, axis):
    return sent_to_all(x, axis).sum(axis=0)


def packed_total(arrays, axis):
    vector, at, done = (jnp.concatenate([a.reshape(-1) for a in arrays]), 0, [])
    total = of_everyone(vector, axis)
    for a in arrays:
        done.append(total[at : at + a.size].reshape(a.shape))
        at += a.size
    return tuple(done)


def cut_along(x, dim, devices):
    before, after = (x.shape[:dim], x.shape[dim + 1 :])
    return jnp.moveaxis(x.reshape(*before, devices, -1, *after), dim, 0)


def sent_and_summed(x, axis, dim):
    blocks = cut_along(x, dim, lax.axis_size(axis))
    arrived = lax.all_to_all(blocks, axis, split_axis=0, concat_axis=0, tiled=True)
    return arrived.astype(jnp.float32).sum(axis=0)


def decay_factors(unscaled_input, lower_bound_gap, extra_decays):
    decay_factor = lower_bound_gap * jax.nn.sigmoid(-unscaled_input.astype(jnp.float32))
    return (jnp.log1p(-decay_factor) + extra_decays, decay_factor)


def local_pass(query, keys, values, log_decay):
    rows, head_count, model_width = query.shape
    span = math.gcd(rows, 128)
    count = rows // span
    triangle = jnp.tril(jnp.ones((span, span), jnp.float32))

    def blocks(array):
        return array.reshape(count, span, head_count, array.shape[2])

    def advance(carry, inputs):
        running_state, offset = carry
        query_block, key_block, value_tile, log_block = inputs
        running = jnp.cumsum(log_block, axis=0)
        final_index = running[-1]
        decayed_query = query_block * jnp.exp(running)
        key_inverse = key_block * jnp.exp(-running)
        key_stop = key_block * jnp.exp(final_index[None] - running)
        scores = (
            jnp.einsum("thk,shk->hts", decayed_query, key_inverse, precision=highest_precision)
            * triangle[None]
        )
        inner = jnp.einsum("hts,shv->thv", scores, value_tile, precision=highest_precision)
        carried_state = jnp.einsum(
            "nex,exl->nel", decayed_query, running_state, precision=highest_precision
        )
        query_start = decayed_query * jnp.exp(offset)[None]
        running_state = jnp.exp(final_index)[:, :, None] * running_state + jnp.einsum(
            "ojy,oje->jye", key_stop, value_tile, precision=highest_precision
        )
        return ((running_state, offset + final_index), (inner + carried_state, query_start))

    start = (
        jnp.zeros((head_count, model_width, values.shape[2]), jnp.float32),
        jnp.zeros((head_count, model_width), jnp.float32),
    )
    final, outputs = lax.scan(
        advance, start, (blocks(query), blocks(keys), blocks(values), blocks(log_decay))
    )
    result = outputs[0].reshape(rows, head_count, values.shape[2])
    query_start = outputs[1].reshape(rows, head_count, model_width)
    return (result, query_start, final[1], final[0])


def join(earlier, later):
    return (earlier[0] + later[0], jnp.exp(later[0])[:, :, None] * earlier[1] + later[1])


def row_norm(before, moments, gain, bias):
    mean = moments[0] / D
    spread = moments[1] / D - mean * mean
    return (before - mean[:, None]) * lax.rsqrt(spread + norm_eps)[:, None] * gain + bias


def shards(
    query_logits,
    value_rows,
    onward_forget_logits,
    reverse_forget_logits,
    output_gate_logits,
    onward_floor_gap,
    reverse_floor_gap,
    extra_log_decay,
    per_head_gain,
    residual,
    output_matrix,
    inner_norm_gain,
    inner_norm_bias,
    gate_matrix,
    up_matrix,
    down_matrix,
    closing_norm_gain,
    closing_norm_bias,
):
    gate_whole, up_whole, down_whole = turned_gather(
        (gate_matrix, up_matrix, down_matrix), SP, (0, 0, 1)
    )
    rows = query_logits.shape[0]
    head_count = extra_log_decay.shape[1]
    model_width = query_logits.shape[1] // head_count
    shape_head = (rows, head_count, model_width)
    query = jax.nn.silu(query_logits.astype(jnp.float32)).reshape(shape_head)
    values = value_rows.astype(jnp.float32).reshape(shape_head)
    extra_decays = jnp.repeat(extra_log_decay, model_width, axis=1)
    onward_log_decay, onward_key_rows = decay_factors(
        onward_forget_logits, onward_floor_gap, extra_decays
    )
    reverse_log_decay, reverse_key_rows = decay_factors(
        reverse_forget_logits, reverse_floor_gap, extra_decays
    )
    empty_total = jnp.zeros((head_count, model_width), jnp.float32)
    empty_state = jnp.zeros((head_count, model_width, model_width), jnp.float32)
    upcoming_part, upcoming_begin, ahead_total, ahead_state = local_pass(
        query, onward_key_rows.reshape(shape_head), values, onward_log_decay.reshape(shape_head)
    )
    incoming_state = prefix_by_axis(
        (ahead_total, ahead_state), SP, join, (empty_total, empty_state), False
    )
    upcoming_part = upcoming_part + jnp.einsum(
        "nex,exl->nel", upcoming_begin, incoming_state[1], precision=highest_precision
    )
    preceding_part, preceding_begin, behind_total, behind_state = local_pass(
        jnp.flip(query, axis=0),
        jnp.flip(reverse_key_rows.reshape(shape_head), axis=0),
        jnp.flip(values, axis=0),
        jnp.flip(reverse_log_decay.reshape(shape_head), axis=0),
    )
    arriving_state = prefix_by_axis(
        (behind_total, behind_state), SP, join, (empty_total, empty_state), True
    )
    preceding_part = jnp.flip(
        preceding_part
        + jnp.einsum(
            "nex,exl->nel", preceding_begin, arriving_state[1], precision=highest_precision
        ),
        axis=0,
    )
    mixed = upcoming_part + preceding_part
    normed = (
        mixed * lax.rsqrt(jnp.mean(mixed * mixed, axis=2, keepdims=True) + head_eps) * per_head_gain
    )
    gated = (
        normed.reshape(rows, head_count * model_width)
        * jax.nn.silu(output_gate_logits.astype(jnp.float32))
    ).astype(jnp.bfloat16)
    mixer = jnp.dot(
        gather_directly(gated, "tp", 1), output_matrix, preferred_element_type=jnp.float32
    )
    before_middle = alpha_mix * residual.astype(jnp.float32) + mixer
    moments = packed_total(
        (jnp.sum(before_middle, axis=1), jnp.sum(before_middle * before_middle, axis=1)), "tp"
    )
    middle = row_norm(before_middle, moments, inner_norm_gain, inner_norm_bias).astype(jnp.bfloat16)
    whole = gather_directly(middle, "tp", 1)
    gate = jnp.dot(whole, gate_whole, preferred_element_type=jnp.float32)
    up = jnp.dot(whole, up_whole, preferred_element_type=jnp.float32)
    hidden = (jax.nn.silu(gate) * up).astype(jnp.bfloat16)
    partial_value = jnp.dot(hidden, down_whole, preferred_element_type=jnp.float32)
    feed = sent_and_summed(partial_value.astype(jnp.bfloat16), "tp", 1)
    before_final = alpha_mix * middle.astype(jnp.float32) + feed
    closing = packed_total(
        (jnp.sum(before_final, axis=1), jnp.sum(before_final * before_final, axis=1)), "tp"
    )
    return row_norm(before_final, closing, closing_norm_gain, closing_norm_bias).astype(
        jnp.bfloat16
    )


def solution(mesh):
    torus = Mesh(mesh.devices.reshape(16, 4, mesh.shape["tp"]), ("sp_0", "sp_1", "tp"))
    in_specs = (
        P(SP, "tp"),
        P(SP, "tp"),
        P(SP, "tp"),
        P(SP, "tp"),
        P(SP, "tp"),
        P("tp"),
        P("tp"),
        P(SP, "tp"),
        P(),
        P(SP, "tp"),
        P(None, "tp"),
        P("tp"),
        P("tp"),
        P(SP, "tp"),
        P(SP, "tp"),
        P("tp", SP),
        P("tp"),
        P("tp"),
    )
    out_specs = P(SP, "tp")
    return jax.shard_map(
        shards, mesh=torus, in_specs=in_specs, out_specs=out_specs, check_vma=False
    )
```

profile of v0, /device:TPU:1, one launch (start us, length us, event | category | flops | bytes accessed | tf_op | source)
XLA Modules:
  0.0 213.9 jit_solution(1228011670985235673)
XLA Ops:
  6.6 1.7 concatenate.26
  8.4 0.8 reverse.15
  9.2 0.9 divide_multiply_fusion
  10.3 0.9 multiply_reduce_fusion.4
  11.4 0.3 fusion.25
  11.7 10.5 %all-gather.6 = bf16[4,129,128]{2,1,0:T(8,128)(2,1)S(1)} all-gather(bf16[1,129,128]{2,1,0:T(8,128)(2,1)S(1)} %maximum_bitcast_fusion.2), channel_id=4, replica_groups=mesh['sp_0'=16,'sp_1'=4,'tp'=8] {'sp_1'}, dimensions={0}, use_global_device_ids=true | all-gather | bytes 165120 | tf_op jit(solution)/shard_map/all_gather | solution.py:47
  22.4 35.3 %all-gather.7 = bf16[16,129,128]{2,1,0:T(8,128)(2,1)S(1)} all-gather(bf16[1,129,128]{2,1,0:T(8,128)(2,1)S(1)} %maximum_bitcast_fusion.3), channel_id=5, replica_groups=mesh['sp_0'=16,'sp_1'=4,'tp'=8] {'sp_0'}, dimensions={0}, use_global_device_ids=true | all-gather | bytes 561408 | tf_op jit(solution)/shard_map/all_gather | solution.py:47
  57.7 0.7 convolution_bitcast_fusion
  58.4 0.3 convolution_multiply_fusion
  59.0 1.1 fusion.24
  60.1 9.6 %all-gather.4 = bf16[4,129,128]{2,1,0:T(8,128)(2,1)S(1)} all-gather(bf16[1,129,128]{2,1,0:T(8,128)(2,1)S(1)} %maximum_bitcast_fusion), channel_id=2, replica_groups=mesh['sp_0'=16,'sp_1'=4,'tp'=8] {'sp_1'}, dimensions={0}, use_global_device_ids=true | all-gather | bytes 165120 | tf_op jit(solution)/shard_map/all_gather | solution.py:47
  69.9 23.8 %all-gather.5 = bf16[16,129,128]{2,1,0:T(8,128)(2,1)S(1)} all-gather(bf16[1,129,128]{2,1,0:T(8,128)(2,1)S(1)} %maximum_bitcast_fusion.1), channel_id=3, replica_groups=mesh['sp_0'=16,'sp_1'=4,'tp'=8] {'sp_0'}, dimensions={0}, use_global_device_ids=true | all-gather | bytes 561408 | tf_op jit(solution)/shard_map/all_gather | solution.py:47
  93.7 1.5 convolution_bitcast_fusion.2
  95.2 0.3 convolution_multiply_fusion.1
  96.1 28.2 %all_to_all.27 = bf16[8,128,128]{1,2,0:T(8,128)(2,1)S(1)} all-to-all(bf16[8,128,128]{1,2,0:T(8,128)(2,1)S(1)} %broadcast_in_dim.32), channel_id=1, replica_groups=mesh['sp_0'=16,'sp_1'=4,'tp'=8] {'tp'}, dimensions={0} | all-to-all | bytes 524288 | tf_op jit(solution)/shard_map/all_to_all | solution.py:78
  124.3 0.4 fusion.398
  124.7 8.0 %all_to_all.28 = f32[8,1,256]{2,1,0:T(1,128)S(1)} all-to-all(f32[8,1,256]{2,1,0:T(1,128)S(1)} %broadcast_in_dim.33), channel_id=1, replica_groups=mesh['sp_0'=16,'sp_1'=4,'tp'=8] {'tp'}, dimensions={0} | all-to-all | bytes 16384 | tf_op jit(solution)/shard_map/all_to_all | solution.py:78
  133.1 12.3 %all_to_all.29 = bf16[8,128,256]{1,2,0:T(8,128)(2,1)S(1)} all-to-all(bf16[8,128,256]{1,2,0:T(8,128)(2,1)S(1)} %broadcast_in_dim.34), channel_id=1, replica_groups=mesh['sp_0'=16,'sp_1'=4,'tp'=8] {'tp'}, dimensions={0} | all-to-all | bytes 1048576 | tf_op jit(solution)/shard_map/all_to_all | solution.py:78
  145.4 20.3 %all-gather.10.cloned.1.call-done = bf16[2048,2112]{1,0:T(8,128)(2,1)} async-done(((bf16[32,2112]{1,0:T(8,128)(2,1)}), bf16[2048,2112]{1,0:T(8,128)(2,1)}) %all-gather.10.cloned.1.call-update) | async-done | bytes 8650768 | tf_op jit(solution)/shard_map/all_gather | solution.py:23
  165.8 3.2 %fusion.4 = f32[128,704]{0,1:T(8,128)S(1)} fusion(bf16[128,2048]{0,1:T(8,128)(2,1)S(1)} %bitcast.195, bf16[2048,2112]{1,0:T(8,128)(2,1)} %all-gather.10.cloned.1.call-done), kind=kOutput, calls=%fused_computation.4 | convolution fusion | flops 369098752 | bytes 4030464 | tf_op jit(solution)/shard_map/dot_general | solution.py:254
  169.0 7.2 %fusion.6 = bf16[128,2048]{1,0:T(8,128)(2,1)S(1)} fusion(bf16[2048,2112]{1,0:T(8,128)(2,1)} %all-gather.10.cloned.1.call-done, bf16[128,2048]{0,1:T(8,128)(2,1)S(1)} %bitcast.196, f32[128,704]{0,1:T(8,128)S(1)} %fusion.4), kind=kOutput, calls=%fused_computation.6 | convolution fusion | flops 739000320 | bytes 7700480 | tf_op jit(solution)/shard_map/dot_general | solution.py:257
  176.3 21.7 %all_to_all.30 = bf16[8,128,256]{2,1,0:T(8,128)(2,1)S(1)} all-to-all(bf16[8,128,256]{2,1,0:T(8,128)(2,1)S(1)} %bitcast.189), channel_id=1, replica_groups=mesh['sp_0'=16,'sp_1'=4,'tp'=8] {'tp'}, dimensions={0} | all-to-all | bytes 1048576 | tf_op jit(solution)/shard_map/all_to_all | solution.py:112
  198.2 8.0 %all_to_all.31 = f32[8,1,256]{2,1,0:T(1,128)S(1)} all-to-all(f32[8,1,256]{2,1,0:T(1,128)S(1)} %broadcast_in_dim.35), channel_id=1, replica_groups=mesh['sp_0'=16,'sp_1'=4,'tp'=8] {'tp'}, dimensions={0} | all-to-all | bytes 16384 | tf_op jit(solution)/shard_map/all_to_all | solution.py:78
  206.3 0.8 add_convert_fusion
  (69 shorter events, 2.3 us)
Async XLA Ops:
  6.5 117.7 %copy-start = (bf16[1024,256]{1,0:T(8,128)(2,1)S(1)}, bf16[1024,256]{1,0:T(8,128)(2,1)}, u32[]{:S(2)}) copy-start(bf16[1024,256]{1,0:T(8,128)(2,1)} %param.28) | copy-start | bytes 1572868
  6.5 89.0 %copy-start.1 = (bf16[128,128]{1,0:T(8,128)(2,1)S(1)}, bf16[128,128]{1,0:T(8,128)(2,1)}, u32[]{:S(2)}) copy-start(bf16[128,128]{1,0:T(8,128)(2,1)} %param.19) | copy-start | bytes 98308
  6.5 88.7 %copy-start.10 = (f32[128]{0:T(128)S(1)}, f32[128]{0:T(128)}, u32[]{:S(2)}) copy-start(f32[128]{0:T(128)} %param.23) | copy-start | bytes 1540
  6.5 88.7 %copy-start.5 = (bf16[128,128]{1,0:T(8,128)(2,1)S(1)}, bf16[128,128]{1,0:T(8,128)(2,1)}, u32[]{:S(2)}) copy-start(bf16[128,128]{1,0:T(8,128)(2,1)} %param.20) | copy-start | bytes 98308
  6.5 88.7 %copy-start.3 = (bf16[128,128]{1,0:T(8,128)(2,1)S(1)}, bf16[128,128]{1,0:T(8,128)(2,1)}, u32[]{:S(2)}) copy-start(bf16[128,128]{1,0:T(8,128)(2,1)} %param.18) | copy-start | bytes 98308
  6.6 89.3 %copy-start.11 = (f32[128]{0:T(128)S(1)}, f32[128]{0:T(128)}, u32[]{:S(2)}) copy-start(f32[128]{0:T(128)} %param.26) | copy-start | bytes 1540
  6.6 89.3 %copy-start.4 = (bf16[128,128]{1,0:T(8,128)(2,1)S(1)}, bf16[128,128]{1,0:T(8,128)(2,1)}, u32[]{:S(2)}) copy-start(bf16[128,128]{1,0:T(8,128)(2,1)} %param.22) | copy-start | bytes 98308
  6.6 117.7 %copy-start.2 = (bf16[128,256]{1,0:T(8,128)(2,1)S(1)}, bf16[128,256]{1,0:T(8,128)(2,1)}, u32[]{:S(2)}) copy-start(bf16[128,256]{1,0:T(8,128)(2,1)} %param.27) | copy-start | bytes 196612
  6.6 126.2 %copy-start.6 = (f32[256]{0:T(256)S(1)}, f32[256]{0:T(256)}, u32[]{:S(2)}) copy-start(f32[256]{0:T(256)} %param.30) | copy-start | bytes 3076
  6.6 126.2 %copy-start.7 = (f32[256]{0:T(256)S(1)}, f32[256]{0:T(256)}, u32[]{:S(2)}) copy-start(f32[256]{0:T(256)} %param.29) | copy-start | bytes 3076
  6.6 159.1 %all-gather.10.cloned.1.call-start = ((), (), s32[]{:S(2)}) async-start(), calls=%async_computation.5 | async-start | bytes 9052160 | tf_op jit(solution)/shard_map/all_gather | solution.py:23
  165.7 40.5 %copy-start.8 = (f32[256]{0:T(256)S(1)}, f32[256]{0:T(256)}, u32[]{:S(2)}) copy-start(f32[256]{0:T(256)} %param.35) | copy-start | bytes 3076
  165.8 40.6 %copy-start.9 = (f32[256]{0:T(256)S(1)}, f32[256]{0:T(256)}, u32[]{:S(2)}) copy-start(f32[256]{0:T(256)} %param.34) | copy-start | bytes 3076
Sparse Core Ops, SparseCore 0:
  10.4 155.3 all-gather.9
where the time goes:
time: 215 us; the launch traced here: 214 us
  blocking collectives  157 us (73%)
  waiting for transfers between devices  20.4 us (9%)
  matrix products  15.4 us (7%)
  between operations  13.9 us (6%)
  other arithmetic  3.86 us (2%)
  local copies, waits for them, and re-layouts  2.97 us (1%)
    all_gather x4, blocking collectives, collected_together(): both, at, found = (lax.all_gather(jnp.concatenate(lines), axis), 0, {})  79.2 us
    all_to_all x4, blocking collectives, sent_to_all(): lax.all_to_all(jnp.broadcast_to(x[None], (devices, *x.shape)), axis, 0, 0...  56.6 us
    all_to_all x1, blocking collectives, sent_and_summed(): lax.all_to_all(blocks, axis, split_axis=0, concat_axis=0, tiled=True)  21.7 us
    all_gather x1, waiting for transfers between devices, turned_gather(): out = lax.all_gather(both, axis, axis=0, tiled=True)  20.3 us
    dot_general x1, matrix products, shards(): jnp.dot(hidden, down_whole, preferred_element_type=jnp.float32)  7.25 us
  transfers between devices with their start and end apart: 1, of which 1 were waited for; matrix products, arithmetic and copies ran while one was open for 4% of the time, Pallas kernels for 0%

commit v1 on v0

v1 whole, which is shorter than its diff:
```python
import math

import jax
import jax.numpy as jnp
from jax import lax
from jax.experimental import pallas as pl
from jax.experimental.pallas import tpu as pltpu
from jax.sharding import Mesh
from jax.sharding import PartitionSpec as P

D = 2048
SP = ("z", "ya", "yb")
PAIR = ("yb", "tp")
HALF = 384

highest_precision = lax.Precision.HIGHEST
alpha_mix = 2.0**0.25
norm_eps = 1e-05
head_eps = 1e-06


def to_all(x, axes):
    devices = lax.axis_size(axes)
    return lax.all_to_all(jnp.broadcast_to(x[None], (devices, *x.shape)), axes, 0, 0, tiled=True)


def packed_total(arrays, axis):
    vector, at, done = (jnp.concatenate([a.reshape(-1) for a in arrays]), 0, [])
    total = to_all(vector, axis).sum(axis=0)
    for a in arrays:
        done.append(total[at : at + a.size].reshape(a.shape))
        at += a.size
    return tuple(done)


def decay_factors(unscaled_input, lower_bound_gap, extra_decays):
    decay_factor = lower_bound_gap * jax.nn.sigmoid(-unscaled_input.astype(jnp.float32))
    return (jnp.log1p(-decay_factor) + extra_decays, decay_factor)


def local_pass(query, keys, values, log_decay):
    rows = query.shape[0]
    triangle = jnp.tril(jnp.ones((rows, rows), jnp.float32))
    running = jnp.cumsum(log_decay, axis=0)
    total = running[-1]
    decayed_query = query * jnp.exp(running)
    key_inverse = keys * jnp.exp(-running)
    key_stop = keys * jnp.exp(total[None] - running)
    scores = (
        jnp.einsum("tk,sk->ts", decayed_query, key_inverse, precision=highest_precision) * triangle
    )
    inner = jnp.einsum("ts,sv->tv", scores, values, precision=highest_precision)
    state = jnp.einsum("ok,ov->kv", key_stop, values, precision=highest_precision)
    return (inner, decayed_query, total, state)


def scan_kernel(chunks, local_ref, before_ref):
    local = local_ref[...].astype(jnp.float32)
    decay = jnp.exp(local[:, 4:8])
    state = local[:, 0:4]
    ahead = [None] * chunks
    run = jnp.zeros((2, 128), jnp.float32)
    for c in range(chunks):
        ahead[c] = run
        run = decay[c, 0:2] * run + state[c, 0:2]
    run = jnp.zeros((2, 128), jnp.float32)
    for c in reversed(range(chunks)):
        before_ref[c] = jnp.concatenate([ahead[c], run], axis=0)
        run = decay[c, 2:4] * run + state[c, 2:4]


def exchanged_states(forward, backward):
    chunks = lax.axis_size(SP)
    mine = []
    for total, state in (forward, backward):
        mine.append(state.reshape(chunks, 2, 128))
    for total, state in (forward, backward):
        mine.append(jnp.broadcast_to(total.reshape(chunks, 2, 1), (chunks, 2, 128)))
    packed = jnp.concatenate(mine, axis=1).astype(jnp.bfloat16)
    arrived = lax.all_to_all(packed, SP, 0, 0, tiled=True)
    before = pl.pallas_call(
        lambda *refs: scan_kernel(chunks, *refs),
        out_shape=jax.ShapeDtypeStruct((chunks, 4, 128), jnp.float32),
        name="scan",
    )(arrived)
    back = lax.all_to_all(before.astype(jnp.bfloat16), SP, 0, 0, tiled=True).astype(jnp.float32)
    return back[:, 0:2].reshape(128, 128), back[:, 2:4].reshape(128, 128)


def gathered_weights(gate, up, down):
    both = jnp.stack([gate, up, down.T])
    first = both[:, :, :HALF]
    second = jnp.pad(both[:, :, HALF:], ((0, 0), (0, 0), (0, 2 * HALF - both.shape[2])))
    halves = jnp.stack([first, second, first, second])
    arrived = lax.all_to_all(halves, ("ya", "yb"), 0, 0, tiled=True)
    shard = jnp.moveaxis(arrived, 0, 1).reshape(3 * 128, HALF)
    return lax.all_gather(shard, "z", axis=0, tiled=True).reshape(-1, 3, 128, HALF)


def feed_kernel(steps, rows_ref, enter_ref, leave_ref, out_ref, gate_ref, up_ref, hidden_ref):
    phase, step = pl.program_id(0), pl.program_id(1)

    @pl.when(jnp.logical_and(phase == 0, step == 0))
    def _():
        gate_ref[...] = jnp.zeros_like(gate_ref)
        up_ref[...] = jnp.zeros_like(up_ref)

    @pl.when(phase == 0)
    def _():
        x = rows_ref[0]
        gate = jnp.concatenate([enter_ref[0, 0], enter_ref[1, 0]], axis=0)
        up = jnp.concatenate([enter_ref[0, 1], enter_ref[1, 1]], axis=0)
        gate_ref[...] += jnp.dot(x, gate, preferred_element_type=jnp.float32)
        up_ref[...] += jnp.dot(x, up, preferred_element_type=jnp.float32)

    @pl.when(jnp.logical_and(phase == 0, step == steps - 1))
    def _():
        gate = gate_ref[...]
        hidden_ref[...] = (gate * jax.nn.sigmoid(gate) * up_ref[...]).astype(jnp.bfloat16)

    @pl.when(phase == 1)
    def _():
        down = jnp.concatenate([leave_ref[0, 0], leave_ref[1, 0]], axis=0)
        product = lax.dot_general(
            hidden_ref[...],
            down,
            (((1,), (1,)), ((), ())),
            preferred_element_type=jnp.float32,
        )
        out_ref[:, 0] = product.astype(jnp.bfloat16).reshape(out_ref.shape[0], *out_ref.shape[2:])


def feed_forward(rows, weights):
    steps, count, width = rows.shape
    return pl.pallas_call(
        lambda *refs: feed_kernel(steps, *refs),
        grid=(2, steps),
        in_specs=[
            pl.BlockSpec((1, count, width), lambda p, s: (jnp.where(p == 0, s, steps - 1), 0, 0)),
            pl.BlockSpec(
                (2, 2, 128, HALF), lambda p, s: (jnp.where(p == 0, s, steps - 1), 0, 0, 0)
            ),
            pl.BlockSpec((2, 1, 128, HALF), lambda p, s: (jnp.where(p == 0, 0, s), 2, 0, 0)),
        ],
        out_specs=pl.BlockSpec(
            (2, 1, count // 2, width), lambda p, s: (0, jnp.where(p == 0, 0, s), 0, 0)
        ),
        out_shape=jax.ShapeDtypeStruct((2, steps, count // 2, width), jnp.bfloat16),
        scratch_shapes=[
            pltpu.VMEM((count, HALF), jnp.float32),
            pltpu.VMEM((count, HALF), jnp.float32),
            pltpu.VMEM((count, HALF), jnp.bfloat16),
        ],
        compiler_params=pltpu.CompilerParams(dimension_semantics=("arbitrary", "arbitrary")),
        cost_estimate=pl.CostEstimate(
            flops=6 * count * D * HALF, bytes_accessed=6 * D * HALF, transcendentals=count * HALF
        ),
        name="feed_forward",
    )(rows, weights, weights)


def row_norm(before, moments, gain, bias):
    mean = moments[0] / D
    spread = moments[1] / D - mean * mean
    return (before - mean[:, None]) * lax.rsqrt(spread + norm_eps)[:, None] * gain + bias


def shards(
    query_logits,
    value_rows,
    onward_forget_logits,
    reverse_forget_logits,
    output_gate_logits,
    onward_floor_gap,
    reverse_floor_gap,
    extra_log_decay,
    per_head_gain,
    residual,
    output_matrix,
    inner_norm_gain,
    inner_norm_bias,
    gate_matrix,
    up_matrix,
    down_matrix,
    closing_norm_gain,
    closing_norm_bias,
):
    weights = gathered_weights(gate_matrix, up_matrix, down_matrix)
    rows = query_logits.shape[0]
    query = jax.nn.silu(query_logits.astype(jnp.float32))
    values = value_rows.astype(jnp.float32)
    onward_log_decay, onward_keys = decay_factors(
        onward_forget_logits, onward_floor_gap, extra_log_decay
    )
    reverse_log_decay, reverse_keys = decay_factors(
        reverse_forget_logits, reverse_floor_gap, extra_log_decay
    )
    ahead, ahead_query, ahead_total, ahead_state = local_pass(
        query, onward_keys, values, onward_log_decay
    )
    behind, behind_query, behind_total, behind_state = local_pass(
        jnp.flip(query, axis=0),
        jnp.flip(reverse_keys, axis=0),
        jnp.flip(values, axis=0),
        jnp.flip(reverse_log_decay, axis=0),
    )
    incoming, arriving = exchanged_states((ahead_total, ahead_state), (behind_total, behind_state))
    ahead = ahead + jnp.dot(ahead_query, incoming, precision=highest_precision)
    behind = behind + jnp.dot(behind_query, arriving, precision=highest_precision)
    mixed = ahead + jnp.flip(behind, axis=0)
    normed = (
        mixed * lax.rsqrt(jnp.mean(mixed * mixed, axis=1, keepdims=True) + head_eps) * per_head_gain
    )
    gated = (normed * jax.nn.silu(output_gate_logits.astype(jnp.float32))).astype(jnp.bfloat16)
    everyone = to_all(gated, PAIR)
    mixer = jnp.einsum(
        "pthk,hkn->ptn",
        jnp.moveaxis(everyone.reshape(2, -1, rows, 128), 1, 2),
        output_matrix.reshape(-1, 128, output_matrix.shape[1]),
        preferred_element_type=jnp.float32,
    ).reshape(2 * rows, -1)
    pair_residual = to_all(residual, "yb").reshape(2 * rows, -1)
    before_middle = alpha_mix * pair_residual.astype(jnp.float32) + mixer
    moments = packed_total(
        (jnp.sum(before_middle, axis=1), jnp.sum(before_middle * before_middle, axis=1)), "tp"
    )
    middle = row_norm(before_middle, moments, inner_norm_gain, inner_norm_bias).astype(jnp.bfloat16)
    partial_value = feed_forward(to_all(middle, "tp"), weights)
    partial_value = partial_value.reshape(-1, *partial_value.shape[2:])
    feed = lax.all_to_all(partial_value, PAIR, 0, 0, tiled=True).astype(jnp.float32).sum(axis=0)
    own = lax.dynamic_slice_in_dim(middle, lax.axis_index("yb") * rows, rows, 0)
    before_final = alpha_mix * own.astype(jnp.float32) + feed
    closing = packed_total(
        (jnp.sum(before_final, axis=1), jnp.sum(before_final * before_final, axis=1)), "tp"
    )
    return row_norm(before_final, closing, closing_norm_gain, closing_norm_bias).astype(
        jnp.bfloat16
    )


def solution(mesh):
    torus = Mesh(mesh.devices.reshape(16, 2, 2, mesh.shape["tp"]), ("z", "ya", "yb", "tp"))
    in_specs = (
        P(SP, "tp"),
        P(SP, "tp"),
        P(SP, "tp"),
        P(SP, "tp"),
        P(SP, "tp"),
        P("tp"),
        P("tp"),
        P(SP, "tp"),
        P(),
        P(SP, "tp"),
        P(None, "tp"),
        P("tp"),
        P("tp"),
        P(SP, "tp"),
        P(SP, "tp"),
        P("tp", SP),
        P("tp"),
        P("tp"),
    )
    out_specs = P(SP, "tp")
    return jax.shard_map(
        shards, mesh=torus, in_specs=in_specs, out_specs=out_specs, check_vma=False
    )
```

time: 215 us -> 187 us (0.87)
  blocking collectives: 157 us -> 46.3 us
  waiting for transfers between devices: 20.4 us -> 59.5 us
  starting transfers between devices: 0.04 us -> 38.7 us
  Pallas kernels: 0 us -> 13.5 us
  matrix products: 15.4 us -> 3.1 us
  local copies, waits for them, and re-layouts: 2.97 us -> 5.71 us
    all_gather x4 -> x0, blocking collectives: 79.2 us -> none  [collected_together(): both, at, found = (lax.all_gather(jnp.concatenate(lines), axis), 0, {})]
    all_to_all x0 -> x5, waiting for transfers between devices: none -> 59.5 us  [the longest x1 16.3 us: exchanged_states(): arrived = lax.all_to_all(packed, SP, 0, 0, tiled=True)]
    all_to_all x0 -> x5, starting transfers between devices: none -> 38.6 us  [the longest x1 16.7 us: exchanged_states(): arrived = lax.all_to_all(packed, SP, 0, 0, tiled=True)]
    all_to_all x5 -> x4, blocking collectives: 78.2 us -> 46.3 us  [the longest x3 35.8 us: to_all(): lax.all_to_all(jnp.broadcast_to(x[None], (devices, *x.shape)), axes, 0, 0...]
    all_gather x1, waiting for transfers between devices: 20.3 us -> 0.01 us  [gathered_weights(): lax.all_gather(shard, 'z', axis=0, tiled=True).reshape(-1, 3, 128, HALF)]
    pallas_call x0 -> x2, Pallas kernels: none -> 13.5 us  [the longest x1 11.8 us: feed_forward(): pl.pallas_call(lambda *refs: feed_kernel(steps, *refs), grid=(2, steps),...]
    dot_general x11 -> x9, matrix products: 15.4 us -> 3.1 us  [the longest x2 1.35 us: local_pass(): jnp.einsum('ok,ov->kv', key_stop, values, precision=highest_precision)]
  transfers between devices with their start and end apart: 1 -> 6, of which waited for: 1 -> 5; matrix products, arithmetic and copies ran while one was open for 4% -> 6% of each run, Pallas kernels for 0% -> 1%
where the time goes in v1:
time: 187 us; the launch traced here: 186 us
  waiting for transfers between devices  59.5 us (32%)
  blocking collectives  46.3 us (25%)
  starting transfers between devices  38.7 us (21%)
  between operations  13.8 us (7%)
  Pallas kernels  13.5 us (7%)
  local copies, waits for them, and re-layouts  5.71 us (3%)
  other arithmetic  5.25 us (3%)
  matrix products  3.1 us (2%)
    all_to_all x3, blocking collectives, to_all(): lax.all_to_all(jnp.broadcast_to(x[None], (devices, *x.shape)), axes, 0, 0...  35.8 us
    all_to_all x1, starting transfers between devices, exchanged_states(): arrived = lax.all_to_all(packed, SP, 0, 0, tiled=True)  16.7 us
    all_to_all x1, waiting for transfers between devices, exchanged_states(): arrived = lax.all_to_all(packed, SP, 0, 0, tiled=True)  16.3 us
    all_to_all x1, waiting for transfers between devices, shards(): lax.all_to_all(partial_value, PAIR, 0, 0, tiled=True).astype(jnp.float32)  15.9 us
    all_to_all x1, waiting for transfers between devices, exchanged_states(): lax.all_to_all(before.astype(jnp.bfloat16), SP, 0, 0, tiled=True)  14.3 us
    all_to_all x2, waiting for transfers between devices, to_all(): lax.all_to_all(jnp.broadcast_to(x[None], (devices, *x.shape)), axes, 0, 0...  13 us
    all_to_all x2, starting transfers between devices, to_all(): lax.all_to_all(jnp.broadcast_to(x[None], (devices, *x.shape)), axes, 0, 0...  12.6 us
    pallas_call x1, Pallas kernels, feed_forward(): pl.pallas_call(lambda *refs: feed_kernel(steps, *refs), grid=(2, steps),...  11.8 us
  transfers between devices with their start and end apart: 6, of which 5 were waited for; matrix products, arithmetic and copies ran while one was open for 6% of the time, Pallas kernels for 1%

profile of v1, /device:TPU:1, one launch (start us, length us, event | category | flops | bytes accessed | tf_op | source)
XLA Modules:
  0.0 185.9 jit_solution(5813773270897315142)
XLA Ops:
  6.6 0.9 pad_maximum_fusion.1
  7.7 10.5 %all_to_all.47 = bf16[4,3,32,384]{3,2,1,0:T(8,128)(2,1)S(1)} all-to-all(bf16[4,3,32,384]{3,2,1,0:T(8,128)(2,1)S(1)} %pad_maximum_fusion), channel_id=1, replica_groups=mesh['z'=16,'ya'=2,'yb'=2,'tp'=8] {'ya','yb'}, dimensions={0} | all-to-all | bytes 589824 | tf_op jit(solution)/shard_map/all_to_all | solution.py:95
  18.2 0.8 copy.88
  18.9 0.9 log-plus-one_add_fusion
  19.9 0.8 rev.18
  21.3 1.1 convolution_convert_fusion.1
  23.0 0.8 pad_maximum_fusion.2
  23.8 16.7 %all-to-all-start.1 = ((bf16[64,8,128]{2,1,0:T(8,128)(2,1)}), bf16[64,8,128]{2,1,0:T(8,128)(2,1)S(1)}, u32[]{:S(2)}, u32[]{:S(2)}) async-start(bf16[64,8,128]{2,1,0:T(8,128)(2,1)} %pad_maximum_fusion.2), calls=%async_computation.1 | async-start | bytes 262144 | tf_op jit(solution)/shard_map/all_to_all | solution.py:80
  41.2 16.3 %all-to-all-done.1.refs_0_ = bf16[64,8,128]{2,1,0:T(8,128)(2,1)S(1)} async-done(((bf16[64,8,128]{2,1,0:T(8,128)(2,1)}), bf16[64,8,128]{2,1,0:T(8,128)(2,1)S(1)}, u32[]{:S(2)}, u32[]{:S(2)}) %all-to-all-start.1) | async-done | bytes 131104 | tf_op jit(solution)/shard_map/all_to_all | solution.py:80
  58.1 1.7 scan.1
  59.9 1.6 convert_element_type.46
  61.4 4.8 %all-to-all-start.2 = ((bf16[64,4,128]{2,1,0:T(4,128)(2,1)}), bf16[64,4,128]{2,1,0:T(4,128)(2,1)S(1)}, u32[]{:S(2)}, u32[]{:S(2)}) async-start(bf16[64,4,128]{2,1,0:T(4,128)(2,1)} %convert_element_type.46), calls=%async_computation.2 | async-start | bytes 131072 | tf_op jit(solution)/shard_map/all_to_all | solution.py:86
  66.7 14.3 %all-to-all-done.2 = bf16[64,4,128]{2,1,0:T(4,128)(2,1)S(1)} async-done(((bf16[64,4,128]{2,1,0:T(4,128)(2,1)}), bf16[64,4,128]{2,1,0:T(4,128)(2,1)S(1)}, u32[]{:S(2)}, u32[]{:S(2)}) %all-to-all-start.2) | async-done | bytes 65568 | tf_op jit(solution)/shard_map/all_to_all | solution.py:86
  81.7 0.9 broadcast_in_dim.29
  82.6 9.2 %all-to-all-start.3 = ((bf16[16,128,128]{2,1,0:T(8,128)(2,1)}), bf16[16,128,128]{2,1,0:T(8,128)(2,1)S(1)}, u32[]{:S(2)}, u32[]{:S(2)}) async-start(bf16[16,128,128]{2,1,0:T(8,128)(2,1)} %broadcast_in_dim.29), calls=%async_computation.3 | async-start | bytes 1048576 | tf_op jit(solution)/shard_map/all_to_all | solution.py:24
  92.0 9.4 %all-to-all-done.3 = bf16[16,128,128]{2,1,0:T(8,128)(2,1)S(1)} async-done(((bf16[16,128,128]{2,1,0:T(8,128)(2,1)}), bf16[16,128,128]{2,1,0:T(8,128)(2,1)S(1)}, u32[]{:S(2)}, u32[]{:S(2)}) %all-to-all-start.3) | async-done | bytes 524320 | tf_op jit(solution)/shard_map/all_to_all | solution.py:24
  102.1 3.4 %all-to-all-start = ((bf16[2,128,256]{1,2,0:T(8,128)(2,1)}), bf16[2,128,256]{1,2,0:T(8,128)(2,1)S(1)}, u32[]{:S(2)}, u32[]{:S(2)}) async-start(bf16[2,128,256]{1,2,0:T(8,128)(2,1)} %broadcast_in_dim.23), calls=%async_computation | async-start | bytes 262144 | tf_op jit(solution)/shard_map/all_to_all | solution.py:24
  105.5 3.5 %all-to-all-done = bf16[2,128,256]{1,2,0:T(8,128)(2,1)S(1)} async-done(((bf16[2,128,256]{1,2,0:T(8,128)(2,1)}), bf16[2,128,256]{1,2,0:T(8,128)(2,1)S(1)}, u32[]{:S(2)}, u32[]{:S(2)}) %all-to-all-start) | async-done | bytes 131104 | tf_op jit(solution)/shard_map/all_to_all | solution.py:24
  109.4 9.3 %all_to_all.48 = f32[8,1,512]{2,1,0:T(1,128)S(1)} all-to-all(f32[8,1,512]{2,1,0:T(1,128)S(1)} %broadcast_in_dim.30), channel_id=1, replica_groups=mesh['z'=16,'ya'=2,'yb'=2,'tp'=8] {'tp'}, dimensions={0} | all-to-all | bytes 32768 | tf_op jit(solution)/shard_map/all_to_all | solution.py:24
  119.1 18.8 %all_to_all.49.refs_0_ = bf16[8,256,256]{2,1,0:T(8,128)(2,1)} all-to-all(bf16[8,256,256]{2,1,0:T(8,128)(2,1)S(1)} %broadcast_in_dim.31), channel_id=1, replica_groups=mesh['z'=16,'ya'=2,'yb'=2,'tp'=8] {'tp'}, dimensions={0} | all-to-all | bytes 2097152 | tf_op jit(solution)/shard_map/all_to_all | solution.py:24
  137.8 11.8 %feed_forward.1 = bf16[2,8,128,256]{3,2,1,0:T(8,128)(2,1)} custom-call(bf16[8,256,256]{2,1,0:T(8,128)(2,1)} %all_to_all.49.refs_0_, bf16[16,3,128,384]{3,2,1,0:T(8,128)(2,1)} %bitcast.48, bf16[16,3,128,384]{3,2,1,0:T(8,128)(2,1)} %bitcast.49), custom_call_target="tpu_custom_call" | custom-call | flops 1207959552 | bytes 4718592 | tf_op jit(solution)/shard_map/feed_forward/pallas_call | solution.py:135
  149.7 4.5 %all-to-all-start.7 = ((bf16[16,128,256]{2,1,0:T(8,128)(2,1)}), bf16[16,128,256]{2,1,0:T(8,128)(2,1)S(1)}, u32[]{:S(2)}, u32[]{:S(2)}) async-start(bf16[16,128,256]{2,1,0:T(8,128)(2,1)} %bitcast.50), calls=%async_computation.7 | async-start | bytes 2097152 | tf_op jit(solution)/shard_map/all_to_all | solution.py:230
  154.1 15.9 %all-to-all-done.7 = bf16[16,128,256]{2,1,0:T(8,128)(2,1)S(1)} async-done(((bf16[16,128,256]{2,1,0:T(8,128)(2,1)}), bf16[16,128,256]{2,1,0:T(8,128)(2,1)S(1)}, u32[]{:S(2)}, u32[]{:S(2)}) %all-to-all-start.7) | async-done | bytes 1048608 | tf_op jit(solution)/shard_map/all_to_all | solution.py:230
  170.3 7.7 %all_to_all.50 = f32[8,1,256]{2,1,0:T(1,128)S(1)} all-to-all(f32[8,1,256]{2,1,0:T(1,128)S(1)} %broadcast_in_dim.32), channel_id=1, replica_groups=mesh['z'=16,'ya'=2,'yb'=2,'tp'=8] {'tp'}, dimensions={0} | all-to-all | bytes 16384 | tf_op jit(solution)/shard_map/all_to_all | solution.py:24
  (76 shorter events, 6.4 us)
Async XLA Ops:
  6.5 102.5 %copy-start = (bf16[1024,256]{1,0:T(8,128)(2,1)S(1)}, bf16[1024,256]{1,0:T(8,128)(2,1)}, u32[]{:S(2)}) copy-start(bf16[1024,256]{1,0:T(8,128)(2,1)} %param.28) | copy-start | bytes 1572868
  6.5 34.0 %copy-start.6 = (bf16[128,128]{1,0:T(8,128)(2,1)S(1)}, bf16[128,128]{1,0:T(8,128)(2,1)}, u32[]{:S(2)}) copy-start(bf16[128,128]{1,0:T(8,128)(2,1)} %param.20) | copy-start | bytes 98308
  6.5 34.1 %copy-start.11 = (f32[128]{0:T(128)S(1)}, f32[128]{0:T(128)}, u32[]{:S(2)}) copy-start(f32[128]{0:T(128)} %param.23) | copy-start | bytes 1540
  6.5 59.7 %copy-start.2 = (bf16[128,128]{1,0:T(8,128)(2,1)S(1)}, bf16[128,128]{1,0:T(8,128)(2,1)}, u32[]{:S(2)}) copy-start(bf16[128,128]{1,0:T(8,128)(2,1)} %param.19) | copy-start | bytes 98308
  6.5 34.0 %copy-start.4 = (bf16[128,128]{1,0:T(8,128)(2,1)S(1)}, bf16[128,128]{1,0:T(8,128)(2,1)}, u32[]{:S(2)}) copy-start(bf16[128,128]{1,0:T(8,128)(2,1)} %param.18) | copy-start | bytes 98308
  6.5 75.0 %copy-start.5 = (bf16[128,128]{1,0:T(8,128)(2,1)S(1)}, bf16[128,128]{1,0:T(8,128)(2,1)}, u32[]{:S(2)}) copy-start(bf16[128,128]{1,0:T(8,128)(2,1)} %param.22) | copy-start | bytes 98308
  6.6 75.0 %copy-start.12 = (f32[128]{0:T(128)S(1)}, f32[128]{0:T(128)}, u32[]{:S(2)}) copy-start(f32[128]{0:T(128)} %param.26) | copy-start | bytes 1540
  6.6 131.3 %all-gather.2.cloned.1.call-start = ((), (), s32[]{:S(2)}) async-start(), calls=%async_computation.9 | async-start | bytes 5013504 | tf_op jit(solution)/shard_map/all_gather | solution.py:97
  7.5 84.3 %copy-start.3 = (bf16[128,256]{1,0:T(8,128)(2,1)S(1)}, bf16[128,256]{1,0:T(8,128)(2,1)}, u32[]{:S(2)}) copy-start(bf16[128,256]{1,0:T(8,128)(2,1)} %param.27) | copy-start | bytes 196612
  20.8 97.9 %copy-start.7 = (f32[256]{0:T(256)S(1)}, f32[256]{0:T(256)}, u32[]{:S(2)}) copy-start(f32[256]{0:T(256)} %param.30) | copy-start | bytes 3076
  20.8 97.9 %copy-start.8 = (f32[256]{0:T(256)S(1)}, f32[256]{0:T(256)}, u32[]{:S(2)}) copy-start(f32[256]{0:T(256)} %param.29) | copy-start | bytes 3076
  23.8 33.7 %all-to-all-start.1 = ((bf16[64,8,128]{2,1,0:T(8,128)(2,1)}), bf16[64,8,128]{2,1,0:T(8,128)(2,1)S(1)}, u32[]{:S(2)}, u32[]{:S(2)}) async-start(bf16[64,8,128]{2,1,0:T(8,128)(2,1)} %pad_maximum_fusion.2), calls=%async_computation.1 | async-start | bytes 262144 | tf_op jit(solution)/shard_map/all_to_all | solution.py:80
  57.5 0.7 copy-start.1
  61.4 19.6 %all-to-all-start.2 = ((bf16[64,4,128]{2,1,0:T(4,128)(2,1)}), bf16[64,4,128]{2,1,0:T(4,128)(2,1)S(1)}, u32[]{:S(2)}, u32[]{:S(2)}) async-start(bf16[64,4,128]{2,1,0:T(4,128)(2,1)} %convert_element_type.46), calls=%async_computation.2 | async-start | bytes 131072 | tf_op jit(solution)/shard_map/all_to_all | solution.py:86
  82.6 18.8 %all-to-all-start.3 = ((bf16[16,128,128]{2,1,0:T(8,128)(2,1)}), bf16[16,128,128]{2,1,0:T(8,128)(2,1)S(1)}, u32[]{:S(2)}, u32[]{:S(2)}) async-start(bf16[16,128,128]{2,1,0:T(8,128)(2,1)} %broadcast_in_dim.29), calls=%async_computation.3 | async-start | bytes 1048576 | tf_op jit(solution)/shard_map/all_to_all | solution.py:24
  102.1 7.0 %all-to-all-start = ((bf16[2,128,256]{1,2,0:T(8,128)(2,1)}), bf16[2,128,256]{1,2,0:T(8,128)(2,1)S(1)}, u32[]{:S(2)}, u32[]{:S(2)}) async-start(bf16[2,128,256]{1,2,0:T(8,128)(2,1)} %broadcast_in_dim.23), calls=%async_computation | async-start | bytes 262144 | tf_op jit(solution)/shard_map/all_to_all | solution.py:24
  137.8 40.3 %copy-start.9 = (f32[256]{0:T(256)S(1)}, f32[256]{0:T(256)}, u32[]{:S(2)}) copy-start(f32[256]{0:T(256)} %param.35) | copy-start | bytes 3076
  137.8 40.3 %copy-start.10 = (f32[256]{0:T(256)S(1)}, f32[256]{0:T(256)}, u32[]{:S(2)}) copy-start(f32[256]{0:T(256)} %param.34) | copy-start | bytes 3076
  149.7 20.3 %all-to-all-start.7 = ((bf16[16,128,256]{2,1,0:T(8,128)(2,1)}), bf16[16,128,256]{2,1,0:T(8,128)(2,1)S(1)}, u32[]{:S(2)}, u32[]{:S(2)}) async-start(bf16[16,128,256]{2,1,0:T(8,128)(2,1)} %bitcast.50), calls=%async_computation.7 | async-start | bytes 2097152 | tf_op jit(solution)/shard_map/all_to_all | solution.py:230
Sparse Core Ops, SparseCore 0:
  19.1 83.0 all-gather.1

commit v2 on v1

v2 whole, which is shorter than its diff:
```python
import math

import jax
import jax.numpy as jnp
from jax import lax
from jax.experimental import pallas as pl
from jax.experimental.pallas import tpu as pltpu
from jax.sharding import Mesh
from jax.sharding import PartitionSpec as P

D = 2048
SP = ("z", "ya", "yb")
TP = ("x", "c")
PAIR = ("yb", "x", "c")
HALF = 384

highest_precision = lax.Precision.HIGHEST
alpha_mix = 2.0**0.25
norm_eps = 1e-05
head_eps = 1e-06


def to_all(x, axes):
    devices = lax.axis_size(axes)
    return lax.all_to_all(jnp.broadcast_to(x[None], (devices, *x.shape)), axes, 0, 0, tiled=True)


def packed_total(arrays, axis):
    vector, at, done = (jnp.concatenate([a.reshape(-1) for a in arrays]), 0, [])
    total = to_all(vector, axis).sum(axis=0)
    for a in arrays:
        done.append(total[at : at + a.size].reshape(a.shape))
        at += a.size
    return tuple(done)


def local_kernel(
    query_ref,
    value_ref,
    onward_ref,
    reverse_ref,
    onward_gap_ref,
    reverse_gap_ref,
    extra_ref,
    inner_ref,
    queries_ref,
    states_ref,
    totals_ref,
):
    def dot(a, b, dims=((1,), (0,))):
        return lax.dot_general(
            a, b, (dims, ((), ())), precision=highest_precision, preferred_element_type=jnp.float32
        )

    rows = query_ref.shape[0]
    logits = query_ref[...].astype(jnp.float32)
    query = logits / (1.0 + jnp.exp(-logits))
    values = value_ref[...].astype(jnp.float32)
    at = lax.broadcasted_iota(jnp.int32, (rows, rows), 0)
    source = lax.broadcasted_iota(jnp.int32, (rows, rows), 1)
    inner = jnp.zeros_like(query)
    for side, (forget_ref, gap_ref, seen, last) in enumerate(
        ((onward_ref, onward_gap_ref, at >= source, rows - 1), (reverse_ref, reverse_gap_ref, at <= source, 0))
    ):
        seen = seen.astype(jnp.float32)
        keys = gap_ref[...] / (1.0 + jnp.exp(forget_ref[...].astype(jnp.float32)))
        running = dot(seen, jnp.log1p(-keys) + extra_ref[...])
        total = running[last : last + 1]
        decayed_query = query * jnp.exp(running)
        scores = dot(decayed_query, keys * jnp.exp(-running), ((1,), (1,))) * seen
        inner = inner + dot(scores, values)
        queries_ref[:, 128 * side : 128 * side + 128] = decayed_query
        states_ref[side] = dot(keys * jnp.exp(total - running), values, ((0,), (0,)))
        totals_ref[side : side + 1] = total
    inner_ref[...] = inner


def local_pass(query, values, onward, reverse, onward_gap, reverse_gap, extra):
    rows, width = query.shape
    shapes = ((rows, width), (rows, 2 * width), (2, width, width), (2, width))
    return pl.pallas_call(
        local_kernel,
        out_shape=[jax.ShapeDtypeStruct(s, jnp.float32) for s in shapes],
        name="local",
    )(query, values, onward, reverse, onward_gap[None], reverse_gap[None], extra)


def scan_kernel(chunks, local_ref, before_ref):
    local = local_ref[...].astype(jnp.float32)
    decay = jnp.exp(local[:, 4:8])
    state = local[:, 0:4]
    ahead = [None] * chunks
    run = jnp.zeros((2, 128), jnp.float32)
    for c in range(chunks):
        ahead[c] = run
        run = decay[c, 0:2] * run + state[c, 0:2]
    run = jnp.zeros((2, 128), jnp.float32)
    for c in reversed(range(chunks)):
        before_ref[c] = jnp.concatenate([ahead[c], run], axis=0).astype(jnp.bfloat16)
        run = decay[c, 2:4] * run + state[c, 2:4]


def exchanged_states(states, totals):
    chunks = lax.axis_size(SP)
    decays = jnp.broadcast_to(totals.reshape(4, chunks, 1), (4, chunks, 128))
    packed = jnp.concatenate([states.reshape(4, chunks, 128), decays])
    packed = jnp.moveaxis(packed.astype(jnp.bfloat16), 1, 0)
    arrived = lax.all_to_all(packed, SP, 0, 0, tiled=True)
    before = pl.pallas_call(
        lambda *refs: scan_kernel(chunks, *refs),
        out_shape=jax.ShapeDtypeStruct((chunks, 4, 128), jnp.bfloat16),
        name="scan",
    )(arrived)
    back = lax.all_to_all(before, SP, 0, 0, tiled=True).astype(jnp.float32)
    return jnp.moveaxis(back, 1, 0).reshape(4 * chunks, 128)


def gathered_weights(gate, up, down):
    both = jnp.stack([gate, up, down.T])
    first = both[:, :, :HALF]
    second = jnp.pad(both[:, :, HALF:], ((0, 0), (0, 0), (0, 2 * HALF - both.shape[2])))
    halves = jnp.stack([first, second, first, second])
    arrived = lax.all_to_all(halves, ("ya", "yb"), 0, 0, tiled=True)
    shard = jnp.moveaxis(arrived, 0, 1).reshape(3 * 128, HALF)
    return lax.all_gather(shard, "z", axis=0, tiled=True).reshape(-1, 3, 128, HALF)


def exact_terms(x):
    terms = []
    for _ in range(3):
        term = lax.reduce_precision(x, 8, 7)
        terms.append(term.astype(jnp.bfloat16))
        x = x - term
    return terms


def whole_columns(output_matrix, residual, gain, bias):
    rows = residual.shape[0]
    other = lax.ppermute(residual, "yb", ((0, 1), (1, 0)))
    first = lax.axis_index("yb") == 0
    vectors = jnp.stack(exact_terms(gain) + exact_terms(bias))
    block = jnp.concatenate(
        [
            output_matrix,
            jnp.where(first, residual, other),
            jnp.where(first, other, residual),
            jnp.pad(vectors, ((0, 10), (0, 0))),
        ]
    )
    both = jnp.stack([block, lax.ppermute(block, "c", ((0, 1), (1, 0)))])
    count = lax.axis_size("x")
    return [both] + [
        lax.ppermute(both, "x", [(i, (i + k) % count) for i in range(count)])
        for k in range(1, count)
    ]


def middle_kernel(place_ref, gated_ref, *refs):
    block_refs, (out_ref, whole_ref, before_ref) = refs[:4], refs[4:]
    heads, rows = 8, gated_ref.shape[2]
    count = 2 * rows
    for core in range(2):
        for pair in range(2):
            for x in range(4):
                head = 2 * x + core
                whole_ref[pair * rows : (pair + 1) * rows, 128 * head : 128 * head + 128] = (
                    gated_ref[core, 4 * pair + x]
                )
    whole = whole_ref[...]
    inner = whole.shape[1]
    total = jnp.zeros((count, 1), jnp.float32)
    for b in range(heads):
        block_ref = block_refs[b // 2]
        mixer = jnp.dot(whole, block_ref[b % 2, :inner], preferred_element_type=jnp.float32)
        residual = block_ref[b % 2, inner : inner + count].astype(jnp.float32)
        before = alpha_mix * residual + mixer
        before_ref[b] = before
        total = total + jnp.sum(before, axis=1, keepdims=True)
    mean = total / D
    spread = jnp.zeros((count, 1), jnp.float32)
    for b in range(heads):
        centre = before_ref[b] - mean
        spread = spread + jnp.sum(centre * centre, axis=1, keepdims=True)
    scale = lax.rsqrt(spread / D + norm_eps)
    for b in range(heads):
        vectors = block_refs[b // 2][b % 2, inner + count : inner + count + 16].astype(jnp.float32)
        gain = vectors[0:1] + vectors[1:2] + vectors[2:3]
        bias = vectors[3:4] + vectors[4:5] + vectors[5:6]
        normed = (before_ref[b] - mean) * scale * gain + bias
        out_ref[place_ref[b]] = normed.astype(jnp.bfloat16)


def middle_rows(gated, blocks):
    rows, width = gated.shape[2], blocks[0].shape[2]
    x, core = lax.axis_index("x"), lax.axis_index("c")
    place = jnp.stack([2 * ((x - b // 2 + 4) % 4) + (core + b) % 2 for b in range(8)])
    vmem = pl.BlockSpec(memory_space=pltpu.VMEM)
    return pl.pallas_call(
        middle_kernel,
        in_specs=[pl.BlockSpec(memory_space=pltpu.SMEM)] + [vmem] * 5,
        out_specs=vmem,
        out_shape=jax.ShapeDtypeStruct((8, 2 * rows, width), jnp.bfloat16),
        scratch_shapes=[
            pltpu.VMEM((2 * rows, 8 * 128), jnp.bfloat16),
            pltpu.VMEM((8, 2 * rows, width), jnp.float32),
        ],
        name="middle",
    )(place.astype(jnp.int32), gated, *blocks)


def feed_kernel(steps, rows_ref, enter_ref, leave_ref, out_ref, gate_ref, up_ref, hidden_ref):
    phase, step = pl.program_id(0), pl.program_id(1)

    @pl.when(jnp.logical_and(phase == 0, step == 0))
    def _():
        gate_ref[...] = jnp.zeros_like(gate_ref)
        up_ref[...] = jnp.zeros_like(up_ref)

    @pl.when(phase == 0)
    def _():
        for to_ref, kind in ((gate_ref, 0), (up_ref, 1)):
            product = 0.0
            for b in range(rows_ref.shape[0]):
                wide = jnp.concatenate([enter_ref[2 * b, kind], enter_ref[2 * b + 1, kind]], axis=0)
                product += jnp.dot(rows_ref[b], wide, preferred_element_type=jnp.float32)
            to_ref[...] += product

    @pl.when(jnp.logical_and(phase == 0, step == steps - 1))
    def _():
        gate = gate_ref[...]
        hidden_ref[...] = (gate / (1.0 + jnp.exp(-gate)) * up_ref[...]).astype(jnp.bfloat16)

    @pl.when(phase == 1)
    def _():
        for b in range(out_ref.shape[1]):
            down = jnp.concatenate([leave_ref[2 * b, 0], leave_ref[2 * b + 1, 0]], axis=0)
            product = lax.dot_general(
                hidden_ref[...],
                down,
                (((1,), (1,)), ((), ())),
                preferred_element_type=jnp.float32,
            ).astype(jnp.bfloat16)
            for pair in range(2):
                rows = out_ref.shape[2]
                out_ref[pair, b] = product[pair * rows : (pair + 1) * rows]


def feed_forward(rows, weights):
    blocks, count, width = rows.shape
    each = 2
    steps = blocks // each
    return pl.pallas_call(
        lambda *refs: feed_kernel(steps, *refs),
        grid=(2, steps),
        in_specs=[
            pl.BlockSpec((each, count, width), lambda p, s: (jnp.where(p == 0, s, steps - 1), 0, 0)),
            pl.BlockSpec(
                (2 * each, 2, 128, HALF), lambda p, s: (jnp.where(p == 0, s, steps - 1), 0, 0, 0)
            ),
            pl.BlockSpec((2 * each, 1, 128, HALF), lambda p, s: (jnp.where(p == 0, 0, s), 2, 0, 0)),
        ],
        out_specs=pl.BlockSpec(
            (2, each, count // 2, width), lambda p, s: (0, jnp.where(p == 0, 0, s), 0, 0)
        ),
        out_shape=jax.ShapeDtypeStruct((2, blocks, count // 2, width), jnp.bfloat16),
        scratch_shapes=[
            pltpu.VMEM((count, HALF), jnp.float32),
            pltpu.VMEM((count, HALF), jnp.float32),
            pltpu.VMEM((count, HALF), jnp.bfloat16),
        ],
        compiler_params=pltpu.CompilerParams(dimension_semantics=("arbitrary", "arbitrary")),
        cost_estimate=pl.CostEstimate(
            flops=6 * count * D * HALF, bytes_accessed=6 * D * HALF, transcendentals=count * HALF
        ),
        name="feed_forward",
    )(rows, weights, weights)


def row_norm(before, moments, gain, bias):
    mean = moments[0] / D
    spread = moments[1] / D - mean * mean
    return (before - mean[:, None]) * lax.rsqrt(spread + norm_eps)[:, None] * gain + bias


def shards(
    query_logits,
    value_rows,
    onward_forget_logits,
    reverse_forget_logits,
    output_gate_logits,
    onward_floor_gap,
    reverse_floor_gap,
    extra_log_decay,
    per_head_gain,
    residual,
    output_matrix,
    inner_norm_gain,
    inner_norm_bias,
    gate_matrix,
    up_matrix,
    down_matrix,
    closing_norm_gain,
    closing_norm_bias,
):
    weights = gathered_weights(gate_matrix, up_matrix, down_matrix)
    blocks = whole_columns(output_matrix, residual, inner_norm_gain, inner_norm_bias)
    rows = query_logits.shape[0]
    inner, queries, states, totals = local_pass(
        query_logits,
        value_rows,
        onward_forget_logits,
        reverse_forget_logits,
        onward_floor_gap,
        reverse_floor_gap,
        extra_log_decay,
    )
    mixed = inner + jnp.dot(queries, exchanged_states(states, totals), precision=highest_precision)
    normed = (
        mixed * lax.rsqrt(jnp.mean(mixed * mixed, axis=1, keepdims=True) + head_eps) * per_head_gain
    )
    gated = (normed * jax.nn.silu(output_gate_logits.astype(jnp.float32))).astype(jnp.bfloat16)
    everyone = lax.all_gather(to_all(gated, ("yb", "x")), "c")
    middle = middle_rows(everyone, blocks)
    partial_value = feed_forward(middle, weights)
    partial_value = partial_value.reshape(-1, *partial_value.shape[2:])
    feed = lax.all_to_all(partial_value, PAIR, 0, 0, tiled=True).astype(jnp.float32).sum(axis=0)
    own = lax.dynamic_slice(
        middle,
        (lax.axis_index(TP), lax.axis_index("yb") * rows, 0),
        (1, rows, middle.shape[2]),
    )[0]
    before_final = alpha_mix * own.astype(jnp.float32) + feed
    closing = packed_total(
        (jnp.sum(before_final, axis=1), jnp.sum(before_final * before_final, axis=1)), TP
    )
    return row_norm(before_final, closing, closing_norm_gain, closing_norm_bias).astype(
        jnp.bfloat16
    )


def solution(mesh):
    torus = Mesh(mesh.devices.reshape(16, 2, 2, 4, 2), ("z", "ya", "yb", "x", "c"))
    in_specs = (
        P(SP, TP),
        P(SP, TP),
        P(SP, TP),
        P(SP, TP),
        P(SP, TP),
        P(TP),
        P(TP),
        P(SP, TP),
        P(),
        P(SP, TP),
        P(None, TP),
        P(TP),
        P(TP),
        P(SP, TP),
        P(SP, TP),
        P(TP, SP),
        P(TP),
        P(TP),
    )
    out_specs = P(SP, TP)
    return jax.shard_map(
        shards, mesh=torus, in_specs=in_specs, out_specs=out_specs, check_vma=False
    )
```

time: 187 us -> 177 us (0.947)
  waiting for transfers between devices: 59.5 us -> 45.7 us
  Pallas kernels: 13.5 us -> 18 us
  starting transfers between devices: 38.7 us -> 43.1 us
  blocking collectives: 46.3 us -> 43.1 us
  matrix products: 3.1 us -> 0.28 us
    all_to_all x3 -> x1, blocking collectives: 35.8 us -> 7.76 us  [to_all(): lax.all_to_all(jnp.broadcast_to(x[None], (devices, *x.shape)), axes, 0, 0...]
    all_to_all x0 -> x1, blocking collectives: none -> 21.4 us  [exchanged_states(): back = lax.all_to_all(before, SP, 0, 0, tiled=True).astype(jnp.float32)]
    ppermute x0 -> x5, starting transfers between devices: none -> 21.3 us  [the longest x3 10.5 us: whole_columns(): lax.ppermute(both, 'x', [(i, (i + k) % count) for i in range(count)])]
    all_to_all x1 -> x0, waiting for transfers between devices: 14.3 us -> none  [exchanged_states(): lax.all_to_all(before.astype(jnp.bfloat16), SP, 0, 0, tiled=True)]
    all_to_all x2 -> x1, starting transfers between devices: 12.6 us -> 3.41 us  [to_all(): lax.all_to_all(jnp.broadcast_to(x[None], (devices, *x.shape)), axes, 0, 0...]
    all_to_all x1, waiting for transfers between devices: 16.3 us -> 7.76 us  [exchanged_states(): arrived = lax.all_to_all(packed, SP, 0, 0, tiled=True)]
    pallas_call x0 -> x2, Pallas kernels: none -> 8.55 us  [the longest x1 5.56 us: middle_rows(): pl.pallas_call(middle_kernel, in_specs=[pl.BlockSpec(memory_space=pltpu.S...]
    all_to_all x2 -> x1, waiting for transfers between devices: 13 us -> 19.5 us  [to_all(): lax.all_to_all(jnp.broadcast_to(x[None], (devices, *x.shape)), axes, 0, 0...]
  transfers between devices with their start and end apart: 6 -> 9, of which waited for: 5 -> 4; matrix products, arithmetic and copies ran while one was open for 6% -> 3% of each run, Pallas kernels for 1% -> 6%
where the time goes in v2:
time: 177 us; the launch traced here: 176 us
  waiting for transfers between devices  45.7 us (26%)
  starting transfers between devices  43.1 us (24%)
  blocking collectives  43.1 us (24%)
  Pallas kernels  18 us (10%)
  between operations  13.9 us (8%)
  other arithmetic  6.36 us (4%)
  local copies, waits for them, and re-layouts  5.2 us (3%)
    all_to_all x1, blocking collectives, exchanged_states(): back = lax.all_to_all(before, SP, 0, 0, tiled=True).astype(jnp.float32)  21.4 us
    all_to_all x1, waiting for transfers between devices, to_all(): lax.all_to_all(jnp.broadcast_to(x[None], (devices, *x.shape)), axes, 0, 0...  19.5 us
    all_to_all x1, waiting for transfers between devices, shards(): lax.all_to_all(partial_value, PAIR, 0, 0, tiled=True).astype(jnp.float32)  15.8 us
    all_to_all x1, starting transfers between devices, exchanged_states(): arrived = lax.all_to_all(packed, SP, 0, 0, tiled=True)  13.1 us
    all_to_all x1, blocking collectives, gathered_weights(): arrived = lax.all_to_all(halves, ('ya', 'yb'), 0, 0, tiled=True)  10.6 us
    ppermute x3, starting transfers between devices, whole_columns(): lax.ppermute(both, 'x', [(i, (i + k) % count) for i in range(count)])  10.5 us
    ppermute x1, starting transfers between devices, whole_columns(): both = jnp.stack([block, lax.ppermute(block, 'c', ((0, 1), (1, 0)))])  8.6 us
    all_to_all x1, blocking collectives, to_all(): lax.all_to_all(jnp.broadcast_to(x[None], (devices, *x.shape)), axes, 0, 0...  7.76 us
  transfers between devices with their start and end apart: 9, of which 4 were waited for; matrix products, arithmetic and copies ran while one was open for 3% of the time, Pallas kernels for 6%

profile of v2, /device:TPU:1, one launch (start us, length us, event | category | flops | bytes accessed | tf_op | source)
XLA Modules:
  0.0 175.6 jit_solution(10033701282308186767)
XLA Ops:
  7.6 10.6 %all_to_all.31 = bf16[4,3,32,384]{3,2,1,0:T(8,128)(2,1)S(1)} all-to-all(bf16[4,3,32,384]{3,2,1,0:T(8,128)(2,1)S(1)} %pad_maximum_fusion.1), channel_id=1, replica_groups=mesh['z'=16,'ya'=2,'yb'=2,'x'=4,'c'=2] {'ya','yb'}, dimensions={0} | all-to-all | bytes 589824 | tf_op jit(solution)/shard_map/all_to_all | solution.py:123
  19.0 2.2 %collective-permute-start = (bf16[128,256]{1,0:T(8,128)(2,1)S(1)}, bf16[128,256]{1,0:T(8,128)(2,1)S(1)}, u32[]{:S(2)}, u32[]{:S(2)}) collective-permute-start(bf16[128,256]{1,0:T(8,128)(2,1)S(1)} %copy-done.6), channel_id=1, source_target_pairs={{0,8},{8,0},{1,9},{9,1},{2,10},{10,2},{3,11},{11,3},{4,12},{12,4},... | collective-permute-start | bytes 196616 | tf_op jit(solution)/shard_map/ppermute | solution.py:139
  21.3 2.6 %collective-permute-done = bf16[128,256]{1,0:T(8,128)(2,1)S(1)} collective-permute-done((bf16[128,256]{1,0:T(8,128)(2,1)S(1)}, bf16[128,256]{1,0:T(8,128)(2,1)S(1)}, u32[]{:S(2)}, u32[]{:S(2)}) %collective-permute-start) | collective-permute-done | bytes 65568 | tf_op jit(solution)/shard_map/ppermute | solution.py:139
  24.1 8.6 %collective-permute-start.1 = (bf16[1296,256]{1,0:T(8,128)(2,1)S(1)}, bf16[1296,256]{1,0:T(8,128)(2,1)S(1)}, u32[]{:S(2)}, u32[]{:S(2)}) collective-permute-start(bf16[1296,256]{1,0:T(8,128)(2,1)S(1)} %fusion.1), channel_id=1, source_target_pairs={{0,1},{1,0},{2,3},{3,2},{4,5},{5,4},{6,7},{7,6},{8,9},{9,8},{10,11... | collective-permute-start | bytes 1990664 | tf_op jit(solution)/shard_map/ppermute | solution.py:150
  33.4 3.0 %local.1 = (f32[128,128]{1,0:T(8,128)}, f32[128,256]{1,0:T(8,128)}, f32[2,128,128]{2,1,0:T(8,128)}, f32[2,128]{1,0:T(2,128)}) custom-call(bf16[128,128]{1,0:T(8,128)(2,1)} %query_ref.1, bf16[128,128]{1,0:T(8,128)(2,1)} %value_ref.1, bf16[128,128]{1,0:T(8,128)(2,1)} %onward_ref.1, bf16[128,128]{1,0:T(8,128)(2,1)} %reverse_ref.1, f32[1,128]{1,0:T(1,128)} %bitcast.55, ...), custom_call_target="tpu_custom_call" | custom-call | tf_op jit(solution)/shard_map/local/pallas_call | solution.py:81
  36.4 0.9 convert.8
  39.2 13.1 %all-to-all-start = ((bf16[64,8,128]{2,1,0:T(8,128)(2,1)}), bf16[64,8,128]{2,1,0:T(8,128)(2,1)S(1)}, u32[]{:S(2)}, u32[]{:S(2)}) async-start(bf16[64,8,128]{2,1,0:T(8,128)(2,1)} %maximum_bitcast_fusion), calls=%async_computation | async-start | bytes 262144 | tf_op jit(solution)/shard_map/all_to_all | solution.py:108
  52.6 3.1 %collective-permute-start.2 = (bf16[2,1296,256]{2,1,0:T(8,128)(2,1)S(1)}, bf16[2,1296,256]{2,1,0:T(8,128)(2,1)S(1)}, u32[]{:S(2)}, u32[]{:S(2)}) collective-permute-start(bf16[2,1296,256]{2,1,0:T(8,128)(2,1)S(1)} %pad_maximum_fusion.refs_0_), channel_id=1, source_target_pairs={{0,2},{2,4},{4,6},{6,0},{1,3},{3,5},{5,7},{7,1},{8,10},{10,12},{12... | collective-permute-start | bytes 3981320 | tf_op jit(solution)/shard_map/ppermute | solution.py:153
  55.7 4.4 %collective-permute-start.3 = (bf16[2,1296,256]{2,1,0:T(8,128)(2,1)S(1)}, bf16[2,1296,256]{2,1,0:T(8,128)(2,1)}, u32[]{:S(2)}, u32[]{:S(2)}) collective-permute-start(bf16[2,1296,256]{2,1,0:T(8,128)(2,1)S(1)} %pad_maximum_fusion.refs_0_), channel_id=1, source_target_pairs={{0,4},{2,6},{4,0},{6,2},{1,5},{3,7},{5,1},{7,3},{8,12},{10,14},{12... | collective-permute-start | bytes 3981320 | tf_op jit(solution)/shard_map/ppermute | solution.py:153
  60.1 3.1 %collective-permute-start.4 = (bf16[2,1296,256]{2,1,0:T(8,128)(2,1)S(1)}, bf16[2,1296,256]{2,1,0:T(8,128)(2,1)}, u32[]{:S(2)}, u32[]{:S(2)}) collective-permute-start(bf16[2,1296,256]{2,1,0:T(8,128)(2,1)S(1)} %pad_maximum_fusion.refs_0_), channel_id=1, source_target_pairs={{0,6},{2,0},{4,2},{6,4},{1,7},{3,1},{5,3},{7,5},{8,14},{10,8},{12,... | collective-permute-start | bytes 3981320 | tf_op jit(solution)/shard_map/ppermute | solution.py:153
  63.1 7.8 %all-to-all-done.refs_0_ = bf16[64,8,128]{2,1,0:T(8,128)(2,1)S(1)} async-done(((bf16[64,8,128]{2,1,0:T(8,128)(2,1)}), bf16[64,8,128]{2,1,0:T(8,128)(2,1)S(1)}, u32[]{:S(2)}, u32[]{:S(2)}) %all-to-all-start) | async-done | bytes 131104 | tf_op jit(solution)/shard_map/all_to_all | solution.py:108
  71.6 1.7 scan.1
  73.3 21.4 %all_to_all.32 = bf16[64,4,128]{2,1,0:T(4,128)(2,1)S(1)} all-to-all(bf16[64,4,128]{2,1,0:T(4,128)(2,1)} %scan.1), channel_id=1, replica_groups=mesh['z'=16,'ya'=2,'yb'=2,'x'=4,'c'=2] {'z','ya','yb'}, dimensions={0} | all-to-all | bytes 131072 | tf_op jit(solution)/shard_map/all_to_all | solution.py:114
  95.9 3.4 %all-to-all-start.2 = ((bf16[8,128,128]{2,1,0:T(8,128)(2,1)}), bf16[8,128,128]{2,1,0:T(8,128)(2,1)S(1)}, u32[]{:S(2)}, u32[]{:S(2)}) async-start(bf16[8,128,128]{2,1,0:T(8,128)(2,1)} %broadcast_in_dim.16), calls=%async_computation.2 | async-start | bytes 524288 | tf_op jit(solution)/shard_map/all_to_all | solution.py:25
  100.1 19.5 %all-to-all-done.2 = bf16[8,128,128]{2,1,0:T(8,128)(2,1)S(1)} async-done(((bf16[8,128,128]{2,1,0:T(8,128)(2,1)}), bf16[8,128,128]{2,1,0:T(8,128)(2,1)S(1)}, u32[]{:S(2)}, u32[]{:S(2)}) %all-to-all-start.2) | async-done | bytes 262176 | tf_op jit(solution)/shard_map/all_to_all | solution.py:25
  119.7 3.3 %all-gather = bf16[16,128,128]{2,1,0:T(8,128)(2,1)} all-gather(bf16[8,128,128]{2,1,0:T(8,128)(2,1)S(1)} %all-to-all-done.2), channel_id=2, replica_groups=mesh['z'=16,'ya'=2,'yb'=2,'x'=4,'c'=2] {'c'}, dimensions={0}, use_global_device_ids=true | all-gather | bytes 786432 | tf_op jit(solution)/shard_map/all_gather | solution.py:322
  123.0 1.1 copy-done.2
  124.0 5.6 %middle.1.refs_0_ = bf16[8,256,256]{2,1,0:T(8,128)(2,1)} custom-call(s32[8]{0:T(128)} %stack.88.place_ref, bf16[2,8,128,128]{3,2,1,0:T(8,128)(2,1)} %bitcast.46, bf16[2,1296,256]{2,1,0:T(8,128)(2,1)} %copy-done, bf16[2,1296,256]{2,1,0:T(8,128)(2,1)} %copy-done.2, bf16[2,1296,256]{2,1,0:T(8,128)(2,1)} %collective-permute-done.3.refs_2_, ...), custom_call_target="tpu_custom_call" | custom-call | tf_op jit(solution)/shard_map/middle/pallas_call | solution.py:198
  129.6 7.7 %feed_forward.1 = bf16[2,8,128,256]{3,2,1,0:T(8,128)(2,1)} custom-call(bf16[8,256,256]{2,1,0:T(8,128)(2,1)} %middle.1.refs_0_, bf16[16,3,128,384]{3,2,1,0:T(8,128)(2,1)} %bitcast.43, bf16[16,3,128,384]{3,2,1,0:T(8,128)(2,1)} %bitcast.44), custom_call_target="tpu_custom_call" | custom-call | flops 1207959552 | bytes 4718592 | tf_op jit(solution)/shard_map/feed_forward/pallas_call | solution.py:252
  137.3 5.2 %all-to-all-start.4 = ((bf16[16,128,256]{2,1,0:T(8,128)(2,1)}), bf16[16,128,256]{2,1,0:T(8,128)(2,1)S(1)}, u32[]{:S(2)}, u32[]{:S(2)}) async-start(bf16[16,128,256]{2,1,0:T(8,128)(2,1)} %bitcast.45), calls=%async_computation.4 | async-start | bytes 2097152 | tf_op jit(solution)/shard_map/all_to_all | solution.py:326
  142.5 15.8 %all-to-all-done.4 = bf16[16,128,256]{2,1,0:T(8,128)(2,1)S(1)} async-done(((bf16[16,128,256]{2,1,0:T(8,128)(2,1)}), bf16[16,128,256]{2,1,0:T(8,128)(2,1)S(1)}, u32[]{:S(2)}, u32[]{:S(2)}) %all-to-all-start.4) | async-done | bytes 1048608 | tf_op jit(solution)/shard_map/all_to_all | solution.py:326
  158.4 1.0 fusion.7
  159.4 7.8 %all_to_all.33 = f32[8,1,256]{2,1,0:T(1,128)S(1)} all-to-all(f32[8,1,256]{2,1,0:T(1,128)S(1)} %broadcast_in_dim.17), channel_id=1, replica_groups=mesh['z'=16,'ya'=2,'yb'=2,'x'=4,'c'=2] {'x','c'}, dimensions={0} | all-to-all | bytes 16384 | tf_op jit(solution)/shard_map/all_to_all | solution.py:25
  167.2 1.6 add_convert_fusion
  (70 shorter events, 7.3 us)
Async XLA Ops:
  6.5 123.1 %all-gather.3.cloned.1.call-start = ((), (), s32[]{:S(2)}) async-start(), calls=%async_computation.6 | async-start | bytes 5013504 | tf_op jit(solution)/shard_map/all_gather | solution.py:125
  6.5 12.4 %copy-start.6 = (bf16[128,256]{1,0:T(8,128)(2,1)S(1)}, bf16[128,256]{1,0:T(8,128)(2,1)}, u32[]{:S(2)}) copy-start(bf16[128,256]{1,0:T(8,128)(2,1)} %param.27) | copy-start | bytes 196612
  6.5 14.6 %copy-start.10 = (f32[256]{0:T(256)S(1)}, f32[256]{0:T(256)}, u32[]{:S(2)}) copy-start(f32[256]{0:T(256)} %param.29) | copy-start | bytes 3076
  6.5 14.7 %copy-start.11 = (f32[256]{0:T(256)S(1)}, f32[256]{0:T(256)}, u32[]{:S(2)}) copy-start(f32[256]{0:T(256)} %param.30) | copy-start | bytes 3076
  7.4 16.6 %copy-start.1 = (bf16[1024,256]{1,0:T(8,128)(2,1)S(1)}, bf16[1024,256]{1,0:T(8,128)(2,1)}, u32[]{:S(2)}) copy-start(bf16[1024,256]{1,0:T(8,128)(2,1)} %param.28) | copy-start | bytes 1572868
  18.2 14.5 %copy-start.12 = (f32[128,1]{0,1:T(1,128)S(1)}, f32[128,1]{0,1:T(1,128)}, u32[]{:S(2)}) copy-start(f32[128,1]{0,1:T(1,128)} %param.25) | copy-start | bytes 1540
  19.0 5.0 %collective-permute-start = (bf16[128,256]{1,0:T(8,128)(2,1)S(1)}, bf16[128,256]{1,0:T(8,128)(2,1)S(1)}, u32[]{:S(2)}, u32[]{:S(2)}) collective-permute-start(bf16[128,256]{1,0:T(8,128)(2,1)S(1)} %copy-done.6), channel_id=1, source_target_pairs={{0,8},{8,0},{1,9},{9,1},{2,10},{10,2},{3,11},{11,3},{4,12},{12,4},... | collective-permute-start | bytes 196616 | tf_op jit(solution)/shard_map/ppermute | solution.py:139
  24.1 28.3 %collective-permute-start.1 = (bf16[1296,256]{1,0:T(8,128)(2,1)S(1)}, bf16[1296,256]{1,0:T(8,128)(2,1)S(1)}, u32[]{:S(2)}, u32[]{:S(2)}) collective-permute-start(bf16[1296,256]{1,0:T(8,128)(2,1)S(1)} %fusion.1), channel_id=1, source_target_pairs={{0,1},{1,0},{2,3},{3,2},{4,5},{5,4},{6,7},{7,6},{8,9},{9,8},{10,11... | collective-permute-start | bytes 1990664 | tf_op jit(solution)/shard_map/ppermute | solution.py:150
  39.2 31.7 %all-to-all-start = ((bf16[64,8,128]{2,1,0:T(8,128)(2,1)}), bf16[64,8,128]{2,1,0:T(8,128)(2,1)S(1)}, u32[]{:S(2)}, u32[]{:S(2)}) async-start(bf16[64,8,128]{2,1,0:T(8,128)(2,1)} %maximum_bitcast_fusion), calls=%async_computation | async-start | bytes 262144 | tf_op jit(solution)/shard_map/all_to_all | solution.py:108
  52.4 42.4 %copy-start.4 = (f32[128,256]{1,0:T(8,128)S(1)}, f32[128,256]{1,0:T(8,128)}, u32[]{:S(2)}) copy-start(f32[128,256]{1,0:T(8,128)} %get-tuple-element.10) | copy-start | bytes 393220
  52.4 42.4 %copy-start.5 = (f32[128,128]{1,0:T(8,128)S(1)}, f32[128,128]{1,0:T(8,128)}, u32[]{:S(2)}) copy-start(f32[128,128]{1,0:T(8,128)} %get-tuple-element.9) | copy-start | bytes 196612
  52.4 42.7 %copy-start.7 = (bf16[128,128]{1,0:T(8,128)(2,1)S(1)}, bf16[128,128]{1,0:T(8,128)(2,1)}, u32[]{:S(2)}) copy-start(bf16[128,128]{1,0:T(8,128)(2,1)} %param.22) | copy-start | bytes 98308
  52.4 42.6 %copy-start.13 = (f32[128]{0:T(128)S(1)}, f32[128]{0:T(128)}, u32[]{:S(2)}) copy-start(f32[128]{0:T(128)} %param.26) | copy-start | bytes 1540
  52.5 70.4 %copy-start = (bf16[2,1296,256]{2,1,0:T(8,128)(2,1)}, bf16[2,1296,256]{2,1,0:T(8,128)(2,1)S(1)}, u32[]{:S(2)}) copy-start(bf16[2,1296,256]{2,1,0:T(8,128)(2,1)S(1)} %pad_maximum_fusion.refs_0_) | copy-start | bytes 3981316
  52.6 70.4 %collective-permute-start.2 = (bf16[2,1296,256]{2,1,0:T(8,128)(2,1)S(1)}, bf16[2,1296,256]{2,1,0:T(8,128)(2,1)S(1)}, u32[]{:S(2)}, u32[]{:S(2)}) collective-permute-start(bf16[2,1296,256]{2,1,0:T(8,128)(2,1)S(1)} %pad_maximum_fusion.refs_0_), channel_id=1, source_target_pairs={{0,2},{2,4},{4,6},{6,0},{1,3},{3,5},{5,7},{7,1},{8,10},{10,12},{12... | collective-permute-start | bytes 3981320 | tf_op jit(solution)/shard_map/ppermute | solution.py:153
  55.7 67.3 %collective-permute-start.3 = (bf16[2,1296,256]{2,1,0:T(8,128)(2,1)S(1)}, bf16[2,1296,256]{2,1,0:T(8,128)(2,1)}, u32[]{:S(2)}, u32[]{:S(2)}) collective-permute-start(bf16[2,1296,256]{2,1,0:T(8,128)(2,1)S(1)} %pad_maximum_fusion.refs_0_), channel_id=1, source_target_pairs={{0,4},{2,6},{4,0},{6,2},{1,5},{3,7},{5,1},{7,3},{8,12},{10,14},{12... | collective-permute-start | bytes 3981320 | tf_op jit(solution)/shard_map/ppermute | solution.py:153
  60.1 62.9 %collective-permute-start.4 = (bf16[2,1296,256]{2,1,0:T(8,128)(2,1)S(1)}, bf16[2,1296,256]{2,1,0:T(8,128)(2,1)}, u32[]{:S(2)}, u32[]{:S(2)}) collective-permute-start(bf16[2,1296,256]{2,1,0:T(8,128)(2,1)S(1)} %pad_maximum_fusion.refs_0_), channel_id=1, source_target_pairs={{0,6},{2,0},{4,2},{6,4},{1,7},{3,1},{5,3},{7,5},{8,14},{10,8},{12,... | collective-permute-start | bytes 3981320 | tf_op jit(solution)/shard_map/ppermute | solution.py:153
  70.9 0.7 copy-start.3
  95.9 23.7 %all-to-all-start.2 = ((bf16[8,128,128]{2,1,0:T(8,128)(2,1)}), bf16[8,128,128]{2,1,0:T(8,128)(2,1)S(1)}, u32[]{:S(2)}, u32[]{:S(2)}) async-start(bf16[8,128,128]{2,1,0:T(8,128)(2,1)} %broadcast_in_dim.16), calls=%async_computation.2 | async-start | bytes 524288 | tf_op jit(solution)/shard_map/all_to_all | solution.py:25
  123.0 1.1 copy-start.2
  137.3 29.9 %copy-start.8 = (f32[256]{0:T(256)S(1)}, f32[256]{0:T(256)}, u32[]{:S(2)}) copy-start(f32[256]{0:T(256)} %param.35) | copy-start | bytes 3076
  137.3 29.9 %copy-start.9 = (f32[256]{0:T(256)S(1)}, f32[256]{0:T(256)}, u32[]{:S(2)}) copy-start(f32[256]{0:T(256)} %param.34) | copy-start | bytes 3076
  137.3 20.9 %all-to-all-start.4 = ((bf16[16,128,256]{2,1,0:T(8,128)(2,1)}), bf16[16,128,256]{2,1,0:T(8,128)(2,1)S(1)}, u32[]{:S(2)}, u32[]{:S(2)}) async-start(bf16[16,128,256]{2,1,0:T(8,128)(2,1)} %bitcast.45), calls=%async_computation.4 | async-start | bytes 2097152 | tf_op jit(solution)/shard_map/all_to_all | solution.py:326
Sparse Core Ops, SparseCore 0:
  19.1 82.9 all-gather.2

commit v3 on v2

v3 whole, which is shorter than its diff:
```python
import jax
import jax.numpy as jnp
from jax import lax
from jax.experimental import pallas as pl
from jax.experimental.pallas import tpu as pltpu
from jax.sharding import Mesh
from jax.sharding import PartitionSpec as P


D = 2048
SP = ("z", "ya", "yb")
TP = ("x", "c")
HALF = 384

highest_precision = lax.Precision.HIGHEST
alpha_mix = 2.0**0.25
norm_eps = 1e-05
head_eps = 1e-06


def exact_dot(a, b, dims=((1,), (0,))):
    return lax.dot_general(
        a, b, (dims, ((), ())), precision=highest_precision, preferred_element_type=jnp.float32
    )


def local_kernel(
    query_ref,
    value_ref,
    onward_ref,
    reverse_ref,
    onward_gap_ref,
    reverse_gap_ref,
    extra_ref,
    inner_ref,
    queries_ref,
    packed_ref,
    rows_ref,
):
    rows, width = query_ref.shape
    half = width // 2
    logits = query_ref[...].astype(jnp.float32)
    query = logits / (1.0 + jnp.exp(-logits))
    values = value_ref[...].astype(jnp.float32)
    extra = extra_ref[...]
    at = lax.broadcasted_iota(jnp.int32, (rows, rows), 0)
    source = lax.broadcasted_iota(jnp.int32, (rows, rows), 1)
    ones = jnp.ones((rows, width), jnp.float32)
    inner = jnp.zeros_like(query)
    for side, (forget_ref, gap_ref, seen, last) in enumerate(
        (
            (onward_ref, onward_gap_ref, at >= source, rows - 1),
            (reverse_ref, reverse_gap_ref, at <= source, 0),
        )
    ):
        seen = seen.astype(jnp.float32)
        keys = gap_ref[...] / (1.0 + jnp.exp(forget_ref[...].astype(jnp.float32)))
        log_decay = jnp.log1p(-keys)
        running = exact_dot(seen, log_decay) + exact_dot(seen * extra, ones)
        total = running[last : last + 1]
        decayed_query = query * jnp.exp(running)
        scores = exact_dot(decayed_query, keys * jnp.exp(-running), ((1,), (1,))) * seen
        inner = inner + exact_dot(scores, values)
        queries_ref[:, width * side : width * (side + 1)] = decayed_query
        state = exact_dot(keys * jnp.exp(total - running), values, ((0,), (0,)))
        decay = exact_dot(log_decay, ones, ((0,), (0,))) + jnp.sum(extra)
        for part in range(2):
            rows_ref[:, 2 * side + part, :] = state[part * half : (part + 1) * half]
            rows_ref[:, 4 + 2 * side + part, :] = decay[part * half : (part + 1) * half]
    packed_ref[...] = rows_ref[...].astype(jnp.bfloat16)
    inner_ref[...] = inner


def local_pass(query, values, onward, reverse, onward_gap, reverse_gap, extra):
    rows, width = query.shape
    half = width // 2
    return pl.pallas_call(
        local_kernel,
        out_shape=[
            jax.ShapeDtypeStruct((rows, width), jnp.float32),
            jax.ShapeDtypeStruct((rows, 2 * width), jnp.float32),
            jax.ShapeDtypeStruct((half, 8, width), jnp.bfloat16),
        ],
        scratch_shapes=[pltpu.VMEM((half, 8, width), jnp.float32)],
        name="local",
    )(query, values, onward, reverse, onward_gap[None], reverse_gap[None], extra.reshape(1, rows))


def gated_kernel(back_ref, inner_ref, queries_ref, gain_ref, gate_ref, out_ref, states_ref):
    states_ref[...] = back_ref[...].astype(jnp.float32)
    width = inner_ref.shape[1]
    mixed = inner_ref[...]
    for side in range(2):
        state = jnp.concatenate([states_ref[:, 2 * side, :], states_ref[:, 2 * side + 1, :]], axis=0)
        mixed = mixed + exact_dot(queries_ref[:, width * side : width * (side + 1)], state)
    mean = jnp.mean(mixed * mixed, axis=1, keepdims=True)
    normed = mixed * lax.rsqrt(mean + head_eps) * gain_ref[...]
    gate = gate_ref[...].astype(jnp.float32)
    gated = (normed * (gate / (1.0 + jnp.exp(-gate)))).astype(jnp.bfloat16)
    for peer in range(out_ref.shape[0]):
        out_ref[peer] = gated


def gated_rows(back, inner, queries, gain, gate, peers):
    return pl.pallas_call(
        gated_kernel,
        out_shape=jax.ShapeDtypeStruct((peers, *inner.shape), jnp.bfloat16),
        scratch_shapes=[pltpu.VMEM(back.shape, jnp.float32)],
        name="gated",
    )(back, inner, queries, gain[None], gate)


def scan_kernel(chunks, local_ref, before_ref):
    local = local_ref[...].astype(jnp.float32)
    decay = jnp.exp(local[:, 4:8])
    state = local[:, 0:4]
    ahead = [None] * chunks
    run = jnp.zeros((2, 128), jnp.float32)
    for c in range(chunks):
        ahead[c] = run
        run = decay[c, 0:2] * run + state[c, 0:2]
    run = jnp.zeros((2, 128), jnp.float32)
    for c in reversed(range(chunks)):
        before_ref[c] = jnp.concatenate([ahead[c], run], axis=0).astype(jnp.bfloat16)
        run = decay[c, 2:4] * run + state[c, 2:4]


def scanned(arrived):
    chunks = arrived.shape[0]
    return pl.pallas_call(
        lambda *refs: scan_kernel(chunks, *refs),
        out_shape=jax.ShapeDtypeStruct((chunks, 4, 128), jnp.bfloat16),
        name="scan",
    )(arrived)


def gathered_weights(gate, up, down):
    both = jnp.stack([gate, up, down.T])
    first = both[:, :, :HALF]
    second = jnp.pad(both[:, :, HALF:], ((0, 0), (0, 0), (0, 2 * HALF - both.shape[2])))
    halves = jnp.stack([first, second, first, second])
    arrived = lax.all_to_all(halves, ("ya", "yb"), 0, 0, tiled=True)
    shard = jnp.moveaxis(arrived, 0, 1).reshape(3 * 128, HALF)
    return lax.all_gather(shard, "z", axis=0, tiled=True).reshape(-1, 3, 128, HALF)


def exact_terms(x):
    terms = []
    for _ in range(3):
        term = lax.reduce_precision(x, 8, 7)
        terms.append(term.astype(jnp.bfloat16))
        x = x - term
    return terms


SWAP = ((0, 1), (1, 0))


def spread_over_x(output_matrix, residual, gain, bias):
    other = lax.ppermute(residual, "yb", SWAP)
    first = lax.axis_index("yb") == 0
    vectors = jnp.stack(exact_terms(gain) + exact_terms(bias))
    block = jnp.concatenate(
        [
            output_matrix,
            jnp.where(first, residual, other),
            jnp.where(first, other, residual),
            jnp.pad(vectors, ((0, 10), (0, 0))),
        ]
    )
    count = lax.axis_size("x")
    return [block] + [
        lax.ppermute(block, "x", [(i, (i + k) % count) for i in range(count)])
        for k in range(1, count)
    ]


def middle_kernel(place_ref, gated_ref, *refs):
    block_refs, (out_ref, whole_ref, before_ref) = refs[:8], refs[8:]
    heads, rows = 8, gated_ref.shape[2]
    count = 2 * rows
    for core in range(2):
        for pair in range(2):
            for x in range(4):
                head = 2 * x + core
                whole_ref[pair * rows : (pair + 1) * rows, 128 * head : 128 * head + 128] = (
                    gated_ref[core, 4 * pair + x]
                )
    whole = whole_ref[...]
    inner = whole.shape[1]
    total = jnp.zeros((count, 1), jnp.float32)
    for b in range(heads):
        mixer = jnp.dot(whole, block_refs[b][:inner], preferred_element_type=jnp.float32)
        residual = block_refs[b][inner : inner + count].astype(jnp.float32)
        before = alpha_mix * residual + mixer
        before_ref[b] = before
        total = total + jnp.sum(before, axis=1, keepdims=True)
    mean = total / D
    spread = jnp.zeros((count, 1), jnp.float32)
    for b in range(heads):
        centre = before_ref[b] - mean
        spread = spread + jnp.sum(centre * centre, axis=1, keepdims=True)
    scale = lax.rsqrt(spread / D + norm_eps)
    for b in range(heads):
        vectors = block_refs[b][inner + count : inner + count + 16].astype(jnp.float32)
        gain = vectors[0:1] + vectors[1:2] + vectors[2:3]
        bias = vectors[3:4] + vectors[4:5] + vectors[5:6]
        normed = (before_ref[b] - mean) * scale * gain + bias
        out_ref[place_ref[b]] = normed.astype(jnp.bfloat16)


def middle_rows(gated, blocks):
    rows, width = gated.shape[2], blocks[0].shape[1]
    x, core = lax.axis_index("x"), lax.axis_index("c")
    place = jnp.stack([2 * ((x - b // 2 + 4) % 4) + (core + b) % 2 for b in range(8)])
    vmem = pl.BlockSpec(memory_space=pltpu.VMEM)
    return pl.pallas_call(
        middle_kernel,
        in_specs=[pl.BlockSpec(memory_space=pltpu.SMEM)] + [vmem] * 9,
        out_specs=vmem,
        out_shape=jax.ShapeDtypeStruct((8, 2 * rows, width), jnp.bfloat16),
        scratch_shapes=[
            pltpu.VMEM((2 * rows, 8 * 128), jnp.bfloat16),
            pltpu.VMEM((8, 2 * rows, width), jnp.float32),
        ],
        name="middle",
    )(place.astype(jnp.int32), gated, *blocks)


def feed_kernel(
    steps, core_ref, rows_ref, enter_ref, leave_ref, keep_ref, send_ref, gate_ref, up_ref, hidden_ref
):
    phase, step = pl.program_id(0), pl.program_id(1)

    @pl.when(jnp.logical_and(phase == 0, step == 0))
    def _():
        gate_ref[...] = jnp.zeros_like(gate_ref)
        up_ref[...] = jnp.zeros_like(up_ref)

    @pl.when(phase == 0)
    def _():
        for to_ref, kind in ((gate_ref, 0), (up_ref, 1)):
            product = 0.0
            for b in range(rows_ref.shape[0]):
                wide = jnp.concatenate([enter_ref[2 * b, kind], enter_ref[2 * b + 1, kind]], axis=0)
                product += jnp.dot(rows_ref[b], wide, preferred_element_type=jnp.float32)
            to_ref[...] += product

    @pl.when(jnp.logical_and(phase == 0, step == steps - 1))
    def _():
        gate = gate_ref[...]
        hidden_ref[...] = (gate / (1.0 + jnp.exp(-gate)) * up_ref[...]).astype(jnp.bfloat16)

    @pl.when(phase == 1)
    def _():
        core = core_ref[0]
        for to_ref, b in ((keep_ref, core), (send_ref, 1 - core)):
            down = jnp.concatenate([leave_ref[2 * b, 0], leave_ref[2 * b + 1, 0]], axis=0)
            product = lax.dot_general(
                hidden_ref[...],
                down,
                (((1,), (1,)), ((), ())),
                preferred_element_type=jnp.float32,
            ).astype(jnp.bfloat16)
            for pair in range(2):
                rows = to_ref.shape[2]
                to_ref[pair, 0] = product[pair * rows : (pair + 1) * rows]


def feed_forward(rows, weights):
    blocks, count, width = rows.shape
    each = 2
    steps = blocks // each
    out = jax.ShapeDtypeStruct((2, steps, count // 2, width), jnp.bfloat16)
    out_spec = pl.BlockSpec(
        (2, 1, count // 2, width), lambda p, s, c: (0, jnp.where(p == 0, 0, s), 0, 0)
    )
    return pl.pallas_call(
        lambda *refs: feed_kernel(steps, *refs),
        grid_spec=pltpu.PrefetchScalarGridSpec(
            num_scalar_prefetch=1,
            grid=(2, steps),
            in_specs=[
                pl.BlockSpec(
                    (each, count, width), lambda p, s, c: (jnp.where(p == 0, s, steps - 1), 0, 0)
                ),
                pl.BlockSpec(
                    (2 * each, 2, 128, HALF),
                    lambda p, s, c: (jnp.where(p == 0, s, steps - 1), 0, 0, 0),
                ),
                pl.BlockSpec(
                    (2 * each, 1, 128, HALF), lambda p, s, c: (jnp.where(p == 0, 0, s), 2, 0, 0)
                ),
            ],
            out_specs=[out_spec, out_spec],
            scratch_shapes=[
                pltpu.VMEM((count, HALF), jnp.float32),
                pltpu.VMEM((count, HALF), jnp.float32),
                pltpu.VMEM((count, HALF), jnp.bfloat16),
            ],
        ),
        out_shape=[out, out],
        compiler_params=pltpu.CompilerParams(dimension_semantics=("arbitrary", "arbitrary")),
        cost_estimate=pl.CostEstimate(
            flops=6 * count * D * HALF, bytes_accessed=6 * D * HALF, transcendentals=count * HALF
        ),
        name="feed_forward",
    )(lax.axis_index("c").astype(jnp.int32)[None], rows, weights, weights)


def total_kernel(arrived_ref, own_ref, before_ref, moments_ref):
    feed = arrived_ref[0].astype(jnp.float32)
    for peer in range(1, arrived_ref.shape[0]):
        feed = feed + arrived_ref[peer].astype(jnp.float32)
    before = alpha_mix * own_ref[...].astype(jnp.float32) + feed
    before_ref[...] = before
    ones = jnp.ones((8, before.shape[1]), jnp.float32)
    sums = exact_dot(ones, before, ((1,), (1,)))
    squares = exact_dot(ones, before * before, ((1,), (1,)))
    moments = jnp.concatenate([sums[0:4], squares[0:4]], axis=0)
    for peer in range(moments_ref.shape[0]):
        moments_ref[peer] = moments


def closing_kernel(moments_ref, before_ref, gain_ref, bias_ref, out_ref):
    moments = moments_ref[0]
    for peer in range(1, moments_ref.shape[0]):
        moments = moments + moments_ref[peer]
    mean = moments[0:1] / D
    spread = moments[4:5] / D - mean * mean
    scale = lax.rsqrt(spread + norm_eps)
    rows, _ = before_ref.shape
    at = lax.broadcasted_iota(jnp.int32, (rows, rows), 0)
    diagonal = (at == lax.broadcasted_iota(jnp.int32, (rows, rows), 1)).astype(jnp.float32)
    column = jnp.sum(diagonal * mean, axis=1, keepdims=True)
    factor = jnp.sum(diagonal * scale, axis=1, keepdims=True)
    out_ref[...] = ((before_ref[...] - column) * factor * gain_ref[...] + bias_ref[...]).astype(
        jnp.bfloat16
    )


def layer(
    query_logits,
    value_rows,
    onward_forget_logits,
    reverse_forget_logits,
    output_gate_logits,
    onward_floor_gap,
    reverse_floor_gap,
    extra_log_decay,
    per_head_gain,
    residual,
    output_matrix,
    inner_norm_gain,
    inner_norm_bias,
    gate_matrix,
    up_matrix,
    down_matrix,
    closing_norm_gain,
    closing_norm_bias,
):
    weights = gathered_weights(gate_matrix, up_matrix, down_matrix)
    rows = query_logits.shape[0]
    inner, queries, packed = local_pass(
        query_logits,
        value_rows,
        onward_forget_logits,
        reverse_forget_logits,
        onward_floor_gap,
        reverse_floor_gap,
        extra_log_decay,
    )
    packed, output_matrix, residual = lax.optimization_barrier((packed, output_matrix, residual))
    arrived = lax.all_to_all(packed, SP, 0, 0, tiled=True)
    blocks = spread_over_x(output_matrix, residual, inner_norm_gain, inner_norm_bias)
    before, *blocks = lax.optimization_barrier((scanned(arrived), *blocks))
    back = lax.all_to_all(before, SP, 0, 0, tiled=True)
    both = []
    for block in blocks:
        both += [block, lax.ppermute(block, "c", SWAP)]
    gated = gated_rows(back, inner, queries, per_head_gain, output_gate_logits, 8)
    everyone = lax.all_gather(lax.all_to_all(gated, ("yb", "x"), 0, 0, tiled=True), "c")
    middle = middle_rows(everyone, both)
    keep, send = feed_forward(middle, weights)
    joined = keep.astype(jnp.float32) + lax.ppermute(send, "c", SWAP).astype(jnp.float32)
    joined = joined.astype(jnp.bfloat16).reshape(-1, *keep.shape[2:])
    shares = lax.all_to_all(joined, ("yb", "x"), 0, 0, tiled=True)
    own = lax.dynamic_slice(
        middle,
        (lax.axis_index(TP), lax.axis_index("yb") * rows, 0),
        (1, rows, middle.shape[2]),
    )[0]
    before_final, moments = pl.pallas_call(
        total_kernel,
        out_shape=[
            jax.ShapeDtypeStruct(own.shape, jnp.float32),
            jax.ShapeDtypeStruct((8, 8, rows), jnp.float32),
        ],
        name="total",
    )(shares, own)
    return pl.pallas_call(
        closing_kernel,
        out_shape=jax.ShapeDtypeStruct(own.shape, jnp.bfloat16),
        name="closing",
    )(
        lax.all_to_all(moments, TP, 0, 0, tiled=True),
        before_final,
        closing_norm_gain[None],
        closing_norm_bias[None],
    )


def solution(mesh):
    torus = Mesh(mesh.devices.reshape(16, 2, 2, 4, 2), ("z", "ya", "yb", "x", "c"))
    in_specs = (
        P(SP, TP),
        P(SP, TP),
        P(SP, TP),
        P(SP, TP),
        P(SP, TP),
        P(TP),
        P(TP),
        P(SP, TP),
        P(),
        P(SP, TP),
        P(None, TP),
        P(TP),
        P(TP),
        P(SP, TP),
        P(SP, TP),
        P(TP, SP),
        P(TP),
        P(TP),
    )
    out_specs = P(SP, TP)
    return jax.shard_map(layer, mesh=torus, in_specs=in_specs, out_specs=out_specs, check_vma=False)
```

time: 177 us -> 178 us (level)
  blocking collectives: 43.1 us -> 77.8 us
  waiting for transfers between devices: 45.7 us -> 18.6 us
  starting transfers between devices: 43.1 us -> 36.3 us
  Pallas kernels: 18 us -> 23.9 us
  other arithmetic: 6.36 us -> 2.96 us
    all_to_all x2 -> x3, blocking collectives: 29.2 us -> 61.7 us  [the longest x1 32.5 us: layer(): arrived = lax.all_to_all(packed, SP, 0, 0, tiled=True)]
    all_to_all x3 -> x2, waiting for transfers between devices: 43.1 us -> 14.2 us  [the longest x1 8.7 us: layer(): shares = lax.all_to_all(joined, ('yb', 'x'), 0, 0, tiled=True)]
    all_to_all x3 -> x2, starting transfers between devices: 21.7 us -> 6.9 us  [the longest x1 3.49 us: layer(): shares = lax.all_to_all(joined, ('yb', 'x'), 0, 0, tiled=True)]
    ppermute x5 -> x9, starting transfers between devices: 21.3 us -> 29.4 us  [the longest x4 14.1 us: layer(): both += [block, lax.ppermute(block, 'c', SWAP)]]
    pallas_call x3 -> x6, Pallas kernels: 12.4 us -> 18.3 us  [the longest x1 7.79 us: feed_forward(): pl.pallas_call(lambda *refs: feed_kernel(steps, *refs), grid_spec=pltpu.P...]
    all_gather x1, blocking collectives: 3.27 us -> 5.38 us  [layer(): lax.all_gather(lax.all_to_all(gated, ('yb', 'x'), 0, 0, tiled=True), 'c')]
    ppermute x5 -> x9, waiting for transfers between devices: 2.66 us -> 4.39 us  [the longest x1 2.65 us: spread_over_x(): other = lax.ppermute(residual, 'yb', SWAP)]
  transfers between devices with their start and end apart: 9 -> 12, of which waited for: 4 -> 4; matrix products, arithmetic and copies ran while one was open for 3% -> 1% of each run, Pallas kernels for 6% -> 7%
where the time goes in v3:
time: 178 us; the launch traced here: 177 us
  blocking collectives  77.8 us (44%)
  starting transfers between devices  36.3 us (20%)
  Pallas kernels  23.9 us (13%)
  waiting for transfers between devices  18.6 us (10%)
  between operations  13.9 us (8%)
  local copies, waits for them, and re-layouts  3.74 us (2%)
  other arithmetic  2.96 us (2%)
    all_to_all x1, blocking collectives, layer(): arrived = lax.all_to_all(packed, SP, 0, 0, tiled=True)  32.5 us
    all_to_all x1, blocking collectives, layer(): back = lax.all_to_all(before, SP, 0, 0, tiled=True)  19.8 us
    ppermute x4, starting transfers between devices, layer(): both += [block, lax.ppermute(block, 'c', SWAP)]  14.1 us
    ppermute x3, starting transfers between devices, spread_over_x(): lax.ppermute(block, 'x', [(i, (i + k) % count) for i in range(count)])  10.7 us
    all_to_all x1, blocking collectives, gathered_weights(): arrived = lax.all_to_all(halves, ('ya', 'yb'), 0, 0, tiled=True)  10.6 us
    all_to_all x1, blocking collectives, layer(): lax.all_to_all(moments, TP, 0, 0, tiled=True)  9.41 us
    all_to_all x1, waiting for transfers between devices, layer(): shares = lax.all_to_all(joined, ('yb', 'x'), 0, 0, tiled=True)  8.7 us
    pallas_call x1, Pallas kernels, feed_forward(): pl.pallas_call(lambda *refs: feed_kernel(steps, *refs), grid_spec=pltpu.P...  7.79 us
  transfers between devices with their start and end apart: 12, of which 4 were waited for; matrix products, arithmetic and copies ran while one was open for 1% of the time, Pallas kernels for 7%

profile of v3, /device:TPU:1, one launch (start us, length us, event | category | flops | bytes accessed | tf_op | source)
XLA Modules:
  0.0 177.2 jit_solution(7893818431910342088)
XLA Ops:
  7.6 10.6 %all_to_all.30 = bf16[4,3,32,384]{3,2,1,0:T(8,128)(2,1)S(1)} all-to-all(bf16[4,3,32,384]{3,2,1,0:T(8,128)(2,1)S(1)} %pad_maximum_fusion), channel_id=1, replica_groups=mesh['z'=16,'ya'=2,'yb'=2,'x'=4,'c'=2] {'ya','yb'}, dimensions={0} | all-to-all | bytes 589824 | tf_op jit(solution)/shard_map/all_to_all | solution.py:142
  19.0 3.0 %local.1 = (f32[128,128]{1,0:T(8,128)}, f32[128,256]{1,0:T(8,128)}, bf16[64,8,128]{2,1,0:T(8,128)(2,1)}) custom-call(bf16[128,128]{1,0:T(8,128)(2,1)} %query_ref.1, bf16[128,128]{1,0:T(8,128)(2,1)} %value_ref.1, bf16[128,128]{1,0:T(8,128)(2,1)} %onward_ref.1, bf16[128,128]{1,0:T(8,128)(2,1)} %reverse_ref.1, f32[1,128]{1,0:T(1,128)} %bitcast.41, ...), custom_call_target="tpu_custom_call" | custom-call | tf_op jit(solution)/shard_map/local/pallas_call | solution.py:77
  22.0 2.3 %collective-permute-start = (bf16[128,256]{1,0:T(8,128)(2,1)S(1)}, bf16[128,256]{1,0:T(8,128)(2,1)S(1)}, u32[]{:S(2)}, u32[]{:S(2)}) collective-permute-start(bf16[128,256]{1,0:T(8,128)(2,1)S(1)} %copy-done.7), channel_id=1, source_target_pairs={{0,8},{8,0},{1,9},{9,1},{2,10},{10,2},{3,11},{11,3},{4,12},{12,4},... | collective-permute-start | bytes 196616 | tf_op jit(solution)/shard_map/ppermute | solution.py:160
  24.5 2.6 %collective-permute-done = bf16[128,256]{1,0:T(8,128)(2,1)S(1)} collective-permute-done((bf16[128,256]{1,0:T(8,128)(2,1)S(1)}, bf16[128,256]{1,0:T(8,128)(2,1)S(1)}, u32[]{:S(2)}, u32[]{:S(2)}) %collective-permute-start) | collective-permute-done | bytes 65568 | tf_op jit(solution)/shard_map/ppermute | solution.py:160
  27.2 3.3 %collective-permute-start.1 = (bf16[1296,256]{1,0:T(8,128)(2,1)S(1)}, bf16[1296,256]{1,0:T(8,128)(2,1)S(1)}, u32[]{:S(2)}, u32[]{:S(2)}) collective-permute-start(bf16[1296,256]{1,0:T(8,128)(2,1)S(1)} %fusion.1.refs_0_), channel_id=1, source_target_pairs={{0,2},{2,4},{4,6},{6,0},{1,3},{3,5},{5,7},{7,1},{8,10},{10,12},{12... | collective-permute-start | bytes 1990664 | tf_op jit(solution)/shard_map/ppermute | solution.py:173
  30.5 4.4 %collective-permute-start.2 = (bf16[1296,256]{1,0:T(8,128)(2,1)S(1)}, bf16[1296,256]{1,0:T(8,128)(2,1)S(1)}, u32[]{:S(2)}, u32[]{:S(2)}) collective-permute-start(bf16[1296,256]{1,0:T(8,128)(2,1)S(1)} %fusion.1.refs_0_), channel_id=1, source_target_pairs={{0,4},{2,6},{4,0},{6,2},{1,5},{3,7},{5,1},{7,3},{8,12},{10,14},{12... | collective-permute-start | bytes 1990664 | tf_op jit(solution)/shard_map/ppermute | solution.py:173
  34.9 3.1 %collective-permute-start.3 = (bf16[1296,256]{1,0:T(8,128)(2,1)S(1)}, bf16[1296,256]{1,0:T(8,128)(2,1)S(1)}, u32[]{:S(2)}, u32[]{:S(2)}) collective-permute-start(bf16[1296,256]{1,0:T(8,128)(2,1)S(1)} %fusion.1.refs_0_), channel_id=1, source_target_pairs={{0,6},{2,0},{4,2},{6,4},{1,7},{3,1},{5,3},{7,5},{8,14},{10,8},{12,... | collective-permute-start | bytes 1990664 | tf_op jit(solution)/shard_map/ppermute | solution.py:173
  38.0 32.5 %all_to_all.31.refs_0_ = bf16[64,8,128]{2,1,0:T(8,128)(2,1)} all-to-all(bf16[64,8,128]{2,1,0:T(8,128)(2,1)S(1)} %copy-done.6), channel_id=1, replica_groups=mesh['z'=16,'ya'=2,'yb'=2,'x'=4,'c'=2] {'z','ya','yb'}, dimensions={0} | all-to-all | bytes 262144 | tf_op jit(solution)/shard_map/all_to_all | solution.py:374
  72.2 7.9 %collective-permute-start.4 = (bf16[1296,256]{1,0:T(8,128)(2,1)S(1)}, bf16[1296,256]{1,0:T(8,128)(2,1)}, u32[]{:S(2)}, u32[]{:S(2)}) collective-permute-start(bf16[1296,256]{1,0:T(8,128)(2,1)S(1)} %fusion.1.refs_0_), channel_id=1, source_target_pairs={{0,1},{1,0},{2,3},{3,2},{4,5},{5,4},{6,7},{7,6},{8,9},{9,8},{10,11... | collective-permute-start | bytes 1990664 | tf_op jit(solution)/shard_map/ppermute | solution.py:380
  82.0 2.4 %collective-permute-start.6 = (bf16[1296,256]{1,0:T(8,128)(2,1)S(1)}, bf16[1296,256]{1,0:T(8,128)(2,1)}, u32[]{:S(2)}, u32[]{:S(2)}) collective-permute-start(bf16[1296,256]{1,0:T(8,128)(2,1)S(1)} %collective-permute-done.2.refs_4_), channel_id=1, source_target_pairs={{0,1},{1,0},{2,3},{3,2},{4,5},{5,4},{6,7},{7,6},{8,9},{9,8},{10,11... | collective-permute-start | bytes 1990664 | tf_op jit(solution)/shard_map/ppermute | solution.py:380
  84.5 1.9 %collective-permute-start.7 = (bf16[1296,256]{1,0:T(8,128)(2,1)S(1)}, bf16[1296,256]{1,0:T(8,128)(2,1)}, u32[]{:S(2)}, u32[]{:S(2)}) collective-permute-start(bf16[1296,256]{1,0:T(8,128)(2,1)S(1)} %collective-permute-done.3.refs_6_), channel_id=1, source_target_pairs={{0,1},{1,0},{2,3},{3,2},{4,5},{5,4},{6,7},{7,6},{8,9},{9,8},{10,11... | collective-permute-start | bytes 1990664 | tf_op jit(solution)/shard_map/ppermute | solution.py:380
  86.4 19.8 %all_to_all.32.back_ref = bf16[64,4,128]{2,1,0:T(4,128)(2,1)} all-to-all(bf16[64,4,128]{2,1,0:T(4,128)(2,1)} %scan.1), channel_id=1, replica_groups=mesh['z'=16,'ya'=2,'yb'=2,'x'=4,'c'=2] {'z','ya','yb'}, dimensions={0} | all-to-all | bytes 131072 | tf_op jit(solution)/shard_map/all_to_all | solution.py:377
  106.2 2.1 %gated.1 = bf16[8,128,128]{2,1,0:T(8,128)(2,1)} custom-call(bf16[64,4,128]{2,1,0:T(4,128)(2,1)} %all_to_all.32.back_ref, f32[128,128]{1,0:T(8,128)} %get-tuple-element.25.inner_ref, f32[128,256]{1,0:T(8,128)} %get-tuple-element.26.queries_ref, f32[1,128]{1,0:T(1,128)} %bitcast.44, bf16[128,128]{1,0:T(8,128)(2,1)} %gate_ref.1), custom_call_target="tpu_custom_call" | custom-call | tf_op jit(solution)/shard_map/gated/pallas_call | solution.py:105
  108.3 3.4 %all-to-all-start.2 = ((bf16[8,128,128]{2,1,0:T(8,128)(2,1)}), bf16[8,128,128]{2,1,0:T(8,128)(2,1)S(1)}, u32[]{:S(2)}, u32[]{:S(2)}) async-start(bf16[8,128,128]{2,1,0:T(8,128)(2,1)} %gated.1), calls=%async_computation.2 | async-start | bytes 524288 | tf_op jit(solution)/shard_map/all_to_all | solution.py:382
  112.4 5.5 %all-to-all-done.2 = bf16[8,128,128]{2,1,0:T(8,128)(2,1)S(1)} async-done(((bf16[8,128,128]{2,1,0:T(8,128)(2,1)}), bf16[8,128,128]{2,1,0:T(8,128)(2,1)S(1)}, u32[]{:S(2)}, u32[]{:S(2)}) %all-to-all-start.2) | async-done | bytes 262176 | tf_op jit(solution)/shard_map/all_to_all | solution.py:382
  117.9 5.4 %all-gather = bf16[16,128,128]{2,1,0:T(8,128)(2,1)} all-gather(bf16[8,128,128]{2,1,0:T(8,128)(2,1)S(1)} %all-to-all-done.2), channel_id=2, replica_groups=mesh['z'=16,'ya'=2,'yb'=2,'x'=4,'c'=2] {'c'}, dimensions={0}, use_global_device_ids=true | all-gather | bytes 786432 | tf_op jit(solution)/shard_map/all_gather | solution.py:382
  123.4 5.6 %middle.1.refs_1_ = bf16[8,256,256]{2,1,0:T(8,128)(2,1)} custom-call(s32[8]{0:T(128)} %stack.79.place_ref, bf16[2,8,128,128]{3,2,1,0:T(8,128)(2,1)} %bitcast.34, bf16[1296,256]{1,0:T(8,128)(2,1)} %copy-done, bf16[1296,256]{1,0:T(8,128)(2,1)} %collective-permute-done.4.refs_1_, bf16[1296,256]{1,0:T(8,128)(2,1)} %copy-done.2, ...), custom_call_target="tpu_custom_call" | custom-call | tf_op jit(solution)/shard_map/middle/pallas_call | solution.py:217
  129.0 7.8 %feed_forward.1 = (bf16[2,4,128,256]{3,2,1,0:T(8,128)(2,1)}, bf16[2,4,128,256]{3,2,1,0:T(8,128)(2,1)}) custom-call(s32[1]{0:T(128)} %bitcast.refs_0_, bf16[8,256,256]{2,1,0:T(8,128)(2,1)} %middle.1.refs_1_, bf16[16,3,128,384]{3,2,1,0:T(8,128)(2,1)} %bitcast.32, bf16[16,3,128,384]{3,2,1,0:T(8,128)(2,1)} %bitcast.33), custom_call_target="tpu_custom_call" | custom-call | flops 1207959552 | bytes 4718592 | tf_op jit(solution)/shard_map/feed_forward/pallas_call | solution.py:278
  136.8 2.3 %collective-permute-start.8 = (bf16[2,4,128,256]{3,2,1,0:T(8,128)(2,1)}, bf16[2,4,128,256]{3,2,1,0:T(8,128)(2,1)S(1)}, u32[]{:S(2)}, u32[]{:S(2)}) collective-permute-start(bf16[2,4,128,256]{3,2,1,0:T(8,128)(2,1)} %get-tuple-element.32), channel_id=1, source_target_pairs={{0,1},{1,0},{2,3},{3,2},{4,5},{5,4},{6,7},{7,6},{8,9},{9,8},{10,11... | collective-permute-start | bytes 1572872 | tf_op jit(solution)/shard_map/ppermute | solution.py:385
  140.8 2.0 %add_convert_fusion = bf16[2,4,128,256]{3,2,1,0:T(8,128)(2,1)} fusion(bf16[2,4,128,256]{3,2,1,0:T(8,128)(2,1)S(1)} %collective-permute-done.8, bf16[2,4,128,256]{3,2,1,0:T(8,128)(2,1)} %get-tuple-element.31), kind=kLoop, calls=%fused_computation.2 | loop fusion | flops 1048576 | bytes 1572864 | tf_op jit(solution)/shard_map/convert_element_type | solution.py:386
  142.7 3.5 %all-to-all-start.4 = ((bf16[8,128,256]{2,1,0:T(8,128)(2,1)}), bf16[8,128,256]{2,1,0:T(8,128)(2,1)S(1)}, u32[]{:S(2)}, u32[]{:S(2)}) async-start(bf16[8,128,256]{2,1,0:T(8,128)(2,1)} %bitcast.23), calls=%async_computation.4 | async-start | bytes 1048576 | tf_op jit(solution)/shard_map/all_to_all | solution.py:387
  147.7 8.7 %all-to-all-done.4.arrived_ref = bf16[8,128,256]{2,1,0:T(8,128)(2,1)S(1)} async-done(((bf16[8,128,256]{2,1,0:T(8,128)(2,1)}), bf16[8,128,256]{2,1,0:T(8,128)(2,1)S(1)}, u32[]{:S(2)}, u32[]{:S(2)}) %all-to-all-start.4) | async-done | bytes 524320 | tf_op jit(solution)/shard_map/all_to_all | solution.py:387
  157.2 2.0 %total.1 = (f32[128,256]{1,0:T(8,128)}, f32[8,8,128]{2,1,0:T(8,128)}) custom-call(bf16[8,128,256]{2,1,0:T(8,128)(2,1)} %copy-done.1, bf16[128,256]{1,0:T(8,128)(2,1)} %dynamic-slice_bitcast_fusion.own_ref), custom_call_target="tpu_custom_call" | custom-call | tf_op jit(solution)/shard_map/total/pallas_call | solution.py:393
  159.3 9.4 %all_to_all.33.moments_ref = f32[8,8,128]{2,1,0:T(8,128)} all-to-all(f32[8,8,128]{2,1,0:T(8,128)} %get-tuple-element.33), channel_id=1, replica_groups=mesh['z'=16,'ya'=2,'yb'=2,'x'=4,'c'=2] {'x','c'}, dimensions={0} | all-to-all | bytes 65536 | tf_op jit(solution)/shard_map/all_to_all | solution.py:406
  (52 shorter events, 11.8 us)
Async XLA Ops:
  6.5 122.4 %all-gather.3.cloned.1.call-start = ((), (), s32[]{:S(2)}) async-start(), calls=%async_computation.6 | async-start | bytes 5013504 | tf_op jit(solution)/shard_map/all_gather | solution.py:144
  7.4 14.6 %copy-start.7 = (bf16[128,256]{1,0:T(8,128)(2,1)S(1)}, bf16[128,256]{1,0:T(8,128)(2,1)}, u32[]{:S(2)}) copy-start(bf16[128,256]{1,0:T(8,128)(2,1)} %param.27) | copy-start | bytes 196612
  7.4 16.9 %copy-start.8 = (f32[256]{0:T(256)S(1)}, f32[256]{0:T(256)}, u32[]{:S(2)}) copy-start(f32[256]{0:T(256)} %param.29) | copy-start | bytes 3076
  7.4 16.9 %copy-start.9 = (f32[256]{0:T(256)S(1)}, f32[256]{0:T(256)}, u32[]{:S(2)}) copy-start(f32[256]{0:T(256)} %param.30) | copy-start | bytes 3076
  7.5 19.7 %copy-start.5 = (bf16[1024,256]{1,0:T(8,128)(2,1)S(1)}, bf16[1024,256]{1,0:T(8,128)(2,1)}, u32[]{:S(2)}) copy-start(bf16[1024,256]{1,0:T(8,128)(2,1)} %param.28) | copy-start | bytes 1572868
  22.0 16.0 %copy-start.6 = (bf16[64,8,128]{2,1,0:T(8,128)(2,1)S(1)}, bf16[64,8,128]{2,1,0:T(8,128)(2,1)}, u32[]{:S(2)}) copy-start(bf16[64,8,128]{2,1,0:T(8,128)(2,1)} %get-tuple-element.21) | copy-start | bytes 393220
  22.0 5.1 %collective-permute-start = (bf16[128,256]{1,0:T(8,128)(2,1)S(1)}, bf16[128,256]{1,0:T(8,128)(2,1)S(1)}, u32[]{:S(2)}, u32[]{:S(2)}) collective-permute-start(bf16[128,256]{1,0:T(8,128)(2,1)S(1)} %copy-done.7), channel_id=1, source_target_pairs={{0,8},{8,0},{1,9},{9,1},{2,10},{10,2},{3,11},{11,3},{4,12},{12,4},... | collective-permute-start | bytes 196616 | tf_op jit(solution)/shard_map/ppermute | solution.py:160
  27.2 96.1 %copy-start = (bf16[1296,256]{1,0:T(8,128)(2,1)}, bf16[1296,256]{1,0:T(8,128)(2,1)S(1)}, u32[]{:S(2)}) copy-start(bf16[1296,256]{1,0:T(8,128)(2,1)S(1)} %fusion.1.refs_0_) | copy-start | bytes 1990660
  27.2 45.0 %collective-permute-start.1 = (bf16[1296,256]{1,0:T(8,128)(2,1)S(1)}, bf16[1296,256]{1,0:T(8,128)(2,1)S(1)}, u32[]{:S(2)}, u32[]{:S(2)}) collective-permute-start(bf16[1296,256]{1,0:T(8,128)(2,1)S(1)} %fusion.1.refs_0_), channel_id=1, source_target_pairs={{0,2},{2,4},{4,6},{6,0},{1,3},{3,5},{5,7},{7,1},{8,10},{10,12},{12... | collective-permute-start | bytes 1990664 | tf_op jit(solution)/shard_map/ppermute | solution.py:173
  30.5 41.7 %collective-permute-start.2 = (bf16[1296,256]{1,0:T(8,128)(2,1)S(1)}, bf16[1296,256]{1,0:T(8,128)(2,1)S(1)}, u32[]{:S(2)}, u32[]{:S(2)}) collective-permute-start(bf16[1296,256]{1,0:T(8,128)(2,1)S(1)} %fusion.1.refs_0_), channel_id=1, source_target_pairs={{0,4},{2,6},{4,0},{6,2},{1,5},{3,7},{5,1},{7,3},{8,12},{10,14},{12... | collective-permute-start | bytes 1990664 | tf_op jit(solution)/shard_map/ppermute | solution.py:173
  34.9 37.3 %collective-permute-start.3 = (bf16[1296,256]{1,0:T(8,128)(2,1)S(1)}, bf16[1296,256]{1,0:T(8,128)(2,1)S(1)}, u32[]{:S(2)}, u32[]{:S(2)}) collective-permute-start(bf16[1296,256]{1,0:T(8,128)(2,1)S(1)} %fusion.1.refs_0_), channel_id=1, source_target_pairs={{0,6},{2,0},{4,2},{6,4},{1,7},{3,1},{5,3},{7,5},{8,14},{10,8},{12,... | collective-permute-start | bytes 1990664 | tf_op jit(solution)/shard_map/ppermute | solution.py:173
  72.2 51.2 %copy-start.2 = (bf16[1296,256]{1,0:T(8,128)(2,1)}, bf16[1296,256]{1,0:T(8,128)(2,1)S(1)}, u32[]{:S(2)}) copy-start(bf16[1296,256]{1,0:T(8,128)(2,1)S(1)} %collective-permute-done.1.refs_2_) | copy-start | bytes 1990660
  72.2 51.2 %copy-start.3 = (bf16[1296,256]{1,0:T(8,128)(2,1)}, bf16[1296,256]{1,0:T(8,128)(2,1)S(1)}, u32[]{:S(2)}) copy-start(bf16[1296,256]{1,0:T(8,128)(2,1)S(1)} %collective-permute-done.2.refs_4_) | copy-start | bytes 1990660
  72.2 51.2 %copy-start.4 = (bf16[1296,256]{1,0:T(8,128)(2,1)}, bf16[1296,256]{1,0:T(8,128)(2,1)S(1)}, u32[]{:S(2)}) copy-start(bf16[1296,256]{1,0:T(8,128)(2,1)S(1)} %collective-permute-done.3.refs_6_) | copy-start | bytes 1990660
  72.2 51.1 %collective-permute-start.4 = (bf16[1296,256]{1,0:T(8,128)(2,1)S(1)}, bf16[1296,256]{1,0:T(8,128)(2,1)}, u32[]{:S(2)}, u32[]{:S(2)}) collective-permute-start(bf16[1296,256]{1,0:T(8,128)(2,1)S(1)} %fusion.1.refs_0_), channel_id=1, source_target_pairs={{0,1},{1,0},{2,3},{3,2},{4,5},{5,4},{6,7},{7,6},{8,9},{9,8},{10,11... | collective-permute-start | bytes 1990664 | tf_op jit(solution)/shard_map/ppermute | solution.py:380
  80.1 43.2 %collective-permute-start.5 = (bf16[1296,256]{1,0:T(8,128)(2,1)S(1)}, bf16[1296,256]{1,0:T(8,128)(2,1)}, u32[]{:S(2)}, u32[]{:S(2)}) collective-permute-start(bf16[1296,256]{1,0:T(8,128)(2,1)S(1)} %collective-permute-done.1.refs_2_), channel_id=1, source_target_pairs={{0,1},{1,0},{2,3},{3,2},{4,5},{5,4},{6,7},{7,6},{8,9},{9,8},{10,11... | collective-permute-start | bytes 1990664 | tf_op jit(solution)/shard_map/ppermute | solution.py:380
  82.0 41.3 %collective-permute-start.6 = (bf16[1296,256]{1,0:T(8,128)(2,1)S(1)}, bf16[1296,256]{1,0:T(8,128)(2,1)}, u32[]{:S(2)}, u32[]{:S(2)}) collective-permute-start(bf16[1296,256]{1,0:T(8,128)(2,1)S(1)} %collective-permute-done.2.refs_4_), channel_id=1, source_target_pairs={{0,1},{1,0},{2,3},{3,2},{4,5},{5,4},{6,7},{7,6},{8,9},{9,8},{10,11... | collective-permute-start | bytes 1990664 | tf_op jit(solution)/shard_map/ppermute | solution.py:380
  84.5 38.9 %collective-permute-start.7 = (bf16[1296,256]{1,0:T(8,128)(2,1)S(1)}, bf16[1296,256]{1,0:T(8,128)(2,1)}, u32[]{:S(2)}, u32[]{:S(2)}) collective-permute-start(bf16[1296,256]{1,0:T(8,128)(2,1)S(1)} %collective-permute-done.3.refs_6_), channel_id=1, source_target_pairs={{0,1},{1,0},{2,3},{3,2},{4,5},{5,4},{6,7},{7,6},{8,9},{9,8},{10,11... | collective-permute-start | bytes 1990664 | tf_op jit(solution)/shard_map/ppermute | solution.py:380
  108.3 9.6 %all-to-all-start.2 = ((bf16[8,128,128]{2,1,0:T(8,128)(2,1)}), bf16[8,128,128]{2,1,0:T(8,128)(2,1)S(1)}, u32[]{:S(2)}, u32[]{:S(2)}) async-start(bf16[8,128,128]{2,1,0:T(8,128)(2,1)} %gated.1), calls=%async_computation.2 | async-start | bytes 524288 | tf_op jit(solution)/shard_map/all_to_all | solution.py:382
  136.8 4.0 %collective-permute-start.8 = (bf16[2,4,128,256]{3,2,1,0:T(8,128)(2,1)}, bf16[2,4,128,256]{3,2,1,0:T(8,128)(2,1)S(1)}, u32[]{:S(2)}, u32[]{:S(2)}) collective-permute-start(bf16[2,4,128,256]{3,2,1,0:T(8,128)(2,1)} %get-tuple-element.32), channel_id=1, source_target_pairs={{0,1},{1,0},{2,3},{3,2},{4,5},{5,4},{6,7},{7,6},{8,9},{9,8},{10,11... | collective-permute-start | bytes 1572872 | tf_op jit(solution)/shard_map/ppermute | solution.py:385
  142.7 13.7 %all-to-all-start.4 = ((bf16[8,128,256]{2,1,0:T(8,128)(2,1)}), bf16[8,128,256]{2,1,0:T(8,128)(2,1)S(1)}, u32[]{:S(2)}, u32[]{:S(2)}) async-start(bf16[8,128,256]{2,1,0:T(8,128)(2,1)} %bitcast.23), calls=%async_computation.4 | async-start | bytes 1048576 | tf_op jit(solution)/shard_map/all_to_all | solution.py:387
  156.4 0.8 copy-start.1
Sparse Core Ops, SparseCore 0:
  19.1 82.6 all-gather.2

commit v4 on v3

--- a/solution.py
+++ b/solution.py
@@ -227,85 +227,129 @@
     )(place.astype(jnp.int32), gated, *blocks)
 
 
-def feed_kernel(
-    steps, core_ref, rows_ref, enter_ref, leave_ref, keep_ref, send_ref, gate_ref, up_ref, hidden_ref
+def leaving(hidden, down):
+    wide = down.reshape(-1, down.shape[-1])
+    return lax.dot_general(
+        hidden, wide, (((1,), (1,)), ((), ())), preferred_element_type=jnp.float32
+    )
+
+
+def enter_kernel(
+    core_ref, rows_ref, weights_ref, send_ref, hidden_ref, enter_ref, leave_ref, enter_sem, leave_sem
 ):
-    phase, step = pl.program_id(0), pl.program_id(1)
-
-    @pl.when(jnp.logical_and(phase == 0, step == 0))
-    def _():
-        gate_ref[...] = jnp.zeros_like(gate_ref)
-        up_ref[...] = jnp.zeros_like(up_ref)
-
-    @pl.when(phase == 0)
-    def _():
-        for to_ref, kind in ((gate_ref, 0), (up_ref, 1)):
-            product = 0.0
-            for b in range(rows_ref.shape[0]):
-                wide = jnp.concatenate([enter_ref[2 * b, kind], enter_ref[2 * b + 1, kind]], axis=0)
-                product += jnp.dot(rows_ref[b], wide, preferred_element_type=jnp.float32)
-            to_ref[...] += product
-
-    @pl.when(jnp.logical_and(phase == 0, step == steps - 1))
-    def _():
-        gate = gate_ref[...]
-        hidden_ref[...] = (gate / (1.0 + jnp.exp(-gate)) * up_ref[...]).astype(jnp.bfloat16)
-
-    @pl.when(phase == 1)
-    def _():
-        core = core_ref[0]
-        for to_ref, b in ((keep_ref, core), (send_ref, 1 - core)):
-            down = jnp.concatenate([leave_ref[2 * b, 0], leave_ref[2 * b + 1, 0]], axis=0)
-            product = lax.dot_general(
-                hidden_ref[...],
-                down,
-                (((1,), (1,)), ((), ())),
-                preferred_element_type=jnp.float32,
-            ).astype(jnp.bfloat16)
-            for pair in range(2):
-                rows = to_ref.shape[2]
-                to_ref[pair, 0] = product[pair * rows : (pair + 1) * rows]
-
-
-def feed_forward(rows, weights):
+    parts, blocks = 4, 4
+    each = enter_ref.shape[0] // parts
+    copies = []
+    for s in range(parts):
+        copies.append(
+            pltpu.make_async_copy(
+                weights_ref.at[pl.ds(s * each, each), pl.ds(0, 2)],
+                enter_ref.at[pl.ds(s * each, each)],
+                enter_sem.at[s],
+            )
+        )
+    for copy in copies:
+        copy.start()
+    other = 1 - core_ref[0]
+    downs = []
+    for s in range(blocks):
+        downs.append(
+            pltpu.make_async_copy(
+                weights_ref.at[pl.ds(4 * s + 2 * other, 2), 2],
+                leave_ref.at[pl.ds(2 * s, 2)],
+                leave_sem.at[s],
+            )
+        )
+    for copy in downs:
+        copy.start()
+    gate = up = 0.0
+    for s in range(parts):
+        x = jnp.concatenate([rows_ref[2 * s], rows_ref[2 * s + 1]], axis=1)
+        copies[s].wait()
+        wide = [enter_ref[s * each : (s + 1) * each, kind].reshape(-1, HALF) for kind in range(2)]
+        gate += jnp.dot(x, wide[0], preferred_element_type=jnp.float32)
+        up += jnp.dot(x, wide[1], preferred_element_type=jnp.float32)
+    hidden = (gate / (1.0 + jnp.exp(-gate)) * up).astype(jnp.bfloat16)
+    hidden_ref[...] = hidden
+    rows = send_ref.shape[2]
+    for s in range(blocks):
+        downs[s].wait()
+        product = leaving(hidden, leave_ref[2 * s : 2 * s + 2]).astype(jnp.bfloat16)
+        send_ref[0, s] = product[:rows]
+        send_ref[1, s] = product[rows:]
+
+
+def leave_kernel(core_ref, other_ref, hidden_ref, weights_ref, out_ref, leave_ref, leave_sem):
+    blocks = 4
+    copies = []
+    for s in range(blocks):
+        copies.append(
+            pltpu.make_async_copy(
+                weights_ref.at[pl.ds(4 * s + 2 * core_ref[0], 2), 2],
+                leave_ref.at[pl.ds(2 * s, 2)],
+                leave_sem.at[s],
+            )
+        )
+    for copy in copies:
+        copy.start()
+    hidden = hidden_ref[...]
+    rows = out_ref.shape[2]
+    for s in range(blocks):
+        copies[s].wait()
+        product = leaving(hidden, leave_ref[2 * s : 2 * s + 2])
+        for pair in range(2):
+            mine = product[pair * rows : (pair + 1) * rows]
+            out_ref[pair, s] = (mine + other_ref[pair, s].astype(jnp.float32)).astype(jnp.bfloat16)
+
+
+SMEM = pl.BlockSpec(memory_space=pltpu.SMEM)
+VMEM = pl.BlockSpec(memory_space=pltpu.VMEM)
+ANY = pl.BlockSpec(memory_space=pl.ANY)
+
+
+def feed_enter(core, rows, weights):
     blocks, count, width = rows.shape
-    each = 2
-    steps = blocks // each
-    out = jax.ShapeDtypeStruct((2, steps, count // 2, width), jnp.bfloat16)
-    out_spec = pl.BlockSpec(
-        (2, 1, count // 2, width), lambda p, s, c: (0, jnp.where(p == 0, 0, s), 0, 0)
-    )
-    return pl.pallas_call(
-        lambda *refs: feed_kernel(steps, *refs),
-        grid_spec=pltpu.PrefetchScalarGridSpec(
-            num_scalar_prefetch=1,
-            grid=(2, steps),
-            in_specs=[
-                pl.BlockSpec(
-                    (each, count, width), lambda p, s, c: (jnp.where(p == 0, s, steps - 1), 0, 0)
-                ),
-                pl.BlockSpec(
-                    (2 * each, 2, 128, HALF),
-                    lambda p, s, c: (jnp.where(p == 0, s, steps - 1), 0, 0, 0),
-                ),
-                pl.BlockSpec(
-                    (2 * each, 1, 128, HALF), lambda p, s, c: (jnp.where(p == 0, 0, s), 2, 0, 0)
-                ),
-            ],
-            out_specs=[out_spec, out_spec],
-            scratch_shapes=[
-                pltpu.VMEM((count, HALF), jnp.float32),
-                pltpu.VMEM((count, HALF), jnp.float32),
-                pltpu.VMEM((count, HALF), jnp.bfloat16),
-            ],
+    return pl.pallas_call(
+        enter_kernel,
+        in_specs=[SMEM, VMEM, ANY],
+        out_specs=[VMEM, VMEM],
+        out_shape=[
+            jax.ShapeDtypeStruct((2, blocks // 2, count // 2, width), jnp.bfloat16),
+            jax.ShapeDtypeStruct((count, HALF), jnp.bfloat16),
+        ],
+        scratch_shapes=[
+            pltpu.VMEM((16, 2, 128, HALF), jnp.bfloat16),
+            pltpu.VMEM((8, 128, HALF), jnp.bfloat16),
+            pltpu.SemaphoreType.DMA((4,)),
+            pltpu.SemaphoreType.DMA((4,)),
+        ],
+        cost_estimate=pl.CostEstimate(
+            flops=5 * count * D * HALF, bytes_accessed=5 * D * HALF, transcendentals=count * HALF
         ),
-        out_shape=[out, out],
-        compiler_params=pltpu.CompilerParams(dimension_semantics=("arbitrary", "arbitrary")),
+        name="feed_enter",
+    )(core, rows, weights)
+
+
+def feed_leave(core, other, hidden, weights):
+    return pl.pallas_call(
+        leave_kernel,
+        in_specs=[SMEM, VMEM, VMEM, ANY],
+        out_specs=VMEM,
+        out_shape=jax.ShapeDtypeStruct(other.shape, jnp.bfloat16),
+        scratch_shapes=[
+            pltpu.VMEM((8, 128, HALF), jnp.bfloat16),
+            pltpu.SemaphoreType.DMA((4,)),
+        ],
         cost_estimate=pl.CostEstimate(
-            flops=6 * count * D * HALF, bytes_accessed=6 * D * HALF, transcendentals=count * HALF
+            flops=hidden.shape[0] * D * HALF, bytes_accessed=D * HALF, transcendentals=0
         ),
-        name="feed_forward",
-    )(lax.axis_index("c").astype(jnp.int32)[None], rows, weights, weights)
+        name="feed_leave",
+    )(core, other, hidden, weights)
+
+
+def diagonal_of(rows):
+    at = lax.broadcasted_iota(jnp.int32, (rows, rows), 0)
+    return (at == lax.broadcasted_iota(jnp.int32, (rows, rows), 1)).astype(jnp.float32)
 
 
 def total_kernel(arrived_ref, own_ref, before_ref, moments_ref):
@@ -314,10 +358,12 @@
         feed = feed + arrived_ref[peer].astype(jnp.float32)
     before = alpha_mix * own_ref[...].astype(jnp.float32) + feed
     before_ref[...] = before
-    ones = jnp.ones((8, before.shape[1]), jnp.float32)
-    sums = exact_dot(ones, before, ((1,), (1,)))
-    squares = exact_dot(ones, before * before, ((1,), (1,)))
-    moments = jnp.concatenate([sums[0:4], squares[0:4]], axis=0)
+    diagonal = diagonal_of(before.shape[0])
+    moments = []
+    for value in (before, before * before):
+        column = jnp.sum(value, axis=1, keepdims=True)
+        moments.append(jnp.sum(diagonal * column, axis=0, keepdims=True))
+    moments = jnp.concatenate(moments, axis=1)
     for peer in range(moments_ref.shape[0]):
         moments_ref[peer] = moments
 
@@ -326,14 +372,12 @@
     moments = moments_ref[0]
     for peer in range(1, moments_ref.shape[0]):
         moments = moments + moments_ref[peer]
-    mean = moments[0:1] / D
-    spread = moments[4:5] / D - mean * mean
-    scale = lax.rsqrt(spread + norm_eps)
-    rows, _ = before_ref.shape
-    at = lax.broadcasted_iota(jnp.int32, (rows, rows), 0)
-    diagonal = (at == lax.broadcasted_iota(jnp.int32, (rows, rows), 1)).astype(jnp.float32)
+    rows = before_ref.shape[0]
+    mean = moments[:, :rows] / D
+    spread = moments[:, rows:] / D - mean * mean
+    diagonal = diagonal_of(rows)
     column = jnp.sum(diagonal * mean, axis=1, keepdims=True)
-    factor = jnp.sum(diagonal * scale, axis=1, keepdims=True)
+    factor = jnp.sum(diagonal * lax.rsqrt(spread + norm_eps), axis=1, keepdims=True)
     out_ref[...] = ((before_ref[...] - column) * factor * gain_ref[...] + bias_ref[...]).astype(
         jnp.bfloat16
     )
@@ -373,17 +417,19 @@
     packed, output_matrix, residual = lax.optimization_barrier((packed, output_matrix, residual))
     arrived = lax.all_to_all(packed, SP, 0, 0, tiled=True)
     blocks = spread_over_x(output_matrix, residual, inner_norm_gain, inner_norm_bias)
-    before, *blocks = lax.optimization_barrier((scanned(arrived), *blocks))
+    before = scanned(arrived)
     back = lax.all_to_all(before, SP, 0, 0, tiled=True)
+    gated = gated_rows(back, inner, queries, per_head_gain, output_gate_logits, 8)
+    everyone = lax.all_to_all(gated, ("yb", "x"), 0, 0, tiled=True)
+    everyone = lax.all_gather(everyone, "c")
     both = []
     for block in blocks:
         both += [block, lax.ppermute(block, "c", SWAP)]
-    gated = gated_rows(back, inner, queries, per_head_gain, output_gate_logits, 8)
-    everyone = lax.all_gather(lax.all_to_all(gated, ("yb", "x"), 0, 0, tiled=True), "c")
     middle = middle_rows(everyone, both)
-    keep, send = feed_forward(middle, weights)
-    joined = keep.astype(jnp.float32) + lax.ppermute(send, "c", SWAP).astype(jnp.float32)
-    joined = joined.astype(jnp.bfloat16).reshape(-1, *keep.shape[2:])
+    core = lax.axis_index("c").astype(jnp.int32)[None]
+    send, hidden = feed_enter(core, middle, weights)
+    joined = feed_leave(core, lax.ppermute(send, "c", SWAP), hidden, weights)
+    joined = joined.reshape(-1, *joined.shape[2:])
     shares = lax.all_to_all(joined, ("yb", "x"), 0, 0, tiled=True)
     own = lax.dynamic_slice(
         middle,
@@ -394,7 +440,7 @@
         total_kernel,
         out_shape=[
             jax.ShapeDtypeStruct(own.shape, jnp.float32),
-            jax.ShapeDtypeStruct((8, 8, rows), jnp.float32),
+            jax.ShapeDtypeStruct((8, 1, 2 * rows), jnp.float32),
         ],
         name="total",
     )(shares, own)

time: 178 us -> 174 us (0.978)
  blocking collectives: 77.8 us -> 52 us
  starting transfers between devices: 36.3 us -> 52.1 us
  waiting for transfers between devices: 18.6 us -> 22.5 us
  Pallas kernels: 23.9 us -> 26.4 us
  other arithmetic: 2.96 us -> 0.99 us
    all_to_all x1 -> x0, blocking collectives: 32.5 us -> none  [layer(): arrived = lax.all_to_all(packed, SP, 0, 0, tiled=True)]
    all_to_all x1 -> x2, starting transfers between devices: 3.41 us -> 21 us  [the longest x1 16.6 us: layer(): arrived = lax.all_to_all(packed, SP, 0, 0, tiled=True)]
    all_to_all x1, blocking collectives: 19.8 us -> 27.6 us  [layer(): back = lax.all_to_all(before, SP, 0, 0, tiled=True)]
    all_to_all x1 -> x2, waiting for transfers between devices: 5.49 us -> 9.39 us  [the longest x1 5.65 us: layer(): everyone = lax.all_to_all(gated, ('yb', 'x'), 0, 0, tiled=True)]
    pallas_call x1 -> x2, Pallas kernels: 7.79 us -> 10.6 us  [the longest x1 6.43 us: feed_enter(): pl.pallas_call(enter_kernel, in_specs=[SMEM, VMEM, ANY], out_specs=[VMEM,...]
    convert_element_type x1 -> x0, other arithmetic: 1.97 us -> none  [layer(): joined = joined.astype(jnp.bfloat16).reshape(-1, *keep.shape[2:])]
  transfers between devices with their start and end apart: 12 -> 13, of which waited for: 4 -> 5; matrix products, arithmetic and copies ran while one was open for 1% -> 1% of each run, Pallas kernels for 7% -> 7%
where the time goes in v4:
time: 174 us; the launch traced here: 173 us
  starting transfers between devices  52.1 us (30%)
  blocking collectives  52 us (30%)
  Pallas kernels  26.4 us (15%)
  waiting for transfers between devices  22.5 us (13%)
  between operations  13.8 us (8%)
  local copies, waits for them, and re-layouts  5.29 us (3%)
    all_to_all x1, blocking collectives, layer(): back = lax.all_to_all(before, SP, 0, 0, tiled=True)  27.6 us
    all_to_all x1, starting transfers between devices, layer(): arrived = lax.all_to_all(packed, SP, 0, 0, tiled=True)  16.6 us
    ppermute x4, starting transfers between devices, layer(): both += [block, lax.ppermute(block, 'c', SWAP)]  12.4 us
    ppermute x3, starting transfers between devices, spread_over_x(): lax.ppermute(block, 'x', [(i, (i + k) % count) for i in range(count)])  10.7 us
    all_to_all x1, blocking collectives, gathered_weights(): arrived = lax.all_to_all(halves, ('ya', 'yb'), 0, 0, tiled=True)  10.6 us
    all_to_all x1, blocking collectives, layer(): lax.all_to_all(moments, TP, 0, 0, tiled=True)  9.32 us
    all_to_all x1, waiting for transfers between devices, layer(): shares = lax.all_to_all(joined, ('yb', 'x'), 0, 0, tiled=True)  8.7 us
    pallas_call x1, Pallas kernels, feed_enter(): pl.pallas_call(enter_kernel, in_specs=[SMEM, VMEM, ANY], out_specs=[VMEM,...  6.43 us
  transfers between devices with their start and end apart: 13, of which 5 were waited for; matrix products, arithmetic and copies ran while one was open for 1% of the time, Pallas kernels for 7%

profile of v4, /device:TPU:1, one launch (start us, length us, event | category | flops | bytes accessed | tf_op | source)
XLA Modules:
  0.0 173.2 jit_solution(12931221314321687603)
XLA Ops:
  7.6 10.6 %all_to_all.30 = bf16[4,3,32,384]{3,2,1,0:T(8,128)(2,1)S(1)} all-to-all(bf16[4,3,32,384]{3,2,1,0:T(8,128)(2,1)S(1)} %pad_maximum_fusion), channel_id=1, replica_groups=mesh['z'=16,'ya'=2,'yb'=2,'x'=4,'c'=2] {'ya','yb'}, dimensions={0} | all-to-all | bytes 589824 | tf_op jit(solution)/shard_map/all_to_all | solution.py:142
  19.0 3.0 %local.1 = (f32[128,128]{1,0:T(8,128)}, f32[128,256]{1,0:T(8,128)}, bf16[64,8,128]{2,1,0:T(8,128)(2,1)}) custom-call(bf16[128,128]{1,0:T(8,128)(2,1)} %query_ref.1, bf16[128,128]{1,0:T(8,128)(2,1)} %value_ref.1, bf16[128,128]{1,0:T(8,128)(2,1)} %onward_ref.1, bf16[128,128]{1,0:T(8,128)(2,1)} %reverse_ref.1, f32[1,128]{1,0:T(1,128)} %bitcast.42, ...), custom_call_target="tpu_custom_call" | custom-call | tf_op jit(solution)/shard_map/local/pallas_call | solution.py:77
  22.0 2.2 %collective-permute-start = (bf16[128,256]{1,0:T(8,128)(2,1)S(1)}, bf16[128,256]{1,0:T(8,128)(2,1)S(1)}, u32[]{:S(2)}, u32[]{:S(2)}) collective-permute-start(bf16[128,256]{1,0:T(8,128)(2,1)S(1)} %copy-done.8), channel_id=1, source_target_pairs={{0,8},{8,0},{1,9},{9,1},{2,10},{10,2},{3,11},{11,3},{4,12},{12,4},... | collective-permute-start | bytes 196616 | tf_op jit(solution)/shard_map/ppermute | solution.py:160
  24.3 2.7 %collective-permute-done = bf16[128,256]{1,0:T(8,128)(2,1)S(1)} collective-permute-done((bf16[128,256]{1,0:T(8,128)(2,1)S(1)}, bf16[128,256]{1,0:T(8,128)(2,1)S(1)}, u32[]{:S(2)}, u32[]{:S(2)}) %collective-permute-start) | collective-permute-done | bytes 65568 | tf_op jit(solution)/shard_map/ppermute | solution.py:160
  27.1 3.3 %collective-permute-start.2 = (bf16[1296,256]{1,0:T(8,128)(2,1)S(1)}, bf16[1296,256]{1,0:T(8,128)(2,1)S(1)}, u32[]{:S(2)}, u32[]{:S(2)}) collective-permute-start(bf16[1296,256]{1,0:T(8,128)(2,1)S(1)} %fusion.1.refs_0_), channel_id=1, source_target_pairs={{0,2},{2,4},{4,6},{6,0},{1,3},{3,5},{5,7},{7,1},{8,10},{10,12},{12... | collective-permute-start | bytes 1990664 | tf_op jit(solution)/shard_map/ppermute | solution.py:173
  30.4 4.4 %collective-permute-start.4 = (bf16[1296,256]{1,0:T(8,128)(2,1)S(1)}, bf16[1296,256]{1,0:T(8,128)(2,1)S(1)}, u32[]{:S(2)}, u32[]{:S(2)}) collective-permute-start(bf16[1296,256]{1,0:T(8,128)(2,1)S(1)} %fusion.1.refs_0_), channel_id=1, source_target_pairs={{0,4},{2,6},{4,0},{6,2},{1,5},{3,7},{5,1},{7,3},{8,12},{10,14},{12... | collective-permute-start | bytes 1990664 | tf_op jit(solution)/shard_map/ppermute | solution.py:173
  34.7 3.1 %collective-permute-start.6 = (bf16[1296,256]{1,0:T(8,128)(2,1)S(1)}, bf16[1296,256]{1,0:T(8,128)(2,1)S(1)}, u32[]{:S(2)}, u32[]{:S(2)}) collective-permute-start(bf16[1296,256]{1,0:T(8,128)(2,1)S(1)} %fusion.1.refs_0_), channel_id=1, source_target_pairs={{0,6},{2,0},{4,2},{6,4},{1,7},{3,1},{5,3},{7,5},{8,14},{10,8},{12,... | collective-permute-start | bytes 1990664 | tf_op jit(solution)/shard_map/ppermute | solution.py:173
  37.8 16.6 %all-to-all-start = ((bf16[64,8,128]{2,1,0:T(8,128)(2,1)}), bf16[64,8,128]{2,1,0:T(8,128)(2,1)S(1)}, u32[]{:S(2)}, u32[]{:S(2)}) async-start(bf16[64,8,128]{2,1,0:T(8,128)(2,1)} %get-tuple-element.16), calls=%async_computation | async-start | bytes 262144 | tf_op jit(solution)/shard_map/all_to_all | solution.py:418
  54.4 6.2 %collective-permute-start.1 = (bf16[1296,256]{1,0:T(8,128)(2,1)S(1)}, bf16[1296,256]{1,0:T(8,128)(2,1)}, u32[]{:S(2)}, u32[]{:S(2)}) collective-permute-start(bf16[1296,256]{1,0:T(8,128)(2,1)S(1)} %fusion.1.refs_0_), channel_id=1, source_target_pairs={{0,1},{1,0},{2,3},{3,2},{4,5},{5,4},{6,7},{7,6},{8,9},{9,8},{10,11... | collective-permute-start | bytes 1990664 | tf_op jit(solution)/shard_map/ppermute | solution.py:427
  60.6 1.9 %collective-permute-start.3 = (bf16[1296,256]{1,0:T(8,128)(2,1)S(1)}, bf16[1296,256]{1,0:T(8,128)(2,1)}, u32[]{:S(2)}, u32[]{:S(2)}) collective-permute-start(bf16[1296,256]{1,0:T(8,128)(2,1)S(1)} %collective-permute-done.2.refs_2_), channel_id=1, source_target_pairs={{0,1},{1,0},{2,3},{3,2},{4,5},{5,4},{6,7},{7,6},{8,9},{9,8},{10,11... | collective-permute-start | bytes 1990664 | tf_op jit(solution)/shard_map/ppermute | solution.py:427
  62.5 2.4 %collective-permute-start.5 = (bf16[1296,256]{1,0:T(8,128)(2,1)S(1)}, bf16[1296,256]{1,0:T(8,128)(2,1)}, u32[]{:S(2)}, u32[]{:S(2)}) collective-permute-start(bf16[1296,256]{1,0:T(8,128)(2,1)S(1)} %collective-permute-done.4.refs_4_), channel_id=1, source_target_pairs={{0,1},{1,0},{2,3},{3,2},{4,5},{5,4},{6,7},{7,6},{8,9},{9,8},{10,11... | collective-permute-start | bytes 1990664 | tf_op jit(solution)/shard_map/ppermute | solution.py:427
  66.9 3.7 %all-to-all-done.refs_0_ = bf16[64,8,128]{2,1,0:T(8,128)(2,1)S(1)} async-done(((bf16[64,8,128]{2,1,0:T(8,128)(2,1)}), bf16[64,8,128]{2,1,0:T(8,128)(2,1)S(1)}, u32[]{:S(2)}, u32[]{:S(2)}) %all-to-all-start) | async-done | bytes 131104 | tf_op jit(solution)/shard_map/all_to_all | solution.py:418
  73.0 27.6 %all_to_all.31.back_ref = bf16[64,4,128]{2,1,0:T(4,128)(2,1)} all-to-all(bf16[64,4,128]{2,1,0:T(4,128)(2,1)} %scan.1), channel_id=1, replica_groups=mesh['z'=16,'ya'=2,'yb'=2,'x'=4,'c'=2] {'z','ya','yb'}, dimensions={0} | all-to-all | bytes 131072 | tf_op jit(solution)/shard_map/all_to_all | solution.py:421
  100.6 2.1 %gated.1 = bf16[8,128,128]{2,1,0:T(8,128)(2,1)} custom-call(bf16[64,4,128]{2,1,0:T(4,128)(2,1)} %all_to_all.31.back_ref, f32[128,128]{1,0:T(8,128)} %get-tuple-element.17.inner_ref, f32[128,256]{1,0:T(8,128)} %get-tuple-element.18.queries_ref, f32[1,128]{1,0:T(1,128)} %bitcast.45, bf16[128,128]{1,0:T(8,128)(2,1)} %gate_ref.1), custom_call_target="tpu_custom_call" | custom-call | tf_op jit(solution)/shard_map/gated/pallas_call | solution.py:105
  102.7 4.5 %all-to-all-start.2 = ((bf16[8,128,128]{2,1,0:T(8,128)(2,1)}), bf16[8,128,128]{2,1,0:T(8,128)(2,1)S(1)}, u32[]{:S(2)}, u32[]{:S(2)}) async-start(bf16[8,128,128]{2,1,0:T(8,128)(2,1)} %gated.1), calls=%async_computation.2 | async-start | bytes 524288 | tf_op jit(solution)/shard_map/all_to_all | solution.py:423
  107.9 5.7 %all-to-all-done.2 = bf16[8,128,128]{2,1,0:T(8,128)(2,1)S(1)} async-done(((bf16[8,128,128]{2,1,0:T(8,128)(2,1)}), bf16[8,128,128]{2,1,0:T(8,128)(2,1)S(1)}, u32[]{:S(2)}, u32[]{:S(2)}) %all-to-all-start.2) | async-done | bytes 262176 | tf_op jit(solution)/shard_map/all_to_all | solution.py:423
  113.5 4.5 %all-gather = bf16[16,128,128]{2,1,0:T(8,128)(2,1)} all-gather(bf16[8,128,128]{2,1,0:T(8,128)(2,1)S(1)} %all-to-all-done.2), channel_id=2, replica_groups=mesh['z'=16,'ya'=2,'yb'=2,'x'=4,'c'=2] {'c'}, dimensions={0}, use_global_device_ids=true | all-gather | bytes 786432 | tf_op jit(solution)/shard_map/all_gather | solution.py:424
  118.1 5.6 %middle.1.rows_ref = bf16[8,256,256]{2,1,0:T(8,128)(2,1)} custom-call(s32[8]{0:T(128)} %stack.79.place_ref, bf16[2,8,128,128]{3,2,1,0:T(8,128)(2,1)} %bitcast.35, bf16[1296,256]{1,0:T(8,128)(2,1)} %copy-done, bf16[1296,256]{1,0:T(8,128)(2,1)} %collective-permute-done.1.refs_1_, bf16[1296,256]{1,0:T(8,128)(2,1)} %copy-done.2, ...), custom_call_target="tpu_custom_call" | custom-call | tf_op jit(solution)/shard_map/middle/pallas_call | solution.py:217
  123.6 6.4 %feed_enter.1 = (bf16[2,4,128,256]{3,2,1,0:T(8,128)(2,1)}, bf16[256,384]{1,0:T(8,128)(2,1)}) custom-call(s32[1]{0:T(128)} %bitcast.core_ref, bf16[8,256,256]{2,1,0:T(8,128)(2,1)} %middle.1.rows_ref, bf16[16,3,128,384]{3,2,1,0:T(8,128)(2,1)} %bitcast.32), custom_call_target="tpu_custom_call" | custom-call | flops 1006632960 | bytes 3932160 | tf_op jit(solution)/shard_map/feed_enter/pallas_call | solution.py:312
  130.1 2.3 %collective-permute-start.8 = (bf16[2,4,128,256]{3,2,1,0:T(8,128)(2,1)}, bf16[2,4,128,256]{3,2,1,0:T(8,128)(2,1)S(1)}, u32[]{:S(2)}, u32[]{:S(2)}) collective-permute-start(bf16[2,4,128,256]{3,2,1,0:T(8,128)(2,1)} %get-tuple-element.21), channel_id=1, source_target_pairs={{0,1},{1,0},{2,3},{3,2},{4,5},{5,4},{6,7},{7,6},{8,9},{9,8},{10,11... | collective-permute-start | bytes 1572872 | tf_op jit(solution)/shard_map/ppermute | solution.py:431
  134.9 4.1 %feed_leave.1 = bf16[2,4,128,256]{3,2,1,0:T(8,128)(2,1)} custom-call(s32[1]{0:T(128)} %bitcast.core_ref, bf16[2,4,128,256]{3,2,1,0:T(8,128)(2,1)} %copy-done.5, bf16[256,384]{1,0:T(8,128)(2,1)} %get-tuple-element.22.hidden_ref, bf16[16,3,128,384]{3,2,1,0:T(8,128)(2,1)} %bitcast.33), custom_call_target="tpu_custom_call" | custom-call | flops 201326592 | bytes 786432 | tf_op jit(solution)/shard_map/feed_leave/pallas_call | solution.py:334
  139.0 3.5 %all-to-all-start.4 = ((bf16[8,128,256]{2,1,0:T(8,128)(2,1)}), bf16[8,128,256]{2,1,0:T(8,128)(2,1)S(1)}, u32[]{:S(2)}, u32[]{:S(2)}) async-start(bf16[8,128,256]{2,1,0:T(8,128)(2,1)} %bitcast.34), calls=%async_computation.4 | async-start | bytes 1048576 | tf_op jit(solution)/shard_map/all_to_all | solution.py:433
  144.0 8.7 %all-to-all-done.4.arrived_ref = bf16[8,128,256]{2,1,0:T(8,128)(2,1)S(1)} async-done(((bf16[8,128,256]{2,1,0:T(8,128)(2,1)}), bf16[8,128,256]{2,1,0:T(8,128)(2,1)S(1)}, u32[]{:S(2)}, u32[]{:S(2)}) %all-to-all-start.4) | async-done | bytes 524320 | tf_op jit(solution)/shard_map/all_to_all | solution.py:433
  155.3 9.3 %all_to_all.32.moments_ref = f32[8,1,256]{2,1,0:T(1,128)} all-to-all(f32[8,1,256]{2,1,0:T(1,128)} %get-tuple-element.23), channel_id=1, replica_groups=mesh['z'=16,'ya'=2,'yb'=2,'x'=4,'c'=2] {'x','c'}, dimensions={0} | all-to-all | bytes 16384 | tf_op jit(solution)/shard_map/all_to_all | solution.py:452
  (55 shorter events, 15.1 us)
Async XLA Ops:
  6.5 117.1 %all-gather.3.cloned.1.call-start = ((), (), s32[]{:S(2)}) async-start(), calls=%async_computation.6 | async-start | bytes 5013504 | tf_op jit(solution)/shard_map/all_gather | solution.py:144
  7.4 14.6 %copy-start.8 = (bf16[128,256]{1,0:T(8,128)(2,1)S(1)}, bf16[128,256]{1,0:T(8,128)(2,1)}, u32[]{:S(2)}) copy-start(bf16[128,256]{1,0:T(8,128)(2,1)} %param.27) | copy-start | bytes 196612
  7.4 16.8 %copy-start.9 = (f32[256]{0:T(256)S(1)}, f32[256]{0:T(256)}, u32[]{:S(2)}) copy-start(f32[256]{0:T(256)} %param.29) | copy-start | bytes 3076
  7.4 16.8 %copy-start.10 = (f32[256]{0:T(256)S(1)}, f32[256]{0:T(256)}, u32[]{:S(2)}) copy-start(f32[256]{0:T(256)} %param.30) | copy-start | bytes 3076
  7.5 19.6 %copy-start.6 = (bf16[1024,256]{1,0:T(8,128)(2,1)S(1)}, bf16[1024,256]{1,0:T(8,128)(2,1)}, u32[]{:S(2)}) copy-start(bf16[1024,256]{1,0:T(8,128)(2,1)} %param.28) | copy-start | bytes 1572868
  22.0 5.0 %collective-permute-start = (bf16[128,256]{1,0:T(8,128)(2,1)S(1)}, bf16[128,256]{1,0:T(8,128)(2,1)S(1)}, u32[]{:S(2)}, u32[]{:S(2)}) collective-permute-start(bf16[128,256]{1,0:T(8,128)(2,1)S(1)} %copy-done.8), channel_id=1, source_target_pairs={{0,8},{8,0},{1,9},{9,1},{2,10},{10,2},{3,11},{11,3},{4,12},{12,4},... | collective-permute-start | bytes 196616 | tf_op jit(solution)/shard_map/ppermute | solution.py:160
  27.1 90.9 %copy-start = (bf16[1296,256]{1,0:T(8,128)(2,1)}, bf16[1296,256]{1,0:T(8,128)(2,1)S(1)}, u32[]{:S(2)}) copy-start(bf16[1296,256]{1,0:T(8,128)(2,1)S(1)} %fusion.1.refs_0_) | copy-start | bytes 1990660
  27.1 33.5 %collective-permute-start.2 = (bf16[1296,256]{1,0:T(8,128)(2,1)S(1)}, bf16[1296,256]{1,0:T(8,128)(2,1)S(1)}, u32[]{:S(2)}, u32[]{:S(2)}) collective-permute-start(bf16[1296,256]{1,0:T(8,128)(2,1)S(1)} %fusion.1.refs_0_), channel_id=1, source_target_pairs={{0,2},{2,4},{4,6},{6,0},{1,3},{3,5},{5,7},{7,1},{8,10},{10,12},{12... | collective-permute-start | bytes 1990664 | tf_op jit(solution)/shard_map/ppermute | solution.py:173
  30.4 32.1 %collective-permute-start.4 = (bf16[1296,256]{1,0:T(8,128)(2,1)S(1)}, bf16[1296,256]{1,0:T(8,128)(2,1)S(1)}, u32[]{:S(2)}, u32[]{:S(2)}) collective-permute-start(bf16[1296,256]{1,0:T(8,128)(2,1)S(1)} %fusion.1.refs_0_), channel_id=1, source_target_pairs={{0,4},{2,6},{4,0},{6,2},{1,5},{3,7},{5,1},{7,3},{8,12},{10,14},{12... | collective-permute-start | bytes 1990664 | tf_op jit(solution)/shard_map/ppermute | solution.py:173
  34.7 30.2 %collective-permute-start.6 = (bf16[1296,256]{1,0:T(8,128)(2,1)S(1)}, bf16[1296,256]{1,0:T(8,128)(2,1)S(1)}, u32[]{:S(2)}, u32[]{:S(2)}) collective-permute-start(bf16[1296,256]{1,0:T(8,128)(2,1)S(1)} %fusion.1.refs_0_), channel_id=1, source_target_pairs={{0,6},{2,0},{4,2},{6,4},{1,7},{3,1},{5,3},{7,5},{8,14},{10,8},{12,... | collective-permute-start | bytes 1990664 | tf_op jit(solution)/shard_map/ppermute | solution.py:173
  37.8 32.8 %all-to-all-start = ((bf16[64,8,128]{2,1,0:T(8,128)(2,1)}), bf16[64,8,128]{2,1,0:T(8,128)(2,1)S(1)}, u32[]{:S(2)}, u32[]{:S(2)}) async-start(bf16[64,8,128]{2,1,0:T(8,128)(2,1)} %get-tuple-element.16), calls=%async_computation | async-start | bytes 262144 | tf_op jit(solution)/shard_map/all_to_all | solution.py:418
  54.4 63.6 %collective-permute-start.1 = (bf16[1296,256]{1,0:T(8,128)(2,1)S(1)}, bf16[1296,256]{1,0:T(8,128)(2,1)}, u32[]{:S(2)}, u32[]{:S(2)}) collective-permute-start(bf16[1296,256]{1,0:T(8,128)(2,1)S(1)} %fusion.1.refs_0_), channel_id=1, source_target_pairs={{0,1},{1,0},{2,3},{3,2},{4,5},{5,4},{6,7},{7,6},{8,9},{9,8},{10,11... | collective-permute-start | bytes 1990664 | tf_op jit(solution)/shard_map/ppermute | solution.py:427
  60.6 57.5 %copy-start.2 = (bf16[1296,256]{1,0:T(8,128)(2,1)}, bf16[1296,256]{1,0:T(8,128)(2,1)S(1)}, u32[]{:S(2)}) copy-start(bf16[1296,256]{1,0:T(8,128)(2,1)S(1)} %collective-permute-done.2.refs_2_) | copy-start | bytes 1990660
  60.6 57.4 %collective-permute-start.3 = (bf16[1296,256]{1,0:T(8,128)(2,1)S(1)}, bf16[1296,256]{1,0:T(8,128)(2,1)}, u32[]{:S(2)}, u32[]{:S(2)}) collective-permute-start(bf16[1296,256]{1,0:T(8,128)(2,1)S(1)} %collective-permute-done.2.refs_2_), channel_id=1, source_target_pairs={{0,1},{1,0},{2,3},{3,2},{4,5},{5,4},{6,7},{7,6},{8,9},{9,8},{10,11... | collective-permute-start | bytes 1990664 | tf_op jit(solution)/shard_map/ppermute | solution.py:427
  62.5 55.5 %copy-start.3 = (bf16[1296,256]{1,0:T(8,128)(2,1)}, bf16[1296,256]{1,0:T(8,128)(2,1)S(1)}, u32[]{:S(2)}) copy-start(bf16[1296,256]{1,0:T(8,128)(2,1)S(1)} %collective-permute-done.4.refs_4_) | copy-start | bytes 1990660
  62.5 55.5 %collective-permute-start.5 = (bf16[1296,256]{1,0:T(8,128)(2,1)S(1)}, bf16[1296,256]{1,0:T(8,128)(2,1)}, u32[]{:S(2)}, u32[]{:S(2)}) collective-permute-start(bf16[1296,256]{1,0:T(8,128)(2,1)S(1)} %collective-permute-done.4.refs_4_), channel_id=1, source_target_pairs={{0,1},{1,0},{2,3},{3,2},{4,5},{5,4},{6,7},{7,6},{8,9},{9,8},{10,11... | collective-permute-start | bytes 1990664 | tf_op jit(solution)/shard_map/ppermute | solution.py:427
  64.9 53.1 %copy-start.4 = (bf16[1296,256]{1,0:T(8,128)(2,1)}, bf16[1296,256]{1,0:T(8,128)(2,1)S(1)}, u32[]{:S(2)}) copy-start(bf16[1296,256]{1,0:T(8,128)(2,1)S(1)} %collective-permute-done.6.refs_6_) | copy-start | bytes 1990660
  65.0 53.1 %collective-permute-start.7 = (bf16[1296,256]{1,0:T(8,128)(2,1)S(1)}, bf16[1296,256]{1,0:T(8,128)(2,1)}, u32[]{:S(2)}, u32[]{:S(2)}) collective-permute-start(bf16[1296,256]{1,0:T(8,128)(2,1)S(1)} %collective-permute-done.6.refs_6_), channel_id=1, source_target_pairs={{0,1},{1,0},{2,3},{3,2},{4,5},{5,4},{6,7},{7,6},{8,9},{9,8},{10,11... | collective-permute-start | bytes 1990664 | tf_op jit(solution)/shard_map/ppermute | solution.py:427
  70.6 0.7 copy-start.7
  102.7 10.8 %all-to-all-start.2 = ((bf16[8,128,128]{2,1,0:T(8,128)(2,1)}), bf16[8,128,128]{2,1,0:T(8,128)(2,1)S(1)}, u32[]{:S(2)}, u32[]{:S(2)}) async-start(bf16[8,128,128]{2,1,0:T(8,128)(2,1)} %gated.1), calls=%async_computation.2 | async-start | bytes 524288 | tf_op jit(solution)/shard_map/all_to_all | solution.py:423
  130.1 4.0 %collective-permute-start.8 = (bf16[2,4,128,256]{3,2,1,0:T(8,128)(2,1)}, bf16[2,4,128,256]{3,2,1,0:T(8,128)(2,1)S(1)}, u32[]{:S(2)}, u32[]{:S(2)}) collective-permute-start(bf16[2,4,128,256]{3,2,1,0:T(8,128)(2,1)} %get-tuple-element.21), channel_id=1, source_target_pairs={{0,1},{1,0},{2,3},{3,2},{4,5},{5,4},{6,7},{7,6},{8,9},{9,8},{10,11... | collective-permute-start | bytes 1572872 | tf_op jit(solution)/shard_map/ppermute | solution.py:431
  134.1 0.8 copy-start.5
  139.0 13.7 %all-to-all-start.4 = ((bf16[8,128,256]{2,1,0:T(8,128)(2,1)}), bf16[8,128,256]{2,1,0:T(8,128)(2,1)S(1)}, u32[]{:S(2)}, u32[]{:S(2)}) async-start(bf16[8,128,256]{2,1,0:T(8,128)(2,1)} %bitcast.34), calls=%async_computation.4 | async-start | bytes 1048576 | tf_op jit(solution)/shard_map/all_to_all | solution.py:433
  152.7 0.8 copy-start.1
Sparse Core Ops, SparseCore 0:
  19.1 82.9 all-gather.2

commit v5 on v4

--- a/solution.py
+++ b/solution.py
@@ -11,6 +11,7 @@
 SP = ("z", "ya", "yb")
 TP = ("x", "c")
 HALF = 384
+QUARTER = 32
 
 highest_precision = lax.Precision.HIGHEST
 alpha_mix = 2.0**0.25
@@ -22,6 +23,11 @@
     return lax.dot_general(
         a, b, (dims, ((), ())), precision=highest_precision, preferred_element_type=jnp.float32
     )
+
+
+def two_terms(x):
+    high = x.astype(jnp.bfloat16).astype(jnp.float32)
+    return high, (x - high).astype(jnp.bfloat16).astype(jnp.float32)
 
 
 def local_kernel(
@@ -38,7 +44,6 @@
     rows_ref,
 ):
     rows, width = query_ref.shape
-    half = width // 2
     logits = query_ref[...].astype(jnp.float32)
     query = logits / (1.0 + jnp.exp(-logits))
     values = value_ref[...].astype(jnp.float32)
@@ -47,6 +52,7 @@
     source = lax.broadcasted_iota(jnp.int32, (rows, rows), 1)
     ones = jnp.ones((rows, width), jnp.float32)
     inner = jnp.zeros_like(query)
+    rows_ref[:, 2 * QUARTER :, :] = jnp.zeros((4, 8, width), jnp.float32)
     for side, (forget_ref, gap_ref, seen, last) in enumerate(
         (
             (onward_ref, onward_gap_ref, at >= source, rows - 1),
@@ -55,44 +61,139 @@
     ):
         seen = seen.astype(jnp.float32)
         keys = gap_ref[...] / (1.0 + jnp.exp(forget_ref[...].astype(jnp.float32)))
-        log_decay = jnp.log1p(-keys)
-        running = exact_dot(seen, log_decay) + exact_dot(seen * extra, ones)
+        running = exact_dot(seen, jnp.log1p(-keys)) + exact_dot(seen * extra, ones)
         total = running[last : last + 1]
         decayed_query = query * jnp.exp(running)
         scores = exact_dot(decayed_query, keys * jnp.exp(-running), ((1,), (1,))) * seen
         inner = inner + exact_dot(scores, values)
         queries_ref[:, width * side : width * (side + 1)] = decayed_query
-        state = exact_dot(keys * jnp.exp(total - running), values, ((0,), (0,)))
-        decay = exact_dot(log_decay, ones, ((0,), (0,))) + jnp.sum(extra)
-        for part in range(2):
-            rows_ref[:, 2 * side + part, :] = state[part * half : (part + 1) * half]
-            rows_ref[:, 4 + 2 * side + part, :] = decay[part * half : (part + 1) * half]
+        state = exact_dot(values, keys * jnp.exp(total - running), ((0,), (0,)))
+        terms = two_terms(total)
+        for y in range(4):
+            rows_ref[y, QUARTER * side : QUARTER * (side + 1), :] = state[
+                QUARTER * y : QUARTER * (y + 1)
+            ]
+            for t in range(2):
+                at_row = 2 * QUARTER + 2 * side + t
+                rows_ref[y, at_row : at_row + 1, :] = terms[t]
     packed_ref[...] = rows_ref[...].astype(jnp.bfloat16)
     inner_ref[...] = inner
 
 
-def local_pass(query, values, onward, reverse, onward_gap, reverse_gap, extra):
-    rows, width = query.shape
-    half = width // 2
+def near(*arrays):
+    return [pltpu.with_memory_space_constraint(a, pltpu.VMEM) for a in arrays]
+
+
+def local_pass(*arrays):
+    rows, width = arrays[0].shape
     return pl.pallas_call(
         local_kernel,
         out_shape=[
-            jax.ShapeDtypeStruct((rows, width), jnp.float32),
-            jax.ShapeDtypeStruct((rows, 2 * width), jnp.float32),
-            jax.ShapeDtypeStruct((half, 8, width), jnp.bfloat16),
+            pltpu.VMEM((rows, width), jnp.float32),
+            pltpu.VMEM((rows, 2 * width), jnp.float32),
+            pltpu.VMEM((4, 2 * QUARTER + 8, width), jnp.bfloat16),
         ],
-        scratch_shapes=[pltpu.VMEM((half, 8, width), jnp.float32)],
+        scratch_shapes=[pltpu.VMEM((4, 2 * QUARTER + 8, width), jnp.float32)],
+        compiler_params=pltpu.CompilerParams(vmem_limit_bytes=6 << 20),
         name="local",
-    )(query, values, onward, reverse, onward_gap[None], reverse_gap[None], extra.reshape(1, rows))
-
-
-def gated_kernel(back_ref, inner_ref, queries_ref, gain_ref, gate_ref, out_ref, states_ref):
-    states_ref[...] = back_ref[...].astype(jnp.float32)
+    )(*near(*arrays))
+
+
+def plane_parts(arrived_ref):
+    parts = []
+    for side in range(2):
+        part = []
+        for y in range(4):
+            block = arrived_ref[y].astype(jnp.float32)
+            decay = block[2 * QUARTER + 2 * side : 2 * QUARTER + 2 * side + 1]
+            decay = decay + block[2 * QUARTER + 2 * side + 1 : 2 * QUARTER + 2 * side + 2]
+            part.append((decay, block[QUARTER * side : QUARTER * (side + 1)]))
+        parts.append(part)
+    return parts
+
+
+def plane_kernel(z_ref, arrived_ref, out_ref, rows_ref):
+    forward, backward = plane_parts(arrived_ref)
+    wholes = []
+    for part in (forward, backward[::-1]):
+        decay, state = part[0]
+        for next_decay, next_state in part[1:]:
+            decay, state = decay + next_decay, jnp.exp(next_decay) * state + next_state
+        wholes.append((decay, state))
+    for side, (decay, state) in enumerate(wholes):
+        rows_ref[side] = jnp.zeros(rows_ref.shape[1:], jnp.float32)
+        rows_ref[side, :QUARTER, :] = state
+        for t, term in enumerate(two_terms(decay)):
+            rows_ref[side, QUARTER + t : QUARTER + t + 1, :] = term
+    ahead, behind = rows_ref[0].astype(jnp.bfloat16), rows_ref[1].astype(jnp.bfloat16)
+    z = z_ref[0]
+    for other in range(out_ref.shape[0]):
+
+        @pl.when(other > z)
+        def _():
+            out_ref[other] = ahead
+
+        @pl.when(other <= z)
+        def _():
+            out_ref[other] = behind
+
+
+def before_kernel(z_ref, planes_ref, arrived_ref, out_ref):
+    z = z_ref[0]
+    planes = planes_ref.shape[0]
+    width = planes_ref.shape[2]
+    states = []
+    for order in (range(planes), reversed(range(planes))):
+        state = jnp.zeros((QUARTER, width), jnp.float32)
+        for other in order:
+            block = planes_ref[other].astype(jnp.float32)
+            decay = block[QUARTER : QUARTER + 1] + block[QUARTER + 1 : QUARTER + 2]
+            passed = other < z if not states else other > z
+            state = jnp.where(passed, jnp.exp(decay) * state + block[:QUARTER], state)
+        states.append(state)
+    forward, backward = plane_parts(arrived_ref)
+    for side, part in enumerate((forward, backward)):
+        state = states[side]
+        for y in range(4) if side == 0 else reversed(range(4)):
+            out_ref[y, QUARTER * side : QUARTER * (side + 1)] = state.astype(jnp.bfloat16)
+            decay, own = part[y]
+            state = jnp.exp(decay) * state + own
+
+
+def states_around(packed):
+    z = lax.axis_index("z").astype(jnp.int32)[None]
+    planes = lax.axis_size("z")
+    width = packed.shape[2]
+    (arrived,) = near(lax.all_to_all(packed, ("ya", "yb"), 0, 0, tiled=True))
+    totals = pl.pallas_call(
+        plane_kernel,
+        in_specs=[SMEM, VMEM],
+        out_specs=VMEM,
+        out_shape=pltpu.VMEM((planes, QUARTER + 8, width), jnp.bfloat16),
+        scratch_shapes=[pltpu.VMEM((2, QUARTER + 8, width), jnp.float32)],
+        compiler_params=pltpu.CompilerParams(vmem_limit_bytes=4 << 20),
+        name="plane",
+    )(z, arrived)
+    (others,) = near(lax.all_to_all(totals, "z", 0, 0, tiled=True))
+    before = pl.pallas_call(
+        before_kernel,
+        in_specs=[SMEM, VMEM, VMEM],
+        out_specs=VMEM,
+        out_shape=pltpu.VMEM((4, 2 * QUARTER, width), jnp.bfloat16),
+        compiler_params=pltpu.CompilerParams(vmem_limit_bytes=4 << 20),
+        name="before",
+    )(z, others, arrived)
+    return lax.all_to_all(before, ("ya", "yb"), 0, 0, tiled=True)
+
+
+def gated_kernel(back_ref, inner_ref, queries_ref, gain_ref, gate_ref, out_ref):
     width = inner_ref.shape[1]
     mixed = inner_ref[...]
     for side in range(2):
-        state = jnp.concatenate([states_ref[:, 2 * side, :], states_ref[:, 2 * side + 1, :]], axis=0)
-        mixed = mixed + exact_dot(queries_ref[:, width * side : width * (side + 1)], state)
+        state = [back_ref[y, QUARTER * side : QUARTER * (side + 1)] for y in range(4)]
+        state = jnp.concatenate([part.astype(jnp.float32) for part in state], axis=0)
+        queries = queries_ref[:, width * side : width * (side + 1)]
+        mixed = mixed + exact_dot(queries, state, ((1,), (1,)))
     mean = jnp.mean(mixed * mixed, axis=1, keepdims=True)
     normed = mixed * lax.rsqrt(mean + head_eps) * gain_ref[...]
     gate = gate_ref[...].astype(jnp.float32)
@@ -101,37 +202,18 @@
         out_ref[peer] = gated
 
 
-def gated_rows(back, inner, queries, gain, gate, peers):
+def gated_rows(*arrays):
     return pl.pallas_call(
         gated_kernel,
-        out_shape=jax.ShapeDtypeStruct((peers, *inner.shape), jnp.bfloat16),
-        scratch_shapes=[pltpu.VMEM(back.shape, jnp.float32)],
+        out_shape=pltpu.VMEM((8, *arrays[1].shape), jnp.bfloat16),
+        compiler_params=pltpu.CompilerParams(vmem_limit_bytes=4 << 20),
         name="gated",
-    )(back, inner, queries, gain[None], gate)
-
-
-def scan_kernel(chunks, local_ref, before_ref):
-    local = local_ref[...].astype(jnp.float32)
-    decay = jnp.exp(local[:, 4:8])
-    state = local[:, 0:4]
-    ahead = [None] * chunks
-    run = jnp.zeros((2, 128), jnp.float32)
-    for c in range(chunks):
-        ahead[c] = run
-        run = decay[c, 0:2] * run + state[c, 0:2]
-    run = jnp.zeros((2, 128), jnp.float32)
-    for c in reversed(range(chunks)):
-        before_ref[c] = jnp.concatenate([ahead[c], run], axis=0).astype(jnp.bfloat16)
-        run = decay[c, 2:4] * run + state[c, 2:4]
-
-
-def scanned(arrived):
-    chunks = arrived.shape[0]
-    return pl.pallas_call(
-        lambda *refs: scan_kernel(chunks, *refs),
-        out_shape=jax.ShapeDtypeStruct((chunks, 4, 128), jnp.bfloat16),
-        name="scan",
-    )(arrived)
+    )(*near(*arrays))
+
+
+SMEM = pl.BlockSpec(memory_space=pltpu.SMEM)
+VMEM = pl.BlockSpec(memory_space=pltpu.VMEM)
+ANY = pl.BlockSpec(memory_space=pl.ANY)
 
 
 def gathered_weights(gate, up, down):
@@ -141,7 +223,8 @@
     halves = jnp.stack([first, second, first, second])
     arrived = lax.all_to_all(halves, ("ya", "yb"), 0, 0, tiled=True)
     shard = jnp.moveaxis(arrived, 0, 1).reshape(3 * 128, HALF)
-    return lax.all_gather(shard, "z", axis=0, tiled=True).reshape(-1, 3, 128, HALF)
+    weights = lax.all_gather(shard, "z", axis=0, tiled=True).reshape(-1, 3, 128, HALF)
+    return pltpu.with_memory_space_constraint(weights, pltpu.HBM)
 
 
 def exact_terms(x):
@@ -218,13 +301,14 @@
         middle_kernel,
         in_specs=[pl.BlockSpec(memory_space=pltpu.SMEM)] + [vmem] * 9,
         out_specs=vmem,
-        out_shape=jax.ShapeDtypeStruct((8, 2 * rows, width), jnp.bfloat16),
+        out_shape=pltpu.VMEM((8, 2 * rows, width), jnp.bfloat16),
         scratch_shapes=[
             pltpu.VMEM((2 * rows, 8 * 128), jnp.bfloat16),
             pltpu.VMEM((8, 2 * rows, width), jnp.float32),
         ],
+        compiler_params=pltpu.CompilerParams(vmem_limit_bytes=14 << 20),
         name="middle",
-    )(place.astype(jnp.int32), gated, *blocks)
+    )(place.astype(jnp.int32), *near(gated), *blocks)
 
 
 def leaving(hidden, down):
@@ -302,11 +386,6 @@
             out_ref[pair, s] = (mine + other_ref[pair, s].astype(jnp.float32)).astype(jnp.bfloat16)
 
 
-SMEM = pl.BlockSpec(memory_space=pltpu.SMEM)
-VMEM = pl.BlockSpec(memory_space=pltpu.VMEM)
-ANY = pl.BlockSpec(memory_space=pl.ANY)
-
-
 def feed_enter(core, rows, weights):
     blocks, count, width = rows.shape
     return pl.pallas_call(
@@ -314,8 +393,8 @@
         in_specs=[SMEM, VMEM, ANY],
         out_specs=[VMEM, VMEM],
         out_shape=[
-            jax.ShapeDtypeStruct((2, blocks // 2, count // 2, width), jnp.bfloat16),
-            jax.ShapeDtypeStruct((count, HALF), jnp.bfloat16),
+            pltpu.VMEM((2, blocks // 2, count // 2, width), jnp.bfloat16),
+            pltpu.VMEM((count, HALF), jnp.bfloat16),
         ],
         scratch_shapes=[
             pltpu.VMEM((16, 2, 128, HALF), jnp.bfloat16),
@@ -326,8 +405,9 @@
         cost_estimate=pl.CostEstimate(
             flops=5 * count * D * HALF, bytes_accessed=5 * D * HALF, transcendentals=count * HALF
         ),
+        compiler_params=pltpu.CompilerParams(vmem_limit_bytes=16 << 20),
         name="feed_enter",
-    )(core, rows, weights)
+    )(core, *near(rows), weights)
 
 
 def feed_leave(core, other, hidden, weights):
@@ -335,7 +415,7 @@
         leave_kernel,
         in_specs=[SMEM, VMEM, VMEM, ANY],
         out_specs=VMEM,
-        out_shape=jax.ShapeDtypeStruct(other.shape, jnp.bfloat16),
+        out_shape=pltpu.VMEM(other.shape, jnp.bfloat16),
         scratch_shapes=[
             pltpu.VMEM((8, 128, HALF), jnp.bfloat16),
             pltpu.SemaphoreType.DMA((4,)),
@@ -343,8 +423,9 @@
         cost_estimate=pl.CostEstimate(
             flops=hidden.shape[0] * D * HALF, bytes_accessed=D * HALF, transcendentals=0
         ),
+        compiler_params=pltpu.CompilerParams(vmem_limit_bytes=8 << 20),
         name="feed_leave",
-    )(core, other, hidden, weights)
+    )(core, *near(other, hidden), weights)
 
 
 def diagonal_of(rows):
@@ -410,16 +491,14 @@
         value_rows,
         onward_forget_logits,
         reverse_forget_logits,
-        onward_floor_gap,
-        reverse_floor_gap,
-        extra_log_decay,
+        onward_floor_gap[None],
+        reverse_floor_gap[None],
+        extra_log_decay.reshape(1, rows),
     )
     packed, output_matrix, residual = lax.optimization_barrier((packed, output_matrix, residual))
-    arrived = lax.all_to_all(packed, SP, 0, 0, tiled=True)
+    back = states_around(packed)
     blocks = spread_over_x(output_matrix, residual, inner_norm_gain, inner_norm_bias)
-    before = scanned(arrived)
-    back = lax.all_to_all(before, SP, 0, 0, tiled=True)
-    gated = gated_rows(back, inner, queries, per_head_gain, output_gate_logits, 8)
+    gated = gated_rows(back, inner, queries, per_head_gain[None], output_gate_logits)
     everyone = lax.all_to_all(gated, ("yb", "x"), 0, 0, tiled=True)
     everyone = lax.all_gather(everyone, "c")
     both = []
@@ -439,21 +518,19 @@
     before_final, moments = pl.pallas_call(
         total_kernel,
         out_shape=[
-            jax.ShapeDtypeStruct(own.shape, jnp.float32),
-            jax.ShapeDtypeStruct((8, 1, 2 * rows), jnp.float32),
+            pltpu.VMEM(own.shape, jnp.float32),
+            pltpu.VMEM((8, 1, 2 * rows), jnp.float32),
         ],
+        compiler_params=pltpu.CompilerParams(vmem_limit_bytes=4 << 20),
         name="total",
-    )(shares, own)
+    )(*near(shares, own))
+    moments = lax.all_to_all(moments, TP, 0, 0, tiled=True)
     return pl.pallas_call(
         closing_kernel,
         out_shape=jax.ShapeDtypeStruct(own.shape, jnp.bfloat16),
+        compiler_params=pltpu.CompilerParams(vmem_limit_bytes=4 << 20),
         name="closing",
-    )(
-        lax.all_to_all(moments, TP, 0, 0, tiled=True),
-        before_final,
-        closing_norm_gain[None],
-        closing_norm_bias[None],
-    )
+    )(*near(moments, before_final, closing_norm_gain[None], closing_norm_bias[None]))
 
 
 def solution(mesh):

time: 174 us -> 152 us (0.87)
  blocking collectives: 52 us -> 36.2 us
  Pallas kernels: 26.4 us -> 16.2 us
  starting transfers between devices: 52.1 us -> 56.2 us
  local copies, waits for them, and re-layouts: 5.29 us -> 2.1 us
  waiting for transfers between devices: 22.5 us -> 24.8 us
    all_to_all x2, blocking collectives: 36.9 us -> 14.7 us  [the longest x1 7.76 us: layer(): moments = lax.all_to_all(moments, TP, 0, 0, tiled=True)]
    all_gather x1, blocking collectives: 4.48 us -> 10.9 us  [layer(): everyone = lax.all_gather(everyone, 'c')]
    pallas_call x4 -> x5, Pallas kernels: 8.66 us -> 4.3 us  [the longest x1 1.96 us: local_pass(): pl.pallas_call(local_kernel, out_shape=[pltpu.VMEM((rows, width), jnp.flo...]
    pallas_call x1, Pallas kernels: 6.43 us -> 4.41 us  [feed_enter(): pl.pallas_call(enter_kernel, in_specs=[SMEM, VMEM, ANY], out_specs=[VMEM,...]
    pallas_call x1, Pallas kernels: 5.57 us -> 3.65 us  [middle_rows(): pl.pallas_call(middle_kernel, in_specs=[pl.BlockSpec(memory_space=pltpu.S...]
    all_to_all x1 -> x2, starting transfers between devices: 16.6 us -> 18.3 us  [the longest x1 15 us: states_around(): others, = near(lax.all_to_all(totals, 'z', 0, 0, tiled=True))]
    all_to_all x1 -> x2, waiting for transfers between devices: 3.73 us -> 4.48 us  [the longest x1 4.48 us: states_around(): arrived, = near(lax.all_to_all(packed, ('ya', 'yb'), 0, 0, tiled=True))]
  transfers between devices with their start and end apart: 13 -> 14, of which waited for: 5 -> 5; matrix products, arithmetic and copies ran while one was open for 1% -> 0% of each run, Pallas kernels for 7% -> 5%
where the time goes in v5:
time: 152 us; the launch traced here: 151 us
  starting transfers between devices  56.2 us (37%)
  blocking collectives  36.2 us (24%)
  waiting for transfers between devices  24.8 us (16%)
  Pallas kernels  16.2 us (11%)
  between operations  14 us (9%)
  local copies, waits for them, and re-layouts  2.1 us (1%)
    all_to_all x1, starting transfers between devices, states_around(): others, = near(lax.all_to_all(totals, 'z', 0, 0, tiled=True))  15 us
    ppermute x4, starting transfers between devices, layer(): both += [block, lax.ppermute(block, 'c', SWAP)]  13.6 us
    all_gather x1, blocking collectives, layer(): everyone = lax.all_gather(everyone, 'c')  10.9 us
    ppermute x3, starting transfers between devices, spread_over_x(): lax.ppermute(block, 'x', [(i, (i + k) % count) for i in range(count)])  10.7 us
    all_to_all x1, blocking collectives, gathered_weights(): arrived = lax.all_to_all(halves, ('ya', 'yb'), 0, 0, tiled=True)  10.6 us
    all_to_all x1, waiting for transfers between devices, layer(): shares = lax.all_to_all(joined, ('yb', 'x'), 0, 0, tiled=True)  10.2 us
    all_to_all x1, blocking collectives, layer(): moments = lax.all_to_all(moments, TP, 0, 0, tiled=True)  7.76 us
    all_to_all x1, blocking collectives, states_around(): return lax.all_to_all(before, ('ya', 'yb'), 0, 0, tiled=True)  6.9 us
  transfers between devices with their start and end apart: 14, of which 5 were waited for; matrix products, arithmetic and copies ran while one was open for 0% of the time, Pallas kernels for 5%

profile of v5, /device:TPU:1, one launch (start us, length us, event | category | flops | bytes accessed | tf_op | source)
XLA Modules:
  0.0 150.6 jit_solution(6113050171856592234)
XLA Ops:
  7.7 10.6 %all_to_all.35 = bf16[4,3,32,384]{3,2,1,0:T(8,128)(2,1)S(1)} all-to-all(bf16[4,3,32,384]{3,2,1,0:T(8,128)(2,1)S(1)} %pad_maximum_fusion), channel_id=1, replica_groups=mesh['z'=16,'ya'=2,'yb'=2,'x'=4,'c'=2] {'ya','yb'}, dimensions={0} | all-to-all | bytes 589824 | tf_op jit(solution)/shard_map/all_to_all | solution.py:224
  19.2 2.0 %local.1 = (f32[128,128]{1,0:T(8,128)S(1)}, f32[128,256]{1,0:T(8,128)S(1)}, bf16[4,72,128]{2,1,0:T(8,128)(2,1)}) custom-call(bf16[128,128]{1,0:T(8,128)(2,1)S(1)} %copy-done.3, bf16[128,128]{1,0:T(8,128)(2,1)S(1)} %copy-done.4, bf16[128,128]{1,0:T(8,128)(2,1)S(1)} %copy-done.5, bf16[128,128]{1,0:T(8,128)(2,1)S(1)} %copy-done.6, f32[1,128]{1,0:T(1,128)S(1)} %bitcast.36, ...), custom_call_target="tpu_custom_call" | custom-call | tf_op jit(solution)/shard_map/local/pallas_call | solution.py:89
  21.1 2.2 %collective-permute-start = (bf16[128,256]{1,0:T(8,128)(2,1)S(1)}, bf16[128,256]{1,0:T(8,128)(2,1)S(1)}, u32[]{:S(2)}, u32[]{:S(2)}) collective-permute-start(bf16[128,256]{1,0:T(8,128)(2,1)S(1)} %copy-done.14), channel_id=1, source_target_pairs={{0,8},{8,0},{1,9},{9,1},{2,10},{10,2},{3,11},{11,3},{4,12},{12,4},... | collective-permute-start | bytes 196616 | tf_op jit(solution)/shard_map/ppermute | solution.py:243
  23.5 2.6 %collective-permute-done = bf16[128,256]{1,0:T(8,128)(2,1)S(1)} collective-permute-done((bf16[128,256]{1,0:T(8,128)(2,1)S(1)}, bf16[128,256]{1,0:T(8,128)(2,1)S(1)}, u32[]{:S(2)}, u32[]{:S(2)}) %collective-permute-start) | collective-permute-done | bytes 65568 | tf_op jit(solution)/shard_map/ppermute | solution.py:243
  26.2 3.3 %collective-permute-start.2 = (bf16[1296,256]{1,0:T(8,128)(2,1)S(1)}, bf16[1296,256]{1,0:T(8,128)(2,1)S(1)}, u32[]{:S(2)}, u32[]{:S(2)}) collective-permute-start(bf16[1296,256]{1,0:T(8,128)(2,1)S(1)} %fusion.1.refs_0_), channel_id=1, source_target_pairs={{0,2},{2,4},{4,6},{6,0},{1,3},{3,5},{5,7},{7,1},{8,10},{10,12},{12... | collective-permute-start | bytes 1990664 | tf_op jit(solution)/shard_map/ppermute | solution.py:256
  29.5 4.4 %collective-permute-start.4 = (bf16[1296,256]{1,0:T(8,128)(2,1)S(1)}, bf16[1296,256]{1,0:T(8,128)(2,1)S(1)}, u32[]{:S(2)}, u32[]{:S(2)}) collective-permute-start(bf16[1296,256]{1,0:T(8,128)(2,1)S(1)} %fusion.1.refs_0_), channel_id=1, source_target_pairs={{0,4},{2,6},{4,0},{6,2},{1,5},{3,7},{5,1},{7,3},{8,12},{10,14},{12... | collective-permute-start | bytes 1990664 | tf_op jit(solution)/shard_map/ppermute | solution.py:256
  33.9 3.1 %collective-permute-start.6 = (bf16[1296,256]{1,0:T(8,128)(2,1)S(1)}, bf16[1296,256]{1,0:T(8,128)(2,1)S(1)}, u32[]{:S(2)}, u32[]{:S(2)}) collective-permute-start(bf16[1296,256]{1,0:T(8,128)(2,1)S(1)} %fusion.1.refs_0_), channel_id=1, source_target_pairs={{0,6},{2,0},{4,2},{6,4},{1,7},{3,1},{5,3},{7,5},{8,14},{10,8},{12,... | collective-permute-start | bytes 1990664 | tf_op jit(solution)/shard_map/ppermute | solution.py:256
  36.9 3.3 %all-to-all-start = ((bf16[4,72,128]{2,1,0:T(8,128)(2,1)}), bf16[4,72,128]{2,1,0:T(8,128)(2,1)S(1)}, u32[]{:S(2)}, u32[]{:S(2)}) async-start(bf16[4,72,128]{2,1,0:T(8,128)(2,1)} %get-tuple-element.16), calls=%async_computation | async-start | bytes 147456 | tf_op jit(solution)/shard_map/all_to_all | solution.py:167
  40.2 4.5 %all-to-all-done.arrived_ref = bf16[4,72,128]{2,1,0:T(8,128)(2,1)S(1)} async-done(((bf16[4,72,128]{2,1,0:T(8,128)(2,1)}), bf16[4,72,128]{2,1,0:T(8,128)(2,1)S(1)}, u32[]{:S(2)}, u32[]{:S(2)}) %all-to-all-start) | async-done | bytes 73760 | tf_op jit(solution)/shard_map/all_to_all | solution.py:167
  45.5 15.0 %all-to-all-start.1 = ((bf16[16,40,128]{2,1,0:T(8,128)(2,1)}), bf16[16,40,128]{2,1,0:T(8,128)(2,1)S(1)}, u32[]{:S(2)}, u32[]{:S(2)}) async-start(bf16[16,40,128]{2,1,0:T(8,128)(2,1)} %plane.1), calls=%async_computation.1 | async-start | bytes 327680 | tf_op jit(solution)/shard_map/all_to_all | solution.py:177
  60.5 7.4 %collective-permute-start.1 = (bf16[1296,256]{1,0:T(8,128)(2,1)S(1)}, bf16[1296,256]{1,0:T(8,128)(2,1)}, u32[]{:S(2)}, u32[]{:S(2)}) collective-permute-start(bf16[1296,256]{1,0:T(8,128)(2,1)S(1)} %fusion.1.refs_0_), channel_id=1, source_target_pairs={{0,1},{1,0},{2,3},{3,2},{4,5},{5,4},{6,7},{7,6},{8,9},{9,8},{10,11... | collective-permute-start | bytes 1990664 | tf_op jit(solution)/shard_map/ppermute | solution.py:506
  67.9 1.9 %collective-permute-start.3 = (bf16[1296,256]{1,0:T(8,128)(2,1)S(1)}, bf16[1296,256]{1,0:T(8,128)(2,1)}, u32[]{:S(2)}, u32[]{:S(2)}) collective-permute-start(bf16[1296,256]{1,0:T(8,128)(2,1)S(1)} %collective-permute-done.2.refs_2_), channel_id=1, source_target_pairs={{0,1},{1,0},{2,3},{3,2},{4,5},{5,4},{6,7},{7,6},{8,9},{9,8},{10,11... | collective-permute-start | bytes 1990664 | tf_op jit(solution)/shard_map/ppermute | solution.py:506
  69.9 2.4 %collective-permute-start.5 = (bf16[1296,256]{1,0:T(8,128)(2,1)S(1)}, bf16[1296,256]{1,0:T(8,128)(2,1)}, u32[]{:S(2)}, u32[]{:S(2)}) collective-permute-start(bf16[1296,256]{1,0:T(8,128)(2,1)S(1)} %collective-permute-done.4.refs_4_), channel_id=1, source_target_pairs={{0,1},{1,0},{2,3},{3,2},{4,5},{5,4},{6,7},{7,6},{8,9},{9,8},{10,11... | collective-permute-start | bytes 1990664 | tf_op jit(solution)/shard_map/ppermute | solution.py:506
  74.4 6.9 %all_to_all.36.back_ref = bf16[4,64,128]{2,1,0:T(8,128)(2,1)S(1)} all-to-all(bf16[4,64,128]{2,1,0:T(8,128)(2,1)S(1)} %before.1), channel_id=1, replica_groups=mesh['z'=16,'ya'=2,'yb'=2,'x'=4,'c'=2] {'ya','yb'}, dimensions={0} | all-to-all | bytes 131072 | tf_op jit(solution)/shard_map/all_to_all | solution.py:186
  82.5 3.4 %all-to-all-start.3 = ((bf16[8,128,128]{2,1,0:T(8,128)(2,1)}), bf16[8,128,128]{2,1,0:T(8,128)(2,1)S(1)}, u32[]{:S(2)}, u32[]{:S(2)}) async-start(bf16[8,128,128]{2,1,0:T(8,128)(2,1)} %gated.1), calls=%async_computation.3 | async-start | bytes 524288 | tf_op jit(solution)/shard_map/all_to_all | solution.py:502
  86.1 5.9 %all-to-all-done.3 = bf16[8,128,128]{2,1,0:T(8,128)(2,1)S(1)} async-done(((bf16[8,128,128]{2,1,0:T(8,128)(2,1)}), bf16[8,128,128]{2,1,0:T(8,128)(2,1)S(1)}, u32[]{:S(2)}, u32[]{:S(2)}) %all-to-all-start.3) | async-done | bytes 262176 | tf_op jit(solution)/shard_map/all_to_all | solution.py:502
  92.0 10.9 %all-gather = bf16[16,128,128]{2,1,0:T(8,128)(2,1)S(1)} all-gather(bf16[8,128,128]{2,1,0:T(8,128)(2,1)S(1)} %all-to-all-done.3), channel_id=2, replica_groups=mesh['z'=16,'ya'=2,'yb'=2,'x'=4,'c'=2] {'c'}, dimensions={0}, use_global_device_ids=true | all-gather | bytes 786432 | tf_op jit(solution)/shard_map/all_gather | solution.py:503
  104.1 3.7 %middle.1.rows_ref = bf16[8,256,256]{2,1,0:T(8,128)(2,1)S(1)} custom-call(s32[8]{0:T(128)S(1)} %stack.79.place_ref, bf16[2,8,128,128]{3,2,1,0:T(8,128)(2,1)S(1)} %bitcast.33, bf16[1296,256]{1,0:T(8,128)(2,1)S(1)} %fusion.1.refs_0_, bf16[1296,256]{1,0:T(8,128)(2,1)} %collective-permute-done.1.refs_1_, bf16[1296,256]{1,0:T(8,128)(2,1)S(1)} %collective-permute-done.2.refs_2_, ...), custom_call_target="tpu_custom_call" | custom-call | tf_op jit(solution)/shard_map/middle/pallas_call | solution.py:300
  107.8 4.4 %feed_enter.1 = (bf16[2,4,128,256]{3,2,1,0:T(8,128)(2,1)S(1)}, bf16[256,384]{1,0:T(8,128)(2,1)S(1)}) custom-call(s32[1]{0:T(128)} %bitcast.core_ref, bf16[8,256,256]{2,1,0:T(8,128)(2,1)S(1)} %middle.1.rows_ref, bf16[16,3,128,384]{3,2,1,0:T(8,128)(2,1)} %bitcast.40), custom_call_target="tpu_custom_call" | custom-call | flops 1006632960 | bytes 3932160 | tf_op jit(solution)/shard_map/feed_enter/pallas_call | solution.py:391
  112.2 3.0 %collective-permute-start.8 = (bf16[2,4,128,256]{3,2,1,0:T(8,128)(2,1)S(1)}, bf16[2,4,128,256]{3,2,1,0:T(8,128)(2,1)S(1)}, u32[]{:S(2)}, u32[]{:S(2)}) collective-permute-start(bf16[2,4,128,256]{3,2,1,0:T(8,128)(2,1)S(1)} %get-tuple-element.21), channel_id=1, source_target_pairs={{0,1},{1,0},{2,3},{3,2},{4,5},{5,4},{6,7},{7,6},{8,9},{9,8},{10,11... | collective-permute-start | bytes 1572872 | tf_op jit(solution)/shard_map/ppermute | solution.py:510
  116.7 3.1 %feed_leave.1 = bf16[2,4,128,256]{3,2,1,0:T(8,128)(2,1)} custom-call(s32[1]{0:T(128)} %bitcast.core_ref, bf16[2,4,128,256]{3,2,1,0:T(8,128)(2,1)S(1)} %collective-permute-done.8.other_ref, bf16[256,384]{1,0:T(8,128)(2,1)S(1)} %get-tuple-element.22.hidden_ref, bf16[16,3,128,384]{3,2,1,0:T(8,128)(2,1)} %bitcast.41), custom_call_target="tpu_custom_call" | custom-call | flops 201326592 | bytes 786432 | tf_op jit(solution)/shard_map/feed_leave/pallas_call | solution.py:414
  119.8 5.1 %all-to-all-start.5 = ((bf16[8,128,256]{2,1,0:T(8,128)(2,1)}), bf16[8,128,256]{2,1,0:T(8,128)(2,1)S(1)}, u32[]{:S(2)}, u32[]{:S(2)}) async-start(bf16[8,128,256]{2,1,0:T(8,128)(2,1)} %bitcast.24), calls=%async_computation.5 | async-start | bytes 1048576 | tf_op jit(solution)/shard_map/all_to_all | solution.py:512
  124.9 10.2 %all-to-all-done.5.arrived_ref = bf16[8,128,256]{2,1,0:T(8,128)(2,1)S(1)} async-done(((bf16[8,128,256]{2,1,0:T(8,128)(2,1)}), bf16[8,128,256]{2,1,0:T(8,128)(2,1)S(1)}, u32[]{:S(2)}, u32[]{:S(2)}) %all-to-all-start.5) | async-done | bytes 524320 | tf_op jit(solution)/shard_map/all_to_all | solution.py:512
  135.3 7.8 %all_to_all.37.moments_ref = f32[8,1,256]{2,1,0:T(1,128)S(1)} all-to-all(f32[8,1,256]{2,1,0:T(1,128)S(1)} %get-tuple-element.23), channel_id=1, replica_groups=mesh['z'=16,'ya'=2,'yb'=2,'x'=4,'c'=2] {'x','c'}, dimensions={0} | all-to-all | bytes 16384 | tf_op jit(solution)/shard_map/all_to_all | solution.py:527
  (70 shorter events, 9.7 us)
Async XLA Ops:
  6.5 101.2 %all-gather.3.cloned.1.call-start = ((), (), s32[]{:S(2)}) async-start(), calls=%async_computation.7 | async-start | bytes 5013504 | tf_op jit(solution)/shard_map/all_gather | solution.py:226
  6.5 12.6 %copy-start.9 = (f32[128]{0:T(128)S(1)}, f32[128]{0:T(128)}, u32[]{:S(2)}) copy-start(f32[128]{0:T(128)} %param.23) | copy-start | bytes 1540
  7.5 13.6 %copy-start.14 = (bf16[128,256]{1,0:T(8,128)(2,1)S(1)}, bf16[128,256]{1,0:T(8,128)(2,1)}, u32[]{:S(2)}) copy-start(bf16[128,256]{1,0:T(8,128)(2,1)} %param.27) | copy-start | bytes 196612
  7.5 15.8 %copy-start.15 = (f32[256]{0:T(256)S(1)}, f32[256]{0:T(256)}, u32[]{:S(2)}) copy-start(f32[256]{0:T(256)} %param.29) | copy-start | bytes 3076
  7.5 15.8 %copy-start.16 = (f32[256]{0:T(256)S(1)}, f32[256]{0:T(256)}, u32[]{:S(2)}) copy-start(f32[256]{0:T(256)} %param.30) | copy-start | bytes 3076
  7.6 18.6 %copy-start.13 = (bf16[1024,256]{1,0:T(8,128)(2,1)S(1)}, bf16[1024,256]{1,0:T(8,128)(2,1)}, u32[]{:S(2)}) copy-start(bf16[1024,256]{1,0:T(8,128)(2,1)} %param.28) | copy-start | bytes 1572868
  21.1 5.0 %collective-permute-start = (bf16[128,256]{1,0:T(8,128)(2,1)S(1)}, bf16[128,256]{1,0:T(8,128)(2,1)S(1)}, u32[]{:S(2)}, u32[]{:S(2)}) collective-permute-start(bf16[128,256]{1,0:T(8,128)(2,1)S(1)} %copy-done.14), channel_id=1, source_target_pairs={{0,8},{8,0},{1,9},{9,1},{2,10},{10,2},{3,11},{11,3},{4,12},{12,4},... | collective-permute-start | bytes 196616 | tf_op jit(solution)/shard_map/ppermute | solution.py:243
  23.5 57.8 %copy-start.2 = (bf16[128,128]{1,0:T(8,128)(2,1)S(1)}, bf16[128,128]{1,0:T(8,128)(2,1)}, u32[]{:S(2)}) copy-start(bf16[128,128]{1,0:T(8,128)(2,1)} %gate_ref.1) | copy-start | bytes 98308
  23.5 57.8 %copy-start.12 = (f32[128]{0:T(128)S(1)}, f32[128]{0:T(128)}, u32[]{:S(2)}) copy-start(f32[128]{0:T(128)} %param.26) | copy-start | bytes 1540
  26.2 41.7 %collective-permute-start.2 = (bf16[1296,256]{1,0:T(8,128)(2,1)S(1)}, bf16[1296,256]{1,0:T(8,128)(2,1)S(1)}, u32[]{:S(2)}, u32[]{:S(2)}) collective-permute-start(bf16[1296,256]{1,0:T(8,128)(2,1)S(1)} %fusion.1.refs_0_), channel_id=1, source_target_pairs={{0,2},{2,4},{4,6},{6,0},{1,3},{3,5},{5,7},{7,1},{8,10},{10,12},{12... | collective-permute-start | bytes 1990664 | tf_op jit(solution)/shard_map/ppermute | solution.py:256
  29.5 40.4 %collective-permute-start.4 = (bf16[1296,256]{1,0:T(8,128)(2,1)S(1)}, bf16[1296,256]{1,0:T(8,128)(2,1)S(1)}, u32[]{:S(2)}, u32[]{:S(2)}) collective-permute-start(bf16[1296,256]{1,0:T(8,128)(2,1)S(1)} %fusion.1.refs_0_), channel_id=1, source_target_pairs={{0,4},{2,6},{4,0},{6,2},{1,5},{3,7},{5,1},{7,3},{8,12},{10,14},{12... | collective-permute-start | bytes 1990664 | tf_op jit(solution)/shard_map/ppermute | solution.py:256
  33.9 38.4 %collective-permute-start.6 = (bf16[1296,256]{1,0:T(8,128)(2,1)S(1)}, bf16[1296,256]{1,0:T(8,128)(2,1)S(1)}, u32[]{:S(2)}, u32[]{:S(2)}) collective-permute-start(bf16[1296,256]{1,0:T(8,128)(2,1)S(1)} %fusion.1.refs_0_), channel_id=1, source_target_pairs={{0,6},{2,0},{4,2},{6,4},{1,7},{3,1},{5,3},{7,5},{8,14},{10,8},{12,... | collective-permute-start | bytes 1990664 | tf_op jit(solution)/shard_map/ppermute | solution.py:256
  36.9 7.8 %all-to-all-start = ((bf16[4,72,128]{2,1,0:T(8,128)(2,1)}), bf16[4,72,128]{2,1,0:T(8,128)(2,1)S(1)}, u32[]{:S(2)}, u32[]{:S(2)}) async-start(bf16[4,72,128]{2,1,0:T(8,128)(2,1)} %get-tuple-element.16), calls=%async_computation | async-start | bytes 147456 | tf_op jit(solution)/shard_map/all_to_all | solution.py:167
  45.5 28.7 %all-to-all-start.1 = ((bf16[16,40,128]{2,1,0:T(8,128)(2,1)}), bf16[16,40,128]{2,1,0:T(8,128)(2,1)S(1)}, u32[]{:S(2)}, u32[]{:S(2)}) async-start(bf16[16,40,128]{2,1,0:T(8,128)(2,1)} %plane.1), calls=%async_computation.1 | async-start | bytes 327680 | tf_op jit(solution)/shard_map/all_to_all | solution.py:177
  60.5 42.4 %collective-permute-start.1 = (bf16[1296,256]{1,0:T(8,128)(2,1)S(1)}, bf16[1296,256]{1,0:T(8,128)(2,1)}, u32[]{:S(2)}, u32[]{:S(2)}) collective-permute-start(bf16[1296,256]{1,0:T(8,128)(2,1)S(1)} %fusion.1.refs_0_), channel_id=1, source_target_pairs={{0,1},{1,0},{2,3},{3,2},{4,5},{5,4},{6,7},{7,6},{8,9},{9,8},{10,11... | collective-permute-start | bytes 1990664 | tf_op jit(solution)/shard_map/ppermute | solution.py:506
  67.9 35.0 %collective-permute-start.3 = (bf16[1296,256]{1,0:T(8,128)(2,1)S(1)}, bf16[1296,256]{1,0:T(8,128)(2,1)}, u32[]{:S(2)}, u32[]{:S(2)}) collective-permute-start(bf16[1296,256]{1,0:T(8,128)(2,1)S(1)} %collective-permute-done.2.refs_2_), channel_id=1, source_target_pairs={{0,1},{1,0},{2,3},{3,2},{4,5},{5,4},{6,7},{7,6},{8,9},{9,8},{10,11... | collective-permute-start | bytes 1990664 | tf_op jit(solution)/shard_map/ppermute | solution.py:506
  69.9 33.1 %collective-permute-start.5 = (bf16[1296,256]{1,0:T(8,128)(2,1)S(1)}, bf16[1296,256]{1,0:T(8,128)(2,1)}, u32[]{:S(2)}, u32[]{:S(2)}) collective-permute-start(bf16[1296,256]{1,0:T(8,128)(2,1)S(1)} %collective-permute-done.4.refs_4_), channel_id=1, source_target_pairs={{0,1},{1,0},{2,3},{3,2},{4,5},{5,4},{6,7},{7,6},{8,9},{9,8},{10,11... | collective-permute-start | bytes 1990664 | tf_op jit(solution)/shard_map/ppermute | solution.py:506
  72.3 30.7 %copy-start = (bf16[1296,256]{1,0:T(8,128)(2,1)}, bf16[1296,256]{1,0:T(8,128)(2,1)S(1)}, u32[]{:S(2)}) copy-start(bf16[1296,256]{1,0:T(8,128)(2,1)S(1)} %collective-permute-done.6.refs_6_) | copy-start | bytes 1990660
  72.3 30.7 %collective-permute-start.7 = (bf16[1296,256]{1,0:T(8,128)(2,1)S(1)}, bf16[1296,256]{1,0:T(8,128)(2,1)}, u32[]{:S(2)}, u32[]{:S(2)}) collective-permute-start(bf16[1296,256]{1,0:T(8,128)(2,1)S(1)} %collective-permute-done.6.refs_6_), channel_id=1, source_target_pairs={{0,1},{1,0},{2,3},{3,2},{4,5},{5,4},{6,7},{7,6},{8,9},{9,8},{10,11... | collective-permute-start | bytes 1990664 | tf_op jit(solution)/shard_map/ppermute | solution.py:506
  82.5 9.5 %all-to-all-start.3 = ((bf16[8,128,128]{2,1,0:T(8,128)(2,1)}), bf16[8,128,128]{2,1,0:T(8,128)(2,1)S(1)}, u32[]{:S(2)}, u32[]{:S(2)}) async-start(bf16[8,128,128]{2,1,0:T(8,128)(2,1)} %gated.1), calls=%async_computation.3 | async-start | bytes 524288 | tf_op jit(solution)/shard_map/all_to_all | solution.py:502
  112.2 4.5 %collective-permute-start.8 = (bf16[2,4,128,256]{3,2,1,0:T(8,128)(2,1)S(1)}, bf16[2,4,128,256]{3,2,1,0:T(8,128)(2,1)S(1)}, u32[]{:S(2)}, u32[]{:S(2)}) collective-permute-start(bf16[2,4,128,256]{3,2,1,0:T(8,128)(2,1)S(1)} %get-tuple-element.21), channel_id=1, source_target_pairs={{0,1},{1,0},{2,3},{3,2},{4,5},{5,4},{6,7},{7,6},{8,9},{9,8},{10,11... | collective-permute-start | bytes 1572872 | tf_op jit(solution)/shard_map/ppermute | solution.py:510
  119.8 23.3 %copy-start.7 = (f32[256]{0:T(256)S(1)}, f32[256]{0:T(256)}, u32[]{:S(2)}) copy-start(f32[256]{0:T(256)} %param.34) | copy-start | bytes 3076
  119.8 23.3 %copy-start.8 = (f32[256]{0:T(256)S(1)}, f32[256]{0:T(256)}, u32[]{:S(2)}) copy-start(f32[256]{0:T(256)} %param.35) | copy-start | bytes 3076
  119.8 15.3 %all-to-all-start.5 = ((bf16[8,128,256]{2,1,0:T(8,128)(2,1)}), bf16[8,128,256]{2,1,0:T(8,128)(2,1)S(1)}, u32[]{:S(2)}, u32[]{:S(2)}) async-start(bf16[8,128,256]{2,1,0:T(8,128)(2,1)} %bitcast.24), calls=%async_computation.5 | async-start | bytes 1048576 | tf_op jit(solution)/shard_map/all_to_all | solution.py:512
  (7 other events, 76.5 us)
Sparse Core Ops, SparseCore 0:
  19.2 81.4 all-gather.2

commit v6 on v5

--- a/solution.py
+++ b/solution.py
@@ -10,7 +10,7 @@
 D = 2048
 SP = ("z", "ya", "yb")
 TP = ("x", "c")
-HALF = 384
+HALF = 352
 QUARTER = 32
 
 highest_precision = lax.Precision.HIGHEST
@@ -216,14 +216,23 @@
 ANY = pl.BlockSpec(memory_space=pl.ANY)
 
 
+def turn_kernel(in_ref, out_ref):
+    for kind in range(3):
+        rows = jnp.concatenate([in_ref[y, kind] for y in range(4)], axis=0)
+        out_ref[kind] = rows.T
+
+
 def gathered_weights(gate, up, down):
     both = jnp.stack([gate, up, down.T])
-    first = both[:, :, :HALF]
-    second = jnp.pad(both[:, :, HALF:], ((0, 0), (0, 0), (0, 2 * HALF - both.shape[2])))
-    halves = jnp.stack([first, second, first, second])
-    arrived = lax.all_to_all(halves, ("ya", "yb"), 0, 0, tiled=True)
-    shard = jnp.moveaxis(arrived, 0, 1).reshape(3 * 128, HALF)
-    weights = lax.all_gather(shard, "z", axis=0, tiled=True).reshape(-1, 3, 128, HALF)
+    halves = [both[:, :, :HALF], both[:, :, HALF:]]
+    arrived = lax.all_to_all(jnp.stack(halves + halves), ("ya", "yb"), 0, 0, tiled=True)
+    shard = pl.pallas_call(
+        turn_kernel,
+        out_shape=jax.ShapeDtypeStruct((3, HALF, 128), jnp.bfloat16),
+        compiler_params=pltpu.CompilerParams(vmem_limit_bytes=6 << 20),
+        name="turn",
+    )(*near(arrived)).reshape(3 * HALF, 128)
+    weights = lax.all_gather(shard, "z", axis=0, tiled=True).reshape(-1, 3, HALF, 128)
     return pltpu.with_memory_space_constraint(weights, pltpu.HBM)
 
 
@@ -259,7 +268,7 @@
 
 
 def middle_kernel(place_ref, gated_ref, *refs):
-    block_refs, (out_ref, whole_ref, before_ref) = refs[:8], refs[8:]
+    block_refs, (out_ref, own_ref, whole_ref, before_ref) = refs[:8], refs[8:]
     heads, rows = 8, gated_ref.shape[2]
     count = 2 * rows
     for core in range(2):
@@ -289,19 +298,26 @@
         gain = vectors[0:1] + vectors[1:2] + vectors[2:3]
         bias = vectors[3:4] + vectors[4:5] + vectors[5:6]
         normed = (before_ref[b] - mean) * scale * gain + bias
-        out_ref[place_ref[b]] = normed.astype(jnp.bfloat16)
+        normed = normed.astype(jnp.bfloat16)
+        out_ref[place_ref[b]] = normed
+        if b == 0:
+            own_ref[...] = jnp.where(place_ref[heads] == 0, normed[:rows], normed[rows:])
 
 
 def middle_rows(gated, blocks):
     rows, width = gated.shape[2], blocks[0].shape[1]
     x, core = lax.axis_index("x"), lax.axis_index("c")
-    place = jnp.stack([2 * ((x - b // 2 + 4) % 4) + (core + b) % 2 for b in range(8)])
+    place = [2 * ((x - b // 2 + 4) % 4) + (core + b) % 2 for b in range(8)]
+    place = jnp.stack(place + [lax.axis_index("yb")])
     vmem = pl.BlockSpec(memory_space=pltpu.VMEM)
     return pl.pallas_call(
         middle_kernel,
         in_specs=[pl.BlockSpec(memory_space=pltpu.SMEM)] + [vmem] * 9,
-        out_specs=vmem,
-        out_shape=pltpu.VMEM((8, 2 * rows, width), jnp.bfloat16),
+        out_specs=[vmem, vmem],
+        out_shape=[
+            pltpu.VMEM((8, 2 * rows, width), jnp.bfloat16),
+            pltpu.VMEM((rows, width), jnp.bfloat16),
+        ],
         scratch_shapes=[
             pltpu.VMEM((2 * rows, 8 * 128), jnp.bfloat16),
             pltpu.VMEM((8, 2 * rows, width), jnp.float32),
@@ -311,18 +327,28 @@
     )(place.astype(jnp.int32), *near(gated), *blocks)
 
 
-def leaving(hidden, down):
-    wide = down.reshape(-1, down.shape[-1])
-    return lax.dot_general(
-        hidden, wide, (((1,), (1,)), ((), ())), preferred_element_type=jnp.float32
-    )
+def leaving(hidden, down_ref, block):
+    wide = jnp.concatenate([down_ref[2 * block], down_ref[2 * block + 1]], axis=1)
+    return jnp.dot(hidden, wide, preferred_element_type=jnp.float32)
+
+
+def down_copies(core, weights_ref, leave_ref, sem_ref):
+    copies = []
+    for s in range(4):
+        copies.append(
+            pltpu.make_async_copy(
+                weights_ref.at[pl.ds(4 * s + 2 * core, 2), 2],
+                leave_ref.at[pl.ds(2 * s, 2)],
+                sem_ref.at[s],
+            )
+        )
+    return copies
 
 
 def enter_kernel(
     core_ref, rows_ref, weights_ref, send_ref, hidden_ref, enter_ref, leave_ref, enter_sem, leave_sem
 ):
-    parts, blocks = 4, 4
-    each = enter_ref.shape[0] // parts
+    parts, each = 4, 4
     copies = []
     for s in range(parts):
         copies.append(
@@ -332,58 +358,50 @@
                 enter_sem.at[s],
             )
         )
-    for copy in copies:
+    downs = down_copies(1 - core_ref[0], weights_ref, leave_ref, leave_sem)
+    for copy in copies + downs:
         copy.start()
-    other = 1 - core_ref[0]
-    downs = []
-    for s in range(blocks):
-        downs.append(
-            pltpu.make_async_copy(
-                weights_ref.at[pl.ds(4 * s + 2 * other, 2), 2],
-                leave_ref.at[pl.ds(2 * s, 2)],
-                leave_sem.at[s],
-            )
-        )
-    for copy in downs:
-        copy.start()
-    gate = up = 0.0
+    sums = [0.0, 0.0]
     for s in range(parts):
         x = jnp.concatenate([rows_ref[2 * s], rows_ref[2 * s + 1]], axis=1)
         copies[s].wait()
-        wide = [enter_ref[s * each : (s + 1) * each, kind].reshape(-1, HALF) for kind in range(2)]
-        gate += jnp.dot(x, wide[0], preferred_element_type=jnp.float32)
-        up += jnp.dot(x, wide[1], preferred_element_type=jnp.float32)
+        for kind in range(2):
+            wide = [enter_ref[each * s + j, kind] for j in range(each)]
+            sums[kind] += lax.dot_general(
+                x,
+                jnp.concatenate(wide, axis=1),
+                (((1,), (1,)), ((), ())),
+                preferred_element_type=jnp.float32,
+            )
+    gate, up = sums
     hidden = (gate / (1.0 + jnp.exp(-gate)) * up).astype(jnp.bfloat16)
     hidden_ref[...] = hidden
     rows = send_ref.shape[2]
-    for s in range(blocks):
+    for s in range(4):
         downs[s].wait()
-        product = leaving(hidden, leave_ref[2 * s : 2 * s + 2]).astype(jnp.bfloat16)
+        product = leaving(hidden, leave_ref, s).astype(jnp.bfloat16)
         send_ref[0, s] = product[:rows]
         send_ref[1, s] = product[rows:]
 
 
-def leave_kernel(core_ref, other_ref, hidden_ref, weights_ref, out_ref, leave_ref, leave_sem):
-    blocks = 4
-    copies = []
-    for s in range(blocks):
-        copies.append(
-            pltpu.make_async_copy(
-                weights_ref.at[pl.ds(4 * s + 2 * core_ref[0], 2), 2],
-                leave_ref.at[pl.ds(2 * s, 2)],
-                leave_sem.at[s],
-            )
-        )
-    for copy in copies:
+def leave_kernel(core_ref, hidden_ref, weights_ref, out_ref, leave_ref, leave_sem):
+    downs = down_copies(core_ref[0], weights_ref, leave_ref, leave_sem)
+    for copy in downs:
         copy.start()
     hidden = hidden_ref[...]
     rows = out_ref.shape[2]
-    for s in range(blocks):
-        copies[s].wait()
-        product = leaving(hidden, leave_ref[2 * s : 2 * s + 2])
-        for pair in range(2):
-            mine = product[pair * rows : (pair + 1) * rows]
-            out_ref[pair, s] = (mine + other_ref[pair, s].astype(jnp.float32)).astype(jnp.bfloat16)
+    for s in range(4):
+        downs[s].wait()
+        product = leaving(hidden, leave_ref, s)
+        out_ref[0, s] = product[:rows]
+        out_ref[1, s] = product[rows:]
+
+
+def join_kernel(mine_ref, other_ref, out_ref):
+    for pair in range(2):
+        for s in range(4):
+            total = mine_ref[pair, s] + other_ref[pair, s].astype(jnp.float32)
+            out_ref[4 * pair + s] = total.astype(jnp.bfloat16)
 
 
 def feed_enter(core, rows, weights):
@@ -397,8 +415,8 @@
             pltpu.VMEM((count, HALF), jnp.bfloat16),
         ],
         scratch_shapes=[
-            pltpu.VMEM((16, 2, 128, HALF), jnp.bfloat16),
-            pltpu.VMEM((8, 128, HALF), jnp.bfloat16),
+            pltpu.VMEM((16, 2, HALF, 128), jnp.bfloat16),
+            pltpu.VMEM((8, HALF, 128), jnp.bfloat16),
             pltpu.SemaphoreType.DMA((4,)),
             pltpu.SemaphoreType.DMA((4,)),
         ],
@@ -410,22 +428,32 @@
     )(core, *near(rows), weights)
 
 
-def feed_leave(core, other, hidden, weights):
+def feed_leave(core, hidden, weights):
+    count = hidden.shape[0]
     return pl.pallas_call(
         leave_kernel,
-        in_specs=[SMEM, VMEM, VMEM, ANY],
+        in_specs=[SMEM, VMEM, ANY],
         out_specs=VMEM,
-        out_shape=pltpu.VMEM(other.shape, jnp.bfloat16),
+        out_shape=pltpu.VMEM((2, 4, count // 2, 256), jnp.float32),
         scratch_shapes=[
-            pltpu.VMEM((8, 128, HALF), jnp.bfloat16),
+            pltpu.VMEM((8, HALF, 128), jnp.bfloat16),
             pltpu.SemaphoreType.DMA((4,)),
         ],
         cost_estimate=pl.CostEstimate(
-            flops=hidden.shape[0] * D * HALF, bytes_accessed=D * HALF, transcendentals=0
+            flops=count * D * HALF, bytes_accessed=D * HALF, transcendentals=0
         ),
         compiler_params=pltpu.CompilerParams(vmem_limit_bytes=8 << 20),
         name="feed_leave",
-    )(core, *near(other, hidden), weights)
+    )(core, *near(hidden), weights)
+
+
+def joined(mine, other):
+    return pl.pallas_call(
+        join_kernel,
+        out_shape=pltpu.VMEM((8, *mine.shape[2:]), jnp.bfloat16),
+        compiler_params=pltpu.CompilerParams(vmem_limit_bytes=8 << 20),
+        name="join",
+    )(*near(mine, other))
 
 
 def diagonal_of(rows):
@@ -504,17 +532,12 @@
     both = []
     for block in blocks:
         both += [block, lax.ppermute(block, "c", SWAP)]
-    middle = middle_rows(everyone, both)
+    middle, own = middle_rows(everyone, both)
     core = lax.axis_index("c").astype(jnp.int32)[None]
     send, hidden = feed_enter(core, middle, weights)
-    joined = feed_leave(core, lax.ppermute(send, "c", SWAP), hidden, weights)
-    joined = joined.reshape(-1, *joined.shape[2:])
-    shares = lax.all_to_all(joined, ("yb", "x"), 0, 0, tiled=True)
-    own = lax.dynamic_slice(
-        middle,
-        (lax.axis_index(TP), lax.axis_index("yb") * rows, 0),
-        (1, rows, middle.shape[2]),
-    )[0]
+    other = lax.ppermute(send, "c", SWAP)
+    mine = feed_leave(core, hidden, weights)
+    shares = lax.all_to_all(joined(mine, other), ("yb", "x"), 0, 0, tiled=True)
     before_final, moments = pl.pallas_call(
         total_kernel,
         out_shape=[

time: 152 us -> 148 us (0.974)
  blocking collectives: 36.2 us -> 50.8 us
  waiting for transfers between devices: 24.8 us -> 13 us
  starting transfers between devices: 56.2 us -> 50.5 us
    all_to_all x1 -> x2, blocking collectives: 10.6 us -> 25.1 us  [the longest x1 14.6 us: layer(): shares = lax.all_to_all(joined(mine, other), ('yb', 'x'), 0, 0, tiled=True)]
    all_to_all x1 -> x0, waiting for transfers between devices: 10.2 us -> none  [layer(): shares = lax.all_to_all(joined, ('yb', 'x'), 0, 0, tiled=True)]
    all_to_all x1 -> x0, starting transfers between devices: 5.07 us -> none  [layer(): shares = lax.all_to_all(joined, ('yb', 'x'), 0, 0, tiled=True)]
    pallas_call x1 -> x3, Pallas kernels: 3.07 us -> 3.1 us  [the longest x1 2.09 us: feed_leave(): pl.pallas_call(leave_kernel, in_specs=[SMEM, VMEM, ANY], out_specs=VMEM,...]
  transfers between devices with their start and end apart: 14 -> 13, of which waited for: 5 -> 3; matrix products, arithmetic and copies ran while one was open for 0% -> 0% of each run, Pallas kernels for 5% -> 7%
where the time goes in v6:
time: 148 us; the launch traced here: 147 us
  blocking collectives  50.8 us (34%)
  starting transfers between devices  50.5 us (34%)
  Pallas kernels  15.8 us (11%)
  between operations  14 us (9%)
  waiting for transfers between devices  13 us (9%)
    all_to_all x1, starting transfers between devices, states_around(): others, = near(lax.all_to_all(totals, 'z', 0, 0, tiled=True))  15 us
    all_to_all x1, blocking collectives, layer(): shares = lax.all_to_all(joined(mine, other), ('yb', 'x'), 0, 0, tiled=True)  14.6 us
    ppermute x4, starting transfers between devices, layer(): both += [block, lax.ppermute(block, 'c', SWAP)]  13.6 us
    all_gather x1, blocking collectives, layer(): everyone = lax.all_gather(everyone, 'c')  11 us
    ppermute x3, starting transfers between devices, spread_over_x(): lax.ppermute(block, 'x', [(i, (i + k) % count) for i in range(count)])  10.7 us
    all_to_all x1, blocking collectives, gathered_weights(): lax.all_to_all(jnp.stack(halves + halves), ('ya', 'yb'), 0, 0, tiled=True)  10.5 us
    all_to_all x1, blocking collectives, layer(): moments = lax.all_to_all(moments, TP, 0, 0, tiled=True)  7.77 us
    all_to_all x1, blocking collectives, states_around(): return lax.all_to_all(before, ('ya', 'yb'), 0, 0, tiled=True)  6.9 us
  transfers between devices with their start and end apart: 13, of which 3 were waited for; matrix products, arithmetic and copies ran while one was open for 0% of the time, Pallas kernels for 7%

profile of v6, /device:TPU:1, one launch (start us, length us, event | category | flops | bytes accessed | tf_op | source)
XLA Modules:
  0.0 146.6 jit_solution(4871536435204627632)
XLA Ops:
  7.8 10.5 %all_to_all.35.in_ref = bf16[4,3,32,352]{3,2,1,0:T(8,128)(2,1)S(1)} all-to-all(bf16[4,3,32,352]{3,2,1,0:T(8,128)(2,1)S(1)} %pad_maximum_fusion), channel_id=1, replica_groups=mesh['z'=16,'ya'=2,'yb'=2,'x'=4,'c'=2] {'ya','yb'}, dimensions={0} | all-to-all | bytes 540672 | tf_op jit(solution)/shard_map/all_to_all | solution.py:228
  19.2 2.0 %local.1 = (f32[128,128]{1,0:T(8,128)S(1)}, f32[128,256]{1,0:T(8,128)S(1)}, bf16[4,72,128]{2,1,0:T(8,128)(2,1)}) custom-call(bf16[128,128]{1,0:T(8,128)(2,1)S(1)} %copy-done.3, bf16[128,128]{1,0:T(8,128)(2,1)S(1)} %copy-done.4, bf16[128,128]{1,0:T(8,128)(2,1)S(1)} %copy-done.5, bf16[128,128]{1,0:T(8,128)(2,1)S(1)} %copy-done.6, f32[1,128]{1,0:T(1,128)S(1)} %bitcast.32, ...), custom_call_target="tpu_custom_call" | custom-call | tf_op jit(solution)/shard_map/local/pallas_call | solution.py:89
  21.2 2.2 %collective-permute-start = (bf16[128,256]{1,0:T(8,128)(2,1)S(1)}, bf16[128,256]{1,0:T(8,128)(2,1)S(1)}, u32[]{:S(2)}, u32[]{:S(2)}) collective-permute-start(bf16[128,256]{1,0:T(8,128)(2,1)S(1)} %copy-done.14), channel_id=1, source_target_pairs={{0,8},{8,0},{1,9},{9,1},{2,10},{10,2},{3,11},{11,3},{4,12},{12,4},... | collective-permute-start | bytes 196616 | tf_op jit(solution)/shard_map/ppermute | solution.py:252
  23.6 2.6 %collective-permute-done = bf16[128,256]{1,0:T(8,128)(2,1)S(1)} collective-permute-done((bf16[128,256]{1,0:T(8,128)(2,1)S(1)}, bf16[128,256]{1,0:T(8,128)(2,1)S(1)}, u32[]{:S(2)}, u32[]{:S(2)}) %collective-permute-start) | collective-permute-done | bytes 65568 | tf_op jit(solution)/shard_map/ppermute | solution.py:252
  26.3 3.3 %collective-permute-start.2 = (bf16[1296,256]{1,0:T(8,128)(2,1)S(1)}, bf16[1296,256]{1,0:T(8,128)(2,1)S(1)}, u32[]{:S(2)}, u32[]{:S(2)}) collective-permute-start(bf16[1296,256]{1,0:T(8,128)(2,1)S(1)} %fusion.1.refs_0_), channel_id=1, source_target_pairs={{0,2},{2,4},{4,6},{6,0},{1,3},{3,5},{5,7},{7,1},{8,10},{10,12},{12... | collective-permute-start | bytes 1990664 | tf_op jit(solution)/shard_map/ppermute | solution.py:265
  29.6 4.4 %collective-permute-start.4 = (bf16[1296,256]{1,0:T(8,128)(2,1)S(1)}, bf16[1296,256]{1,0:T(8,128)(2,1)S(1)}, u32[]{:S(2)}, u32[]{:S(2)}) collective-permute-start(bf16[1296,256]{1,0:T(8,128)(2,1)S(1)} %fusion.1.refs_0_), channel_id=1, source_target_pairs={{0,4},{2,6},{4,0},{6,2},{1,5},{3,7},{5,1},{7,3},{8,12},{10,14},{12... | collective-permute-start | bytes 1990664 | tf_op jit(solution)/shard_map/ppermute | solution.py:265
  33.9 3.1 %collective-permute-start.6 = (bf16[1296,256]{1,0:T(8,128)(2,1)S(1)}, bf16[1296,256]{1,0:T(8,128)(2,1)S(1)}, u32[]{:S(2)}, u32[]{:S(2)}) collective-permute-start(bf16[1296,256]{1,0:T(8,128)(2,1)S(1)} %fusion.1.refs_0_), channel_id=1, source_target_pairs={{0,6},{2,0},{4,2},{6,4},{1,7},{3,1},{5,3},{7,5},{8,14},{10,8},{12,... | collective-permute-start | bytes 1990664 | tf_op jit(solution)/shard_map/ppermute | solution.py:265
  37.0 3.3 %all-to-all-start = ((bf16[4,72,128]{2,1,0:T(8,128)(2,1)}), bf16[4,72,128]{2,1,0:T(8,128)(2,1)S(1)}, u32[]{:S(2)}, u32[]{:S(2)}) async-start(bf16[4,72,128]{2,1,0:T(8,128)(2,1)} %get-tuple-element.18), calls=%async_computation | async-start | bytes 147456 | tf_op jit(solution)/shard_map/all_to_all | solution.py:167
  40.3 4.5 %all-to-all-done.arrived_ref = bf16[4,72,128]{2,1,0:T(8,128)(2,1)S(1)} async-done(((bf16[4,72,128]{2,1,0:T(8,128)(2,1)}), bf16[4,72,128]{2,1,0:T(8,128)(2,1)S(1)}, u32[]{:S(2)}, u32[]{:S(2)}) %all-to-all-start) | async-done | bytes 73760 | tf_op jit(solution)/shard_map/all_to_all | solution.py:167
  45.6 15.0 %all-to-all-start.1 = ((bf16[16,40,128]{2,1,0:T(8,128)(2,1)}), bf16[16,40,128]{2,1,0:T(8,128)(2,1)S(1)}, u32[]{:S(2)}, u32[]{:S(2)}) async-start(bf16[16,40,128]{2,1,0:T(8,128)(2,1)} %plane.1), calls=%async_computation.1 | async-start | bytes 327680 | tf_op jit(solution)/shard_map/all_to_all | solution.py:177
  60.6 7.4 %collective-permute-start.1 = (bf16[1296,256]{1,0:T(8,128)(2,1)S(1)}, bf16[1296,256]{1,0:T(8,128)(2,1)}, u32[]{:S(2)}, u32[]{:S(2)}) collective-permute-start(bf16[1296,256]{1,0:T(8,128)(2,1)S(1)} %fusion.1.refs_0_), channel_id=1, source_target_pairs={{0,1},{1,0},{2,3},{3,2},{4,5},{5,4},{6,7},{7,6},{8,9},{9,8},{10,11... | collective-permute-start | bytes 1990664 | tf_op jit(solution)/shard_map/ppermute | solution.py:534
  68.0 1.9 %collective-permute-start.3 = (bf16[1296,256]{1,0:T(8,128)(2,1)S(1)}, bf16[1296,256]{1,0:T(8,128)(2,1)}, u32[]{:S(2)}, u32[]{:S(2)}) collective-permute-start(bf16[1296,256]{1,0:T(8,128)(2,1)S(1)} %collective-permute-done.2.refs_2_), channel_id=1, source_target_pairs={{0,1},{1,0},{2,3},{3,2},{4,5},{5,4},{6,7},{7,6},{8,9},{9,8},{10,11... | collective-permute-start | bytes 1990664 | tf_op jit(solution)/shard_map/ppermute | solution.py:534
  69.9 2.4 %collective-permute-start.5 = (bf16[1296,256]{1,0:T(8,128)(2,1)S(1)}, bf16[1296,256]{1,0:T(8,128)(2,1)}, u32[]{:S(2)}, u32[]{:S(2)}) collective-permute-start(bf16[1296,256]{1,0:T(8,128)(2,1)S(1)} %collective-permute-done.4.refs_4_), channel_id=1, source_target_pairs={{0,1},{1,0},{2,3},{3,2},{4,5},{5,4},{6,7},{7,6},{8,9},{9,8},{10,11... | collective-permute-start | bytes 1990664 | tf_op jit(solution)/shard_map/ppermute | solution.py:534
  72.3 1.9 %collective-permute-start.7 = (bf16[1296,256]{1,0:T(8,128)(2,1)S(1)}, bf16[1296,256]{1,0:T(8,128)(2,1)}, u32[]{:S(2)}, u32[]{:S(2)}) collective-permute-start(bf16[1296,256]{1,0:T(8,128)(2,1)S(1)} %collective-permute-done.6.refs_6_), channel_id=1, source_target_pairs={{0,1},{1,0},{2,3},{3,2},{4,5},{5,4},{6,7},{7,6},{8,9},{9,8},{10,11... | collective-permute-start | bytes 1990664 | tf_op jit(solution)/shard_map/ppermute | solution.py:534
  74.4 6.9 %all_to_all.36.back_ref = bf16[4,64,128]{2,1,0:T(8,128)(2,1)S(1)} all-to-all(bf16[4,64,128]{2,1,0:T(8,128)(2,1)S(1)} %before.1), channel_id=1, replica_groups=mesh['z'=16,'ya'=2,'yb'=2,'x'=4,'c'=2] {'ya','yb'}, dimensions={0} | all-to-all | bytes 131072 | tf_op jit(solution)/shard_map/all_to_all | solution.py:186
  82.5 3.4 %all-to-all-start.3 = ((bf16[8,128,128]{2,1,0:T(8,128)(2,1)}), bf16[8,128,128]{2,1,0:T(8,128)(2,1)S(1)}, u32[]{:S(2)}, u32[]{:S(2)}) async-start(bf16[8,128,128]{2,1,0:T(8,128)(2,1)} %gated.1), calls=%async_computation.3 | async-start | bytes 524288 | tf_op jit(solution)/shard_map/all_to_all | solution.py:530
  86.1 5.9 %all-to-all-done.3 = bf16[8,128,128]{2,1,0:T(8,128)(2,1)S(1)} async-done(((bf16[8,128,128]{2,1,0:T(8,128)(2,1)}), bf16[8,128,128]{2,1,0:T(8,128)(2,1)S(1)}, u32[]{:S(2)}, u32[]{:S(2)}) %all-to-all-start.3) | async-done | bytes 262176 | tf_op jit(solution)/shard_map/all_to_all | solution.py:530
  92.0 11.0 %all-gather = bf16[16,128,128]{2,1,0:T(8,128)(2,1)S(1)} all-gather(bf16[8,128,128]{2,1,0:T(8,128)(2,1)S(1)} %all-to-all-done.3), channel_id=2, replica_groups=mesh['z'=16,'ya'=2,'yb'=2,'x'=4,'c'=2] {'c'}, dimensions={0}, use_global_device_ids=true | all-gather | bytes 786432 | tf_op jit(solution)/shard_map/all_gather | solution.py:531
  104.1 3.7 %middle.1 = (bf16[8,256,256]{2,1,0:T(8,128)(2,1)S(1)}, bf16[128,256]{1,0:T(8,128)(2,1)S(1)}) custom-call(s32[9]{0:T(128)S(1)} %stack.83.place_ref, bf16[2,8,128,128]{3,2,1,0:T(8,128)(2,1)S(1)} %bitcast.29, bf16[1296,256]{1,0:T(8,128)(2,1)S(1)} %fusion.1.refs_0_, bf16[1296,256]{1,0:T(8,128)(2,1)} %collective-permute-done.1.refs_1_, ...), custom_call_target="tpu_custom_call" | custom-call | tf_op jit(solution)/shard_map/middle/pallas_call | solution.py:313
  107.8 4.0 %feed_enter.1 = (bf16[2,4,128,256]{3,2,1,0:T(8,128)(2,1)S(1)}, bf16[256,352]{1,0:T(8,128)(2,1)S(1)}) custom-call(s32[1]{0:T(128)} %bitcast.core_ref, bf16[8,256,256]{2,1,0:T(8,128)(2,1)S(1)} %get-tuple-element.23.rows_ref, bf16[16,3,352,128]{3,2,1,0:T(8,128)(2,1)} %bitcast.36), custom_call_target="tpu_custom_call" | custom-call | flops 922746880 | bytes 3604480 | tf_op jit(solution)/shard_map/feed_enter/pallas_call | solution.py:409
  111.9 2.3 %collective-permute-start.8 = (bf16[2,4,128,256]{3,2,1,0:T(8,128)(2,1)S(1)}, bf16[2,4,128,256]{3,2,1,0:T(8,128)(2,1)S(1)}, u32[]{:S(2)}, u32[]{:S(2)}) collective-permute-start(bf16[2,4,128,256]{3,2,1,0:T(8,128)(2,1)S(1)} %get-tuple-element.25), channel_id=1, source_target_pairs={{0,1},{1,0},{2,3},{3,2},{4,5},{5,4},{6,7},{7,6},{8,9},{9,8},{10,11... | collective-permute-start | bytes 1572872 | tf_op jit(solution)/shard_map/ppermute | solution.py:538
  114.2 2.1 %feed_leave.1.mine_ref = f32[2,4,128,256]{3,2,1,0:T(8,128)S(1)} custom-call(s32[1]{0:T(128)} %bitcast.core_ref, bf16[256,352]{1,0:T(8,128)(2,1)S(1)} %get-tuple-element.24.hidden_ref, bf16[16,3,352,128]{3,2,1,0:T(8,128)(2,1)} %bitcast.37), custom_call_target="tpu_custom_call" | custom-call | flops 184549376 | bytes 720896 | tf_op jit(solution)/shard_map/feed_leave/pallas_call | solution.py:433
  116.4 14.6 %all_to_all.37.arrived_ref = bf16[8,128,256]{2,1,0:T(8,128)(2,1)S(1)} all-to-all(bf16[8,128,256]{2,1,0:T(8,128)(2,1)S(1)} %join.1), channel_id=1, replica_groups=mesh['z'=16,'ya'=2,'yb'=2,'x'=4,'c'=2] {'yb','x'}, dimensions={0} | all-to-all | bytes 1048576 | tf_op jit(solution)/shard_map/all_to_all | solution.py:540
  131.2 7.8 %all_to_all.38.moments_ref = f32[8,1,256]{2,1,0:T(1,128)S(1)} all-to-all(f32[8,1,256]{2,1,0:T(1,128)S(1)} %get-tuple-element.27), channel_id=1, replica_groups=mesh['z'=16,'ya'=2,'yb'=2,'x'=4,'c'=2] {'x','c'}, dimensions={0} | all-to-all | bytes 16384 | tf_op jit(solution)/shard_map/all_to_all | solution.py:550
  (68 shorter events, 6.6 us)
Async XLA Ops:
  6.5 12.7 %copy-start.5 = (bf16[128,128]{1,0:T(8,128)(2,1)S(1)}, bf16[128,128]{1,0:T(8,128)(2,1)}, u32[]{:S(2)}) copy-start(bf16[128,128]{1,0:T(8,128)(2,1)} %onward_ref.1) | copy-start | bytes 98308
  6.6 12.7 %copy-start.6 = (bf16[128,128]{1,0:T(8,128)(2,1)S(1)}, bf16[128,128]{1,0:T(8,128)(2,1)}, u32[]{:S(2)}) copy-start(bf16[128,128]{1,0:T(8,128)(2,1)} %reverse_ref.1) | copy-start | bytes 98308
  6.6 14.6 %copy-start.14 = (bf16[128,256]{1,0:T(8,128)(2,1)S(1)}, bf16[128,256]{1,0:T(8,128)(2,1)}, u32[]{:S(2)}) copy-start(bf16[128,256]{1,0:T(8,128)(2,1)} %param.27) | copy-start | bytes 196612
  6.6 16.8 %copy-start.15 = (f32[256]{0:T(256)S(1)}, f32[256]{0:T(256)}, u32[]{:S(2)}) copy-start(f32[256]{0:T(256)} %param.29) | copy-start | bytes 3076
  6.6 16.8 %copy-start.16 = (f32[256]{0:T(256)S(1)}, f32[256]{0:T(256)}, u32[]{:S(2)}) copy-start(f32[256]{0:T(256)} %param.30) | copy-start | bytes 3076
  6.6 101.2 %all-gather.3.cloned.1.call-start = ((), (), s32[]{:S(2)}) async-start(), calls=%async_computation.7 | async-start | bytes 4595712 | tf_op jit(solution)/shard_map/all_gather | solution.py:235
  7.6 18.6 %copy-start.13 = (bf16[1024,256]{1,0:T(8,128)(2,1)S(1)}, bf16[1024,256]{1,0:T(8,128)(2,1)}, u32[]{:S(2)}) copy-start(bf16[1024,256]{1,0:T(8,128)(2,1)} %param.28) | copy-start | bytes 1572868
  21.2 5.0 %collective-permute-start = (bf16[128,256]{1,0:T(8,128)(2,1)S(1)}, bf16[128,256]{1,0:T(8,128)(2,1)S(1)}, u32[]{:S(2)}, u32[]{:S(2)}) collective-permute-start(bf16[128,256]{1,0:T(8,128)(2,1)S(1)} %copy-done.14), channel_id=1, source_target_pairs={{0,8},{8,0},{1,9},{9,1},{2,10},{10,2},{3,11},{11,3},{4,12},{12,4},... | collective-permute-start | bytes 196616 | tf_op jit(solution)/shard_map/ppermute | solution.py:252
  23.5 57.8 %copy-start.2 = (bf16[128,128]{1,0:T(8,128)(2,1)S(1)}, bf16[128,128]{1,0:T(8,128)(2,1)}, u32[]{:S(2)}) copy-start(bf16[128,128]{1,0:T(8,128)(2,1)} %gate_ref.1) | copy-start | bytes 98308
  23.6 57.8 %copy-start.12 = (f32[128]{0:T(128)S(1)}, f32[128]{0:T(128)}, u32[]{:S(2)}) copy-start(f32[128]{0:T(128)} %param.26) | copy-start | bytes 1540
  26.3 41.7 %collective-permute-start.2 = (bf16[1296,256]{1,0:T(8,128)(2,1)S(1)}, bf16[1296,256]{1,0:T(8,128)(2,1)S(1)}, u32[]{:S(2)}, u32[]{:S(2)}) collective-permute-start(bf16[1296,256]{1,0:T(8,128)(2,1)S(1)} %fusion.1.refs_0_), channel_id=1, source_target_pairs={{0,2},{2,4},{4,6},{6,0},{1,3},{3,5},{5,7},{7,1},{8,10},{10,12},{12... | collective-permute-start | bytes 1990664 | tf_op jit(solution)/shard_map/ppermute | solution.py:265
  29.6 40.3 %collective-permute-start.4 = (bf16[1296,256]{1,0:T(8,128)(2,1)S(1)}, bf16[1296,256]{1,0:T(8,128)(2,1)S(1)}, u32[]{:S(2)}, u32[]{:S(2)}) collective-permute-start(bf16[1296,256]{1,0:T(8,128)(2,1)S(1)} %fusion.1.refs_0_), channel_id=1, source_target_pairs={{0,4},{2,6},{4,0},{6,2},{1,5},{3,7},{5,1},{7,3},{8,12},{10,14},{12... | collective-permute-start | bytes 1990664 | tf_op jit(solution)/shard_map/ppermute | solution.py:265
  33.9 38.4 %collective-permute-start.6 = (bf16[1296,256]{1,0:T(8,128)(2,1)S(1)}, bf16[1296,256]{1,0:T(8,128)(2,1)S(1)}, u32[]{:S(2)}, u32[]{:S(2)}) collective-permute-start(bf16[1296,256]{1,0:T(8,128)(2,1)S(1)} %fusion.1.refs_0_), channel_id=1, source_target_pairs={{0,6},{2,0},{4,2},{6,4},{1,7},{3,1},{5,3},{7,5},{8,14},{10,8},{12,... | collective-permute-start | bytes 1990664 | tf_op jit(solution)/shard_map/ppermute | solution.py:265
  37.0 7.8 %all-to-all-start = ((bf16[4,72,128]{2,1,0:T(8,128)(2,1)}), bf16[4,72,128]{2,1,0:T(8,128)(2,1)S(1)}, u32[]{:S(2)}, u32[]{:S(2)}) async-start(bf16[4,72,128]{2,1,0:T(8,128)(2,1)} %get-tuple-element.18), calls=%async_computation | async-start | bytes 147456 | tf_op jit(solution)/shard_map/all_to_all | solution.py:167
  45.6 28.7 %all-to-all-start.1 = ((bf16[16,40,128]{2,1,0:T(8,128)(2,1)}), bf16[16,40,128]{2,1,0:T(8,128)(2,1)S(1)}, u32[]{:S(2)}, u32[]{:S(2)}) async-start(bf16[16,40,128]{2,1,0:T(8,128)(2,1)} %plane.1), calls=%async_computation.1 | async-start | bytes 327680 | tf_op jit(solution)/shard_map/all_to_all | solution.py:177
  60.6 42.4 %collective-permute-start.1 = (bf16[1296,256]{1,0:T(8,128)(2,1)S(1)}, bf16[1296,256]{1,0:T(8,128)(2,1)}, u32[]{:S(2)}, u32[]{:S(2)}) collective-permute-start(bf16[1296,256]{1,0:T(8,128)(2,1)S(1)} %fusion.1.refs_0_), channel_id=1, source_target_pairs={{0,1},{1,0},{2,3},{3,2},{4,5},{5,4},{6,7},{7,6},{8,9},{9,8},{10,11... | collective-permute-start | bytes 1990664 | tf_op jit(solution)/shard_map/ppermute | solution.py:534
  68.0 35.0 %collective-permute-start.3 = (bf16[1296,256]{1,0:T(8,128)(2,1)S(1)}, bf16[1296,256]{1,0:T(8,128)(2,1)}, u32[]{:S(2)}, u32[]{:S(2)}) collective-permute-start(bf16[1296,256]{1,0:T(8,128)(2,1)S(1)} %collective-permute-done.2.refs_2_), channel_id=1, source_target_pairs={{0,1},{1,0},{2,3},{3,2},{4,5},{5,4},{6,7},{7,6},{8,9},{9,8},{10,11... | collective-permute-start | bytes 1990664 | tf_op jit(solution)/shard_map/ppermute | solution.py:534
  69.9 33.1 %collective-permute-start.5 = (bf16[1296,256]{1,0:T(8,128)(2,1)S(1)}, bf16[1296,256]{1,0:T(8,128)(2,1)}, u32[]{:S(2)}, u32[]{:S(2)}) collective-permute-start(bf16[1296,256]{1,0:T(8,128)(2,1)S(1)} %collective-permute-done.4.refs_4_), channel_id=1, source_target_pairs={{0,1},{1,0},{2,3},{3,2},{4,5},{5,4},{6,7},{7,6},{8,9},{9,8},{10,11... | collective-permute-start | bytes 1990664 | tf_op jit(solution)/shard_map/ppermute | solution.py:534
  72.3 30.7 %copy-start = (bf16[1296,256]{1,0:T(8,128)(2,1)}, bf16[1296,256]{1,0:T(8,128)(2,1)S(1)}, u32[]{:S(2)}) copy-start(bf16[1296,256]{1,0:T(8,128)(2,1)S(1)} %collective-permute-done.6.refs_6_) | copy-start | bytes 1990660
  72.3 30.7 %collective-permute-start.7 = (bf16[1296,256]{1,0:T(8,128)(2,1)S(1)}, bf16[1296,256]{1,0:T(8,128)(2,1)}, u32[]{:S(2)}, u32[]{:S(2)}) collective-permute-start(bf16[1296,256]{1,0:T(8,128)(2,1)S(1)} %collective-permute-done.6.refs_6_), channel_id=1, source_target_pairs={{0,1},{1,0},{2,3},{3,2},{4,5},{5,4},{6,7},{7,6},{8,9},{9,8},{10,11... | collective-permute-start | bytes 1990664 | tf_op jit(solution)/shard_map/ppermute | solution.py:534
  82.5 9.5 %all-to-all-start.3 = ((bf16[8,128,128]{2,1,0:T(8,128)(2,1)}), bf16[8,128,128]{2,1,0:T(8,128)(2,1)S(1)}, u32[]{:S(2)}, u32[]{:S(2)}) async-start(bf16[8,128,128]{2,1,0:T(8,128)(2,1)} %gated.1), calls=%async_computation.3 | async-start | bytes 524288 | tf_op jit(solution)/shard_map/all_to_all | solution.py:530
  111.9 4.4 %collective-permute-start.8 = (bf16[2,4,128,256]{3,2,1,0:T(8,128)(2,1)S(1)}, bf16[2,4,128,256]{3,2,1,0:T(8,128)(2,1)S(1)}, u32[]{:S(2)}, u32[]{:S(2)}) collective-permute-start(bf16[2,4,128,256]{3,2,1,0:T(8,128)(2,1)S(1)} %get-tuple-element.25), channel_id=1, source_target_pairs={{0,1},{1,0},{2,3},{3,2},{4,5},{5,4},{6,7},{7,6},{8,9},{9,8},{10,11... | collective-permute-start | bytes 1572872 | tf_op jit(solution)/shard_map/ppermute | solution.py:538
  116.4 22.6 %copy-start.7 = (f32[256]{0:T(256)S(1)}, f32[256]{0:T(256)}, u32[]{:S(2)}) copy-start(f32[256]{0:T(256)} %param.34) | copy-start | bytes 3076
  116.4 22.6 %copy-start.8 = (f32[256]{0:T(256)S(1)}, f32[256]{0:T(256)}, u32[]{:S(2)}) copy-start(f32[256]{0:T(256)} %param.35) | copy-start | bytes 3076
  (6 other events, 64.3 us)
Sparse Core Ops, SparseCore 0:
  19.3 79.7 all-gather.2
